TPU v7x, 256 devices: a 4x2x16 block of a 4x16x16 slice. The times are simulated.
256 devices in a mesh: grp: 2 (over y), sp: 32 (over z, core), tp: 4 (over x).
Axes of the slice: x: 4, y: 2, z: 16, core: 2. Of those that a mesh axis runs over, the one named last changes fastest.
The devices are a block of a 4x16x16 slice.
Arguments:
- residual: bfloat16 [32768, 2048], P(('grp', 'sp', 'tp')), parts along dimension 0, may hold values from -6 to 6
- queries: bfloat16 [32768, 2048], P(('grp', 'sp'), 'tp'), parts along dimension 0, may hold values from -200 to 200
- key_heads: bfloat16 [32768, 256], P(('grp', 'sp'), 'tp'), parts along dimension 0, may hold values from -8 to 8
- value_heads: bfloat16 [32768, 256], P(('grp', 'sp'), 'tp'), parts along dimension 0, may hold values from -6 to 6
- documents: int32 [32768], P(('grp', 'sp')), parts along dimension 0, may hold values from 0 to 7, never falling along the last dimension, each value on 1 to 8192 neighbouring positions
- sink_logits: float32 [32], P('tp'), may hold values from 4 to 7
- out_weight: bfloat16 [2048, 2048], P('tp'), may hold values from -1 to 1
- norm_gain: bfloat16 [2048], replicated, may hold values from 0.099609375 to 1.8984375
- gate_weight: bfloat16 [2048, 5632], P('sp', 'tp'), may hold values from -0.125 to 0.125
- up_weight: bfloat16 [2048, 5632], P('sp', 'tp'), may hold values from -0.125 to 0.125
- down_weight: bfloat16 [2048, 5632], P('sp', 'tp'), may hold values from -0.078125 to 0.078125
Outputs:
- updated: bfloat16 [32768, 2048], P(('grp', 'sp', 'tp')), parts along dimension 0
There are 2 independent parts, one for each index of `grp`. A program takes and returns all parts, laid end to end along the dimension named above; an argument that names none is the same for every part. Nothing has to cross between parts.
Inputs may be any that keep to these rules, and one draw needn't show every extreme that they name: `documents`: document numbers never fall along the sequence.
All inputs are finite; a program needn't handle non-finite values.
Results may differ from a plain program's by a relative error of at most 0.012.
Values may be sent and summed in bfloat16 or wider, within the bound.
No kernel may reach another device: no remote copies, remote signals or barrier semaphores. Data moves between devices by JAX's collectives and lax.ppermute only.
A program may use at most 128 MiB of HBM per device.

v0:
```python
import jax
import jax.numpy as jnp
from jax import lax
from jax.sharding import PartitionSpec as P

HD = 64
WINDOW = 128


epsilon = 1e-06
masked = -1e30


def padded(shard, sides, width):
    for axis, dim in sides:
        size, length = (lax.axis_size(axis), shard.shape[dim])
        up = [(i, (i + 1) % size) for i in range(size - 1)]
        down = [(j, i) for i, j in up]
        last = lax.slice_in_dim(shard, length - width, length, axis=dim)
        initial = lax.slice_in_dim(shard, 0, width, axis=dim)
        before = lax.ppermute(last, axis, up)
        after = lax.ppermute(initial, axis, down)
        shard = jnp.concatenate([before, shard, after], axis=dim)
    return shard


def split_up(shard, dim, length):
    dims = shard.shape
    blocks = shard.reshape(*dims[:dim], length, dims[dim] // length, *dims[dim + 1 :])
    return jnp.moveaxis(blocks, dim, 0)


def sent_and_summed(shard, axis, dim):
    length = lax.axis_size(axis)
    blocks = lax.all_to_all(split_up(shard, dim, length), axis, 0, 0, tiled=True)
    return jnp.sum(blocks.astype(jnp.float32), axis=0)


def in_one_piece(arrays, axis, dim, along):
    widths = [a.shape[along] for a in arrays]
    both = jnp.concatenate(arrays, axis=along)
    out = lax.all_gather(both, axis, axis=dim, tiled=True)
    return tuple(jnp.split(out, [sum(widths[:k]) for k in range(1, len(widths))], axis=along))


def in_order(blocks, dim):
    dims = list(blocks.shape[1:])
    dims[dim] *= blocks.shape[0]
    return jnp.moveaxis(blocks, 0, dim).reshape(dims)


def sent_to_all(shard, axis):
    copies = jnp.broadcast_to(shard, (lax.axis_size(axis), *shard.shape))
    return lax.all_to_all(copies, axis, split_axis=0, concat_axis=0, tiled=True)


def gathered_copies(shard, axis, dim):
    return in_order(sent_to_all(shard, axis), dim)


def on_device(
    residual,
    queries,
    key_heads,
    value_heads,
    documents,
    sink_logits,
    out_weight,
    norm_gain,
    gate_weight,
    up_weight,
    down_weight,
):
    tok_rows = queries.shape[0]
    kv_local = key_heads.shape[1] // HD
    q_local = queries.shape[1] // HD
    groups = q_local // kv_local
    own_docs = documents.astype(jnp.bfloat16)
    spread_keys, spread_values, spread_docs = (
        padded(key_heads, (("sp", 0),), WINDOW),
        padded(value_heads, (("sp", 0),), WINDOW),
        padded(own_docs, (("sp", 0),), WINDOW),
    )
    offset = lax.axis_index("sp") * tok_rows
    total_length = tok_rows * lax.axis_size("sp")
    query_pos = offset + jnp.arange(tok_rows, dtype=jnp.int32)
    key_pos = offset - WINDOW + jnp.arange(tok_rows + 2 * WINDOW, dtype=jnp.int32)
    allowed = (
        (jnp.abs(query_pos[:, None] - key_pos[None, :]) <= WINDOW)
        & (key_pos >= 0)[None, :]
        & (key_pos < total_length)[None, :]
        & (own_docs[:, None] == spread_docs[None, :])
    )
    query_block = queries.reshape(tok_rows, kv_local, groups, HD)
    key_block = spread_keys.reshape(-1, kv_local, HD)
    value_block = spread_values.reshape(-1, kv_local, HD)
    scores = jnp.einsum(
        "qkgd,jkd->kgqj", query_block, key_block, preferred_element_type=jnp.float32
    ) * HD ** (-0.5)
    scores = jnp.where(allowed[None, None], scores, masked)
    sink_table = sink_logits.reshape(kv_local, groups)[:, :, None]
    row_max = jnp.maximum(jnp.max(scores, axis=-1), sink_table)
    expo = jnp.exp(scores - row_max[..., None])
    total = jnp.sum(expo, axis=-1) + jnp.exp(sink_table - row_max)
    probs = (expo / total[..., None]).astype(jnp.bfloat16)
    mixed = jnp.einsum("kgqj,jkd->qkgd", probs, value_block, preferred_element_type=jnp.float32)
    attended = mixed.reshape(tok_rows, q_local * HD).astype(jnp.bfloat16)
    projected = sent_and_summed(
        jnp.dot(attended, out_weight, preferred_element_type=jnp.float32).astype(jnp.bfloat16),
        "tp",
        0,
    ).astype(jnp.bfloat16)
    middle = (
        residual.astype(jnp.float32) + lax.optimization_barrier(projected).astype(jnp.float32)
    ).astype(jnp.bfloat16)
    middle_wide = middle.astype(jnp.float32)
    scaled = middle_wide * lax.rsqrt(
        jnp.mean(middle_wide * middle_wide, axis=-1, keepdims=True) + epsilon
    )
    normed = (scaled * norm_gain.astype(jnp.float32)).astype(jnp.bfloat16)
    whole_gate, whole_up, whole_down = in_one_piece(
        (gate_weight, up_weight, down_weight), "sp", 0, 1
    )
    row_piece = gathered_copies(normed, "tp", 0)
    gate_value = jnp.dot(row_piece, whole_gate, preferred_element_type=jnp.float32)
    up_value = jnp.dot(row_piece, whole_up, preferred_element_type=jnp.float32)
    hidden = (jax.nn.silu(gate_value) * up_value).astype(jnp.bfloat16)
    mixer_out = sent_and_summed(
        lax.dot_general(
            hidden, whole_down, (((1,), (1,)), ((), ())), preferred_element_type=jnp.float32
        ).astype(jnp.bfloat16),
        "tp",
        0,
    ).astype(jnp.bfloat16)
    updated = middle.astype(jnp.float32) + 0.5 * lax.optimization_barrier(mixer_out).astype(
        jnp.float32
    )
    return updated.astype(jnp.bfloat16)


def solution(mesh):
    return jax.shard_map(
        on_device,
        mesh=mesh,
        in_specs=(
            P(("grp", "sp", "tp"), None),
            P(("grp", "sp"), "tp"),
            P(("grp", "sp"), "tp"),
            P(("grp", "sp"), "tp"),
            P(("grp", "sp")),
            P("tp"),
            P("tp", None),
            P(),
            P("sp", "tp"),
            P("sp", "tp"),
            P("sp", "tp"),
        ),
        out_specs=P(("grp", "sp", "tp"), None),
        check_vma=False,
    )
```

profile of v0, /device:TPU:33, one launch (start us, length us, event | category | flops | bytes accessed | tf_op | source)
XLA Modules:
  0.0 196.3 jit_solution(10482502472398155545)
XLA Ops:
  6.5 0.0 copy-start
  6.6 0.0 copy-start.2
  6.6 0.0 all-gather.2.cloned.1.call-start
  6.6 2.1 %pad_maximum_fusion = bf16[64,4224]{1,0:T(8,128)(2,1)} fusion(bf16[64,1408]{1,0:T(8,128)(2,1)} %param.21, bf16[64,1408]{1,0:T(8,128)(2,1)} %param.20, bf16[64,1408]{1,0:T(8,128)(2,1)} %param.19), kind=kLoop, calls=%fused_computation.31 | loop fusion | flops 1622016 | bytes 1081344 | tf_op jit(solution)/shard_map/concatenate | solution.py:41
  8.7 0.1 all-gather.2.cloned.1.call-update
  8.7 0.7 convert_element_type.57
  9.4 5.7 %collective-permute-start.2 = (bf16[128]{0:T(256)(128)(2,1)S(1)}, bf16[128]{0:T(256)(128)(2,1)S(1)}, u32[]{:S(2)}, u32[]{:S(2)}) collective-permute-start(bf16[128]{0:T(256)(128)(2,1)S(1)} %get-tuple-element.9), channel_id=1, source_target_pairs={{0,4},{4,8},{8,12},{12,16},{16,20},{20,24},{24,28},{28,32},{32,36}... | collective-permute-start | bytes 776 | tf_op jit(solution)/shard_map/ppermute | solution.py:21
  15.2 17.9 %collective-permute-start.3 = (bf16[128]{0:T(256)(128)(2,1)S(1)}, bf16[128]{0:T(256)(128)(2,1)S(1)}, u32[]{:S(2)}, u32[]{:S(2)}) collective-permute-start(bf16[128]{0:T(256)(128)(2,1)S(1)} %get-tuple-element.10), channel_id=1, source_target_pairs={{4,0},{8,4},{12,8},{16,12},{20,16},{24,20},{28,24},{32,28},{36,32}... | collective-permute-start | bytes 776 | tf_op jit(solution)/shard_map/ppermute | solution.py:22
  33.1 0.7 fusion.49
  33.8 1.9 collective-permute-start.4
  35.8 2.4 %collective-permute-start.5 = (bf16[128,64]{0,1:T(8,128)(2,1)S(1)}, bf16[128,64]{0,1:T(8,128)(2,1)S(1)}, u32[]{:S(2)}, u32[]{:S(2)}) collective-permute-start(bf16[128,64]{0,1:T(8,128)(2,1)S(1)} %get-tuple-element.8), channel_id=1, source_target_pairs={{4,0},{8,4},{12,8},{16,12},{20,16},{24,20},{28,24},{32,28},{36,32}... | collective-permute-start | bytes 49160 | tf_op jit(solution)/shard_map/ppermute | solution.py:22
  38.2 0.8 fusion.48
  39.0 3.1 %collective-permute-start = (bf16[128,64]{0,1:T(8,128)(2,1)S(1)}, bf16[128,64]{0,1:T(8,128)(2,1)S(1)}, u32[]{:S(2)}, u32[]{:S(2)}) collective-permute-start(bf16[128,64]{0,1:T(8,128)(2,1)S(1)} %get-tuple-element.5), channel_id=1, source_target_pairs={{0,4},{4,8},{8,12},{12,16},{16,20},{20,24},{24,28},{28,32},{32,36}... | collective-permute-start | bytes 49160 | tf_op jit(solution)/shard_map/ppermute | solution.py:21
  42.2 1.3 copy.14
  43.4 0.0 collective-permute-done.2
  43.4 2.0 collective-permute-start.1
  45.4 0.0 collective-permute-done.3
  45.4 1.0 fusion.23
  46.4 0.0 collective-permute-done.4
  46.4 0.0 collective-permute-done.5
  46.4 0.0 copy-done.2
  46.5 0.0 copy-start.5
  46.5 2.0 %fusion.1 = (f32[8,512]{1,0:T(8,128)S(1)}, f32[768,512,8]{1,0,2:T(8,128)S(1)}) fusion(pred[512,768]{0,1:T(8,128)(4,1)S(1)} %fusion.23, bf16[512,8,64]{0,2,1:T(8,128)(2,1)S(1)} %bitcast.46, bf16[128,64]{0,1:T(8,128)(2,1)S(1)} %collective-permute-done.5, bf16[512,64]{0,1:T(8,128)(2,1)S(1)} %copy-done.2, bf16[128,64]{0,1:T(8,128)(2,1)S(1)} %collective-permute-done.4), kind=kOutput, calls=%fused_computation.4 | convolution fusion | flops 412381184 | bytes 13615104 | tf_op jit(solution)/shard_map/qkgd,jkd->kgqj/dot_general | solution.py:97
  48.5 0.0 copy-done.5
  48.5 0.1 broadcast_maximum_fusion
  48.6 2.6 %fusion = f32[8,512]{1,0:T(8,128)S(1)} fusion(f32[768,512,8]{1,0,2:T(8,128)S(1)} %get-tuple-element.12, f32[8,512]{1,0:T(8,128)S(1)} %broadcast_maximum_fusion, pred[512,768]{0,1:T(8,128)(4,1)S(1)} %fusion.23), kind=kLoop, calls=%fused_computation.3 | loop fusion | flops 12578816 | bytes 13008896 | tf_op jit(solution)/shard_map/reduce_sum | solution.py:104
  51.2 0.1 exponential_add_fusion
  51.3 0.0 collective-permute-done
  51.3 0.0 collective-permute-done.1
  51.3 0.0 copy-done.3
  51.3 3.6 %fusion.25 = bf16[64,8,512]{2,0,1:T(8,128)(2,1)S(1)} fusion(f32[8,512]{1,0:T(8,128)S(1)} %exponential_add_fusion, f32[8,512]{1,0:T(8,128)S(1)} %broadcast_maximum_fusion, f32[768,512,8]{1,0,2:T(8,128)S(1)} %get-tuple-element.12, pred[512,768]{0,1:T(8,128)(4,1)S(1)} %fusion.23, bf16[128,64]{0,1:T(8,128)(2,1)S(1)} %collective-permute-done.1, ...), kind=kOutput, calls=%fused_computation.25 | convolution fusion | flops 418938880 | bytes 13631488 | tf_op jit(solution)/shard_map/kgqj,jkd->qkgd/dot_general | solution.py:106
  54.9 0.0 copy-done
  54.9 2.6 %convolution_convert_fusion = bf16[512,2048]{1,0:T(8,128)(2,1)} fusion(bf16[512,512]{0,1:T(8,128)(2,1)S(1)} %bitcast.47, bf16[512,2048]{1,0:T(8,128)(2,1)S(1)} %copy-done), kind=kOutput, calls=%fused_computation.15 | convolution fusion | flops 1074790400 | bytes 4718592 | tf_op jit(solution)/shard_map/dot_general | solution.py:109
  57.5 4.7 %all-to-all-start = ((bf16[4,128,2048]{2,1,0:T(8,128)(2,1)}), bf16[4,128,2048]{2,1,0:T(8,128)(2,1)}, u32[]{:S(2)}, u32[]{:S(2)}) async-start(bf16[4,128,2048]{2,1,0:T(8,128)(2,1)} %bitcast.44), calls=%async_computation | async-start | bytes 4194304 | tf_op jit(solution)/shard_map/all_to_all | solution.py:35
  62.2 0.0 copy-done.4
  62.2 25.7 %all-to-all-done = bf16[4,128,2048]{2,1,0:T(8,128)(2,1)} async-done(((bf16[4,128,2048]{2,1,0:T(8,128)(2,1)}), bf16[4,128,2048]{2,1,0:T(8,128)(2,1)}, u32[]{:S(2)}, u32[]{:S(2)}) %all-to-all-start) | async-done | bytes 2097184 | tf_op jit(solution)/shard_map/all_to_all | solution.py:35
  87.9 2.1 %reduce_sum.43 = bf16[128,2048]{1,0:T(8,128)(2,1)S(1)} reduce(bf16[4,128,2048]{2,1,0:T(8,128)(2,1)} %all-to-all-done, bf16[]{:T(256)} %constant.33.clone.1), dimensions={0}, to_apply=%region_2.3 | reduce | flops 786432 | bytes 2621442 | tf_op jit(solution)/shard_map/reduce_sum | solution.py:36
  90.0 0.0 copy-done.1
  90.0 0.3 fusion.28
  90.2 0.2 fusion.30
  90.5 0.2 broadcast_in_dim.16
  90.7 29.9 %all_to_all.15 = bf16[4,128,2048]{2,1,0:T(8,128)(2,1)} all-to-all(bf16[4,128,2048]{2,1,0:T(8,128)(2,1)S(1)} %broadcast_in_dim.16), channel_id=1, replica_groups=mesh['grp'=2,'sp'=32,'tp'=4] {'tp'}, dimensions={0} | all-to-all | bytes 4194304 | tf_op jit(solution)/shard_map/all_to_all | solution.py:54
  120.6 11.1 %all-gather.2.cloned.1.call-done = bf16[2048,4224]{1,0:T(8,128)(2,1)} async-done(((bf16[64,4224]{1,0:T(8,128)(2,1)}), bf16[2048,4224]{1,0:T(8,128)(2,1)}) %all-gather.2.cloned.1.call-update) | async-done | bytes 17301520 | tf_op jit(solution)/shard_map/all_gather | solution.py:42
  131.7 8.2 %fusion.8 = f32[512,1408]{1,0:T(8,128)} fusion(bf16[512,2048]{1,0:T(8,128)(2,1)} %bitcast.42, bf16[2048,4224]{1,0:T(8,128)(2,1)} %all-gather.2.cloned.1.call-done), kind=kOutput, calls=%fused_computation.11 | convolution fusion | flops 2952790016 | bytes 10747904 | tf_op jit(solution)/shard_map/dot_general | solution.py:125
  140.0 13.8 %fusion.16 = bf16[512,2048]{1,0:T(8,128)(2,1)} fusion(bf16[2048,4224]{1,0:T(8,128)(2,1)} %all-gather.2.cloned.1.call-done, bf16[512,2048]{1,0:T(8,128)(2,1)} %bitcast.43, f32[512,1408]{1,0:T(8,128)} %fusion.8), kind=kOutput, calls=%fused_computation.16 | convolution fusion | flops 5910953984 | bytes 18612224 | tf_op jit(solution)/shard_map/dot_general | solution.py:129
  153.8 30.6 %all_to_all.16 = bf16[4,128,2048]{2,1,0:T(8,128)(2,1)} all-to-all(bf16[4,128,2048]{2,1,0:T(8,128)(2,1)} %bitcast.45), channel_id=1, replica_groups=mesh['grp'=2,'sp'=32,'tp'=4] {'tp'}, dimensions={0} | all-to-all | bytes 4194304 | tf_op jit(solution)/shard_map/all_to_all | solution.py:35
  184.4 2.9 %reduce_sum.45 = bf16[128,2048]{1,0:T(8,128)(2,1)} reduce(bf16[4,128,2048]{2,1,0:T(8,128)(2,1)} %all_to_all.16, bf16[]{:T(256)} %constant.33.clone.1), dimensions={0}, to_apply=%region_4.5 | reduce | flops 786432 | bytes 2621442 | tf_op jit(solution)/shard_map/reduce_sum | solution.py:36
  187.4 2.1 %fusion.31 = bf16[128,2048]{1,0:T(8,128)(2,1)} fusion(bf16[128,2048]{1,0:T(8,128)(2,1)} %reduce_sum.45, bf16[128,2048]{1,0:T(8,128)(2,1)S(1)} %reduce_sum.43, bf16[128,2048]{1,0:T(8,128)(2,1)S(1)} %copy-done.1), kind=kLoop, calls=%fused_computation.29 | loop fusion | flops 2359296 | bytes 2097152 | tf_op jit(solution)/shard_map/convert_element_type | solution.py:138
  (10 shorter events, 0.1 us)
Async XLA Ops:
  6.5 48.3 %copy-start = (bf16[512,2048]{1,0:T(8,128)(2,1)S(1)}, bf16[512,2048]{1,0:T(8,128)(2,1)}, u32[]{:S(2)}) copy-start(bf16[512,2048]{1,0:T(8,128)(2,1)} %param.17) | copy-start | bytes 6291460
  6.6 39.9 %copy-start.2 = (bf16[512,64]{0,1:T(8,128)(2,1)S(1)}, bf16[512,64]{0,1:T(8,128)(2,1)}, u32[]{:S(2)}) copy-start(bf16[512,64]{0,1:T(8,128)(2,1)} %param.13) | copy-start | bytes 196612
  6.6 125.2 %all-gather.2.cloned.1.call-start = ((), (), s32[]{:S(2)}) async-start(), calls=%async_computation.3 | async-start | bytes 17842176 | tf_op jit(solution)/shard_map/all_gather | solution.py:42
  9.4 34.0 %collective-permute-start.2 = (bf16[128]{0:T(256)(128)(2,1)S(1)}, bf16[128]{0:T(256)(128)(2,1)S(1)}, u32[]{:S(2)}, u32[]{:S(2)}) collective-permute-start(bf16[128]{0:T(256)(128)(2,1)S(1)} %get-tuple-element.9), channel_id=1, source_target_pairs={{0,4},{4,8},{8,12},{12,16},{16,20},{20,24},{24,28},{28,32},{32,36}... | collective-permute-start | bytes 776 | tf_op jit(solution)/shard_map/ppermute | solution.py:21
  15.2 30.3 %collective-permute-start.3 = (bf16[128]{0:T(256)(128)(2,1)S(1)}, bf16[128]{0:T(256)(128)(2,1)S(1)}, u32[]{:S(2)}, u32[]{:S(2)}) collective-permute-start(bf16[128]{0:T(256)(128)(2,1)S(1)} %get-tuple-element.10), channel_id=1, source_target_pairs={{4,0},{8,4},{12,8},{16,12},{20,16},{24,20},{28,24},{32,28},{36,32}... | collective-permute-start | bytes 776 | tf_op jit(solution)/shard_map/ppermute | solution.py:22
  33.8 12.6 %collective-permute-start.4 = (bf16[128,64]{0,1:T(8,128)(2,1)S(1)}, bf16[128,64]{0,1:T(8,128)(2,1)S(1)}, u32[]{:S(2)}, u32[]{:S(2)}) collective-permute-start(bf16[128,64]{0,1:T(8,128)(2,1)S(1)} %get-tuple-element.7), channel_id=1, source_target_pairs={{0,4},{4,8},{8,12},{12,16},{16,20},{20,24},{24,28},{28,32},{32,36}... | collective-permute-start | bytes 49160 | tf_op jit(solution)/shard_map/ppermute | solution.py:21
  35.8 10.7 %collective-permute-start.5 = (bf16[128,64]{0,1:T(8,128)(2,1)S(1)}, bf16[128,64]{0,1:T(8,128)(2,1)S(1)}, u32[]{:S(2)}, u32[]{:S(2)}) collective-permute-start(bf16[128,64]{0,1:T(8,128)(2,1)S(1)} %get-tuple-element.8), channel_id=1, source_target_pairs={{4,0},{8,4},{12,8},{16,12},{20,16},{24,20},{28,24},{32,28},{36,32}... | collective-permute-start | bytes 49160 | tf_op jit(solution)/shard_map/ppermute | solution.py:22
  39.0 12.3 %collective-permute-start = (bf16[128,64]{0,1:T(8,128)(2,1)S(1)}, bf16[128,64]{0,1:T(8,128)(2,1)S(1)}, u32[]{:S(2)}, u32[]{:S(2)}) collective-permute-start(bf16[128,64]{0,1:T(8,128)(2,1)S(1)} %get-tuple-element.5), channel_id=1, source_target_pairs={{0,4},{4,8},{8,12},{12,16},{16,20},{20,24},{24,28},{28,32},{32,36}... | collective-permute-start | bytes 49160 | tf_op jit(solution)/shard_map/ppermute | solution.py:21
  43.4 7.8 %collective-permute-start.1 = (bf16[128,64]{0,1:T(8,128)(2,1)S(1)}, bf16[128,64]{0,1:T(8,128)(2,1)S(1)}, u32[]{:S(2)}, u32[]{:S(2)}) collective-permute-start(bf16[128,64]{0,1:T(8,128)(2,1)S(1)} %get-tuple-element.6), channel_id=1, source_target_pairs={{4,0},{8,4},{12,8},{16,12},{20,16},{24,20},{28,24},{32,28},{36,32}... | collective-permute-start | bytes 49160 | tf_op jit(solution)/shard_map/ppermute | solution.py:22
  46.5 2.1 %copy-start.5 = (f32[8]{0:T(128)S(1)}, f32[8]{0:T(128)}, u32[]{:S(2)}) copy-start(f32[8]{0:T(128)} %param.16) | copy-start | bytes 100
  48.6 2.7 %copy-start.3 = (bf16[512,64]{0,1:T(8,128)(2,1)S(1)}, bf16[512,64]{0,1:T(8,128)(2,1)}, u32[]{:S(2)}) copy-start(bf16[512,64]{0,1:T(8,128)(2,1)} %param.14) | copy-start | bytes 196612
  57.5 4.7 %copy-start.4 = (bf16[2048]{0:T(1024)(128)(2,1)S(1)}, bf16[2048]{0:T(1024)(128)(2,1)}, u32[]{:S(2)}) copy-start(bf16[2048]{0:T(1024)(128)(2,1)} %param.18) | copy-start | bytes 12292
  57.5 32.4 %copy-start.1 = (bf16[128,2048]{1,0:T(8,128)(2,1)S(1)}, bf16[128,2048]{1,0:T(8,128)(2,1)}, u32[]{:S(2)}) copy-start(bf16[128,2048]{1,0:T(8,128)(2,1)} %param.11) | copy-start | bytes 1572868
  57.5 30.4 %all-to-all-start = ((bf16[4,128,2048]{2,1,0:T(8,128)(2,1)}), bf16[4,128,2048]{2,1,0:T(8,128)(2,1)}, u32[]{:S(2)}, u32[]{:S(2)}) async-start(bf16[4,128,2048]{2,1,0:T(8,128)(2,1)} %bitcast.44), calls=%async_computation | async-start | bytes 4194304 | tf_op jit(solution)/shard_map/all_to_all | solution.py:35
Sparse Core Ops, SparseCore 0:
  9.2 122.4 all-gather.1
where the time goes:
time: 197 us; the launch traced here: 196 us
  blocking collectives  60.6 us (31%)
  starting transfers between devices  37.8 us (19%)
  waiting for transfers between devices  36.8 us (19%)
  matrix products  30.3 us (15%)
  other arithmetic  14.1 us (7%)
  between operations  13.7 us (7%)
  local copies, waits for them, and re-layouts  3.05 us (2%)
    all_to_all x1, blocking collectives, sent_and_summed(): lax.all_to_all(split_up(shard, dim, length), axis, 0, 0, tiled=True)  30.6 us
    all_to_all x1, blocking collectives, sent_to_all(): return lax.all_to_all(copies, axis, split_axis=0, concat_axis=0, tiled=True)  29.9 us
    all_to_all x1, waiting for transfers between devices, sent_and_summed(): lax.all_to_all(split_up(shard, dim, length), axis, 0, 0, tiled=True)  25.7 us
    ppermute x3, starting transfers between devices, padded(): after = lax.ppermute(initial, axis, down)  22.3 us
    dot_general x1, matrix products, on_device(): lax.dot_general(hidden, whole_down, (((1,), (1,)), ((), ())), preferred_e...  13.8 us
    all_gather x1, waiting for transfers between devices, in_one_piece(): out = lax.all_gather(both, axis, axis=dim, tiled=True)  11.1 us
    ppermute x3, starting transfers between devices, padded(): before = lax.ppermute(last, axis, up)  10.8 us
    dot_general x1, matrix products, on_device(): jnp.dot(row_piece, whole_gate, preferred_element_type=jnp.float32)  8.24 us
  transfers between devices with their start and end apart: 8, of which 2 were waited for; matrix products, arithmetic and copies ran while one was open for 9% of the time, Pallas kernels for 0%

commit v1 on v0

v1 whole, which is shorter than its diff:
```python
import functools

import jax
import jax.numpy as jnp
from jax import lax
from jax.experimental import pallas as pl
from jax.experimental.pallas import tpu as pltpu
from jax.sharding import PartitionSpec as P

HD = 64
WINDOW = 128
LANES = 128

epsilon = 1e-06
masked = -1e30

VMEM = pl.BlockSpec(memory_space=pltpu.VMEM)
HBM = pl.BlockSpec(memory_space=pl.ANY)
LIMIT = pltpu.CompilerParams(vmem_limit_bytes=56 * 1024 * 1024)


def split_up(shard, length):
    return shard.reshape(length, shard.shape[0] // length, *shard.shape[1:])


def pack_body(gate, up, down, out):
    ff = gate.shape[1]
    for i in range(ff // LANES):
        at = slice(i * LANES, (i + 1) * LANES)
        out[:, 2 * i * LANES : (2 * i + 1) * LANES] = gate[:, at]
        out[:, (2 * i + 1) * LANES : (2 * i + 2) * LANES] = up[:, at]
    out[:, 2 * ff :] = down[...]


def pack(gate, up, down):
    rows, ff = gate.shape
    return pl.pallas_call(
        pack_body,
        out_shape=jax.ShapeDtypeStruct((rows, 3 * ff), gate.dtype),
        in_specs=[VMEM] * 3,
        out_specs=VMEM,
        name="pack",
    )(gate, up, down)


def down_part(hidden, weight):
    return lax.dot_general(
        hidden, weight, (((1,), (1,)), ((), ())), preferred_element_type=jnp.float32
    ).astype(jnp.bfloat16)


def first_body(width, x, w, hidden, part, wide, narrow, sems, sem):
    ff = hidden.shape[1]
    steps = [(a, min(a + 512, 2 * ff)) for a in range(0, 2 * ff, 512)]
    copies = [
        pltpu.make_async_copy(w.at[:, a:b], wide.at[:, a:b], sems.at[k])
        for k, (a, b) in enumerate(steps)
    ]
    last = pltpu.make_async_copy(w.at[0:width, 2 * ff :], narrow, sem)
    for c in copies:
        c.start()
    last.start()
    for c, (a, b) in zip(copies, steps):
        c.wait()
        both = jnp.dot(x[...], wide[:, a:b], preferred_element_type=jnp.float32)
        for k in range((b - a) // (2 * LANES)):
            gate = both[:, 2 * k * LANES : (2 * k + 1) * LANES]
            up = both[:, (2 * k + 1) * LANES : (2 * k + 2) * LANES]
            at = a // 2 + k * LANES
            hidden[:, at : at + LANES] = (gate / (1.0 + jnp.exp(-gate)) * up).astype(hidden.dtype)
    last.wait()
    part[...] = down_part(hidden[...], narrow[...])


def ffn_first(x, w, width):
    rows, d = x.shape
    ff = w.shape[1] // 3
    n = -(-2 * ff // 512)
    return pl.pallas_call(
        functools.partial(first_body, width),
        out_shape=(
            jax.ShapeDtypeStruct((rows, ff), x.dtype),
            jax.ShapeDtypeStruct((rows, width), x.dtype),
        ),
        in_specs=[VMEM, HBM],
        out_specs=(VMEM, VMEM),
        scratch_shapes=[
            pltpu.VMEM((d, 2 * ff), x.dtype),
            pltpu.VMEM((width, ff), x.dtype),
            pltpu.SemaphoreType.DMA((n,)),
            pltpu.SemaphoreType.DMA,
        ],
        compiler_params=LIMIT,
        cost_estimate=pl.CostEstimate(
            flops=2 * rows * ff * (2 * d + width), bytes_accessed=4 * d * ff + 4 * rows * d, transcendentals=rows * ff
        ),
        name="ffn_first",
    )(x, w)


def next_body(start, width, hidden, w, part, narrow, sem):
    ff = hidden.shape[1]
    copy = pltpu.make_async_copy(w.at[start : start + width, 2 * ff :], narrow, sem)
    copy.start()
    copy.wait()
    part[...] = down_part(hidden[...], narrow[...])


def ffn_next(hidden, w, start, width):
    rows, ff = hidden.shape
    return pl.pallas_call(
        functools.partial(next_body, start, width),
        out_shape=jax.ShapeDtypeStruct((rows, width), hidden.dtype),
        in_specs=[VMEM, HBM],
        out_specs=VMEM,
        scratch_shapes=[pltpu.VMEM((width, ff), hidden.dtype), pltpu.SemaphoreType.DMA],
        compiler_params=LIMIT,
        cost_estimate=pl.CostEstimate(
            flops=2 * rows * ff * width, bytes_accessed=2 * (rows + width) * ff, transcendentals=0
        ),
        name="ffn_next",
    )(hidden, w)


def finish_body(*refs):
    middle, parts, out = refs[0], refs[1:-1], refs[-1]
    at = 0
    for part in parts:
        width = part.shape[2]
        total = part[0].astype(jnp.float32)
        for k in range(1, part.shape[0]):
            total = total + part[k].astype(jnp.float32)
        mixed = total.astype(jnp.bfloat16).astype(jnp.float32)
        here = slice(at, at + width)
        out[:, here] = (middle[:, here].astype(jnp.float32) + 0.5 * mixed).astype(out.dtype)
        at += width


def finish(middle, parts):
    return pl.pallas_call(
        finish_body,
        out_shape=jax.ShapeDtypeStruct(middle.shape, middle.dtype),
        in_specs=[VMEM] * (1 + len(parts)),
        out_specs=VMEM,
        name="finish",
    )(middle, *parts)


def middle_body(residual, parts, gain, middle, normed):
    total = parts[0].astype(jnp.float32)
    for k in range(1, parts.shape[0]):
        total = total + parts[k].astype(jnp.float32)
    projected = total.astype(jnp.bfloat16).astype(jnp.float32)
    mid = (residual[...].astype(jnp.float32) + projected).astype(jnp.bfloat16)
    middle[...] = mid
    wide = mid.astype(jnp.float32)
    scaled = wide * lax.rsqrt(jnp.mean(wide * wide, axis=-1, keepdims=True) + epsilon)
    out = (scaled * gain[...].astype(jnp.float32)).astype(normed.dtype)
    for k in range(normed.shape[0]):
        normed[k] = out


def middle_and_normed(residual, parts, gain):
    rows, d = residual.shape
    return pl.pallas_call(
        middle_body,
        out_shape=(
            jax.ShapeDtypeStruct((rows, d), residual.dtype),
            jax.ShapeDtypeStruct((parts.shape[0], rows, d), residual.dtype),
        ),
        in_specs=[VMEM] * 3,
        out_specs=(VMEM, VMEM),
        name="middle",
    )(residual, parts, gain.reshape(1, d))


def exchanged(blocks):
    return lax.all_to_all(blocks, "tp", 0, 0, tiled=True)


def attention(queries, key_heads, value_heads, documents, sink_logits):
    tok_rows = queries.shape[0]
    q_local = queries.shape[1] // HD
    kv_local = key_heads.shape[1] // HD
    groups = q_local // kv_local
    size = lax.axis_size("sp")
    own_docs = documents.astype(jnp.bfloat16)
    keys_values = jnp.concatenate([key_heads, value_heads], axis=1)
    width = keys_values.shape[1]

    def edge(lo):
        docs = jnp.broadcast_to(own_docs[lo : lo + WINDOW].reshape(-1, width), (16, width))
        return jnp.concatenate([keys_values[lo : lo + WINDOW], docs], axis=0)

    up = [(i, i + 1) for i in range(size - 1)]
    down = [(j, i) for i, j in up]
    before = lax.ppermute(edge(tok_rows - WINDOW), "sp", up)
    after = lax.ppermute(edge(0), "sp", down)
    spread = jnp.concatenate([before[:WINDOW], keys_values, after[:WINDOW]], axis=0)
    spread_docs = jnp.concatenate([before[WINDOW], own_docs, after[WINDOW]])
    spread_keys, spread_values = spread[:, : kv_local * HD], spread[:, kv_local * HD :]
    offset = lax.axis_index("sp") * tok_rows
    total_length = tok_rows * size
    query_pos = offset + jnp.arange(tok_rows, dtype=jnp.int32)
    key_pos = offset - WINDOW + jnp.arange(tok_rows + 2 * WINDOW, dtype=jnp.int32)
    allowed = (
        (jnp.abs(query_pos[:, None] - key_pos[None, :]) <= WINDOW)
        & (key_pos >= 0)[None, :]
        & (key_pos < total_length)[None, :]
        & (own_docs[:, None] == spread_docs[None, :])
    )
    query_block = queries.reshape(tok_rows, kv_local, groups, HD)
    key_block = spread_keys.reshape(-1, kv_local, HD)
    value_block = spread_values.reshape(-1, kv_local, HD)
    scores = jnp.einsum(
        "qkgd,jkd->kgqj", query_block, key_block, preferred_element_type=jnp.float32
    ) * HD ** (-0.5)
    scores = jnp.where(allowed[None, None], scores, masked)
    sink_table = sink_logits.reshape(kv_local, groups)[:, :, None]
    row_max = jnp.maximum(jnp.max(scores, axis=-1), sink_table)
    expo = jnp.exp(scores - row_max[..., None])
    total = jnp.sum(expo, axis=-1) + jnp.exp(sink_table - row_max)
    probs = (expo / total[..., None]).astype(jnp.bfloat16)
    mixed = jnp.einsum("kgqj,jkd->qkgd", probs, value_block, preferred_element_type=jnp.float32)
    return mixed.reshape(tok_rows, q_local * HD).astype(jnp.bfloat16)


def on_device(
    residual,
    queries,
    key_heads,
    value_heads,
    documents,
    sink_logits,
    out_weight,
    norm_gain,
    gate_weight,
    up_weight,
    down_weight,
):
    n_tp = lax.axis_size("tp")
    d = residual.shape[1]
    whole = lax.all_gather(pack(gate_weight, up_weight, down_weight), "sp", axis=0, tiled=True)
    attended = attention(queries, key_heads, value_heads, documents, sink_logits)
    partial = jnp.dot(attended, out_weight, preferred_element_type=jnp.float32)
    parts = exchanged(split_up(partial.astype(jnp.bfloat16), n_tp))
    middle, copies = middle_and_normed(residual, parts, norm_gain)
    rows = exchanged(copies).reshape(-1, d)
    width = d // 4
    hidden, part = ffn_first(rows, whole, width)
    mixes = [exchanged(split_up(part, n_tp))]
    for k in range(1, 4):
        part = ffn_next(hidden, whole, k * width, width)
        mixes.append(exchanged(split_up(part, n_tp)))
    return finish(middle, mixes)


def solution(mesh):
    return jax.shard_map(
        on_device,
        mesh=mesh,
        in_specs=(
            P(("grp", "sp", "tp"), None),
            P(("grp", "sp"), "tp"),
            P(("grp", "sp"), "tp"),
            P(("grp", "sp"), "tp"),
            P(("grp", "sp")),
            P("tp"),
            P("tp", None),
            P(),
            P("sp", "tp"),
            P("sp", "tp"),
            P("sp", "tp"),
        ),
        out_specs=P(("grp", "sp", "tp"), None),
        check_vma=False,
    )
```

time: 197 us -> 206 us (1.046); the launches traced: 196 us -> 202 us
  Pallas kernels: 0 us -> 35.9 us
  matrix products: 30.3 us -> 8.26 us
  blocking collectives: 60.6 us -> 40.4 us
  waiting for transfers between devices: 36.8 us -> 54.6 us
  other arithmetic: 14.1 us -> 4.47 us
  starting transfers between devices: 37.8 us -> 40.6 us
    pallas_call x0 -> x7, Pallas kernels: none -> 35.9 us  [the longest x1 13.7 us: ffn_first(): pl.pallas_call(functools.partial(first_body, width), out_shape=(jax.Shape...]
    dot_general x5 -> x3, matrix products: 30.3 us -> 8.26 us  [the longest x1 3.61 us: attention(): jnp.einsum('kgqj,jkd->qkgd', probs, value_block, preferred_element_type=j...]
    all_to_all x2, blocking collectives: 60.6 us -> 40.4 us  [exchanged(): return lax.all_to_all(blocks, 'tp', 0, 0, tiled=True)]
    all_to_all x1 -> x4, starting transfers between devices: 4.65 us -> 16.3 us  [exchanged(): return lax.all_to_all(blocks, 'tp', 0, 0, tiled=True)]
    all_to_all x1 -> x4, waiting for transfers between devices: 25.7 us -> 35.4 us  [exchanged(): return lax.all_to_all(blocks, 'tp', 0, 0, tiled=True)]
    ppermute x6 -> x2, starting transfers between devices: 33.1 us -> 24.3 us  [the longest x1 22.4 us: attention(): after = lax.ppermute(edge(0), 'sp', down)]
    all_gather x1, waiting for transfers between devices: 11.1 us -> 19.2 us  [on_device(): lax.all_gather(pack(gate_weight, up_weight, down_weight), 'sp', axis=0, t...]
    reduce_sum x4 -> x1, other arithmetic: 7.82 us -> 2.57 us  [attention(): total = jnp.sum(expo, axis=-1) + jnp.exp(sink_table - row_max)]
  transfers between devices with their start and end apart: 8 -> 7, of which waited for: 2 -> 5; matrix products, arithmetic and copies ran while one was open for 9% -> 8% of each run, Pallas kernels for 0% -> 9%
where the time goes in v1:
time: 206 us; the launch traced here: 202 us
  waiting for transfers between devices  54.6 us (27%)
  starting transfers between devices  40.6 us (20%)
  blocking collectives  40.4 us (20%)
  Pallas kernels  35.9 us (17%)
  between operations  13.7 us (7%)
  matrix products  8.26 us (4%)
  other arithmetic  4.47 us (2%)
  local copies, waits for them, and re-layouts  3.97 us (2%)
    all_to_all x2, blocking collectives, exchanged(): return lax.all_to_all(blocks, 'tp', 0, 0, tiled=True)  40.4 us
    all_to_all x4, waiting for transfers between devices, exchanged(): return lax.all_to_all(blocks, 'tp', 0, 0, tiled=True)  35.4 us
    ppermute x1, starting transfers between devices, attention(): after = lax.ppermute(edge(0), 'sp', down)  22.4 us
    all_gather x1, waiting for transfers between devices, on_device(): lax.all_gather(pack(gate_weight, up_weight, down_weight), 'sp', axis=0, t...  19.2 us
    all_to_all x4, starting transfers between devices, exchanged(): return lax.all_to_all(blocks, 'tp', 0, 0, tiled=True)  16.3 us
    pallas_call x1, Pallas kernels, ffn_first(): pl.pallas_call(functools.partial(first_body, width), out_shape=(jax.Shape...  13.7 us
    pallas_call x3, Pallas kernels, ffn_next(): pl.pallas_call(functools.partial(next_body, start, width), out_shape=jax....  13.6 us
  transfers between devices with their start and end apart: 7, of which 5 were waited for; matrix products, arithmetic and copies ran while one was open for 8% of the time, Pallas kernels for 9%

profile of v1, /device:TPU:33, one launch (start us, length us, event | category | flops | bytes accessed | tf_op | source)
XLA Modules:
  0.0 201.9 jit_solution(8896537287477193952)
XLA Ops:
  6.5 0.0 copy-start
  6.6 0.0 copy-start.4
  6.6 0.0 all-gather.2.cloned.1.call-start
  6.6 2.1 %pack.1 = bf16[64,4224]{1,0:T(8,128)(2,1)} custom-call(bf16[64,1408]{1,0:T(8,128)(2,1)} %gate.1, bf16[64,1408]{1,0:T(8,128)(2,1)} %up.1, bf16[64,1408]{1,0:T(8,128)(2,1)} %down.1), custom_call_target="tpu_custom_call" | custom-call | tf_op jit(solution)/shard_map/pack/pallas_call | solution.py:37
  8.7 0.1 all-gather.2.cloned.1.call-update
  8.7 0.7 convert_element_type.21
  9.4 0.8 constant_dynamic-update-slice_fusion.1
  10.3 0.8 constant_dynamic-update-slice_fusion
  11.1 0.1 broadcast_in_dim.13
  11.3 22.4 %collective-permute-start.1 = (bf16[144,128]{0,1:T(8,128)(2,1)S(1)}, bf16[144,128]{0,1:T(8,128)(2,1)S(1)}, u32[]{:S(2)}, u32[]{:S(2)}) collective-permute-start(bf16[144,128]{0,1:T(8,128)(2,1)S(1)} %pad_maximum_fusion.2), channel_id=1, source_target_pairs={{4,0},{8,4},{12,8},{16,12},{20,16},{24,20},{28,24},{32,28},{36,32}... | collective-permute-start | bytes 110600 | tf_op jit(solution)/shard_map/ppermute | solution.py:198
  33.6 0.1 broadcast_in_dim.12
  33.7 2.0 collective-permute-start
  35.7 1.3 copy.14
  37.0 0.0 collective-permute-done.1
  37.0 0.0 collective-permute-done
  37.0 0.1 slice_reduce_fusion
  37.1 0.1 slice_reduce_fusion.1
  37.3 1.0 fusion.6
  38.3 2.0 %fusion.1 = (f32[8,512]{1,0:T(8,128)S(1)}, f32[768,512,8]{1,0,2:T(8,128)S(1)}) fusion(pred[512,768]{0,1:T(8,128)(4,1)S(1)} %fusion.6, bf16[512,8,64]{0,2,1:T(8,128)(2,1)S(1)} %bitcast.48, bf16[768,128]{0,1:T(8,128)(2,1)S(1)} %pad_maximum_fusion), kind=kOutput, calls=%fused_computation.4 | convolution fusion | flops 412086272 | bytes 13615104 | tf_op jit(solution)/shard_map/qkgd,jkd->kgqj/dot_general | solution.py:215
  40.4 0.0 copy-done.4
  40.4 0.1 broadcast_maximum_fusion
  40.4 2.6 %fusion = f32[8,512]{1,0:T(8,128)S(1)} fusion(f32[768,512,8]{1,0,2:T(8,128)S(1)} %get-tuple-element.18, f32[8,512]{1,0:T(8,128)S(1)} %broadcast_maximum_fusion, pred[512,768]{0,1:T(8,128)(4,1)S(1)} %fusion.6), kind=kLoop, calls=%fused_computation.3 | loop fusion | flops 12578816 | bytes 13008896 | tf_op jit(solution)/shard_map/reduce_sum | solution.py:222
  43.0 0.1 exponential_add_fusion
  43.1 0.0 copy-start.3
  43.1 3.6 %fusion.7 = bf16[64,8,512]{2,0,1:T(8,128)(2,1)S(1)} fusion(f32[8,512]{1,0:T(8,128)S(1)} %exponential_add_fusion, f32[8,512]{1,0:T(8,128)S(1)} %broadcast_maximum_fusion, f32[768,512,8]{1,0,2:T(8,128)S(1)} %get-tuple-element.18, pred[512,768]{0,1:T(8,128)(4,1)S(1)} %fusion.6, bf16[768,128]{0,1:T(8,128)(2,1)S(1)} %pad_maximum_fusion), kind=kOutput, calls=%fused_computation.12 | convolution fusion | flops 418643968 | bytes 13631488 | tf_op jit(solution)/shard_map/kgqj,jkd->qkgd/dot_general | solution.py:224
  46.7 0.0 copy-done
  46.7 2.6 %convolution_convert_fusion = bf16[512,2048]{1,0:T(8,128)(2,1)} fusion(bf16[512,512]{0,1:T(8,128)(2,1)S(1)} %bitcast.50, bf16[512,2048]{1,0:T(8,128)(2,1)S(1)} %copy-done), kind=kOutput, calls=%fused_computation.7 | convolution fusion | flops 1074790400 | bytes 4718592 | tf_op jit(solution)/shard_map/dot_general | solution.py:245
  49.3 4.5 %all-to-all-start = ((bf16[4,128,2048]{2,1,0:T(8,128)(2,1)}), bf16[4,128,2048]{2,1,0:T(8,128)(2,1)}, u32[]{:S(2)}, u32[]{:S(2)}) async-start(bf16[4,128,2048]{2,1,0:T(8,128)(2,1)} %bitcast.47), calls=%async_computation | async-start | bytes 4194304 | tf_op jit(solution)/shard_map/all_to_all | solution.py:178
  53.9 0.0 copy-done.3
  53.9 0.6 reshape.217.gain
  54.5 25.3 %all-to-all-done.parts = bf16[4,128,2048]{2,1,0:T(8,128)(2,1)} async-done(((bf16[4,128,2048]{2,1,0:T(8,128)(2,1)}), bf16[4,128,2048]{2,1,0:T(8,128)(2,1)}, u32[]{:S(2)}, u32[]{:S(2)}) %all-to-all-start) | async-done | bytes 2097184 | tf_op jit(solution)/shard_map/all_to_all | solution.py:178
  79.8 3.6 %middle.1 = (bf16[128,2048]{1,0:T(8,128)(2,1)}, bf16[4,128,2048]{2,1,0:T(8,128)(2,1)}) custom-call(bf16[128,2048]{1,0:T(8,128)(2,1)} %residual.1, bf16[4,128,2048]{2,1,0:T(8,128)(2,1)} %all-to-all-done.parts, bf16[1,2048]{1,0:T(2,128)(2,1)} %reshape.217.gain), custom_call_target="tpu_custom_call" | custom-call | tf_op jit(solution)/shard_map/middle/pallas_call | solution.py:165
  83.4 29.2 %all_to_all.30 = bf16[4,128,2048]{2,1,0:T(8,128)(2,1)} all-to-all(bf16[4,128,2048]{2,1,0:T(8,128)(2,1)} %get-tuple-element.10), channel_id=1, replica_groups=mesh['grp'=2,'sp'=32,'tp'=4] {'tp'}, dimensions={0} | all-to-all | bytes 4194304 | tf_op jit(solution)/shard_map/all_to_all | solution.py:178
  112.6 19.2 %all-gather.2.cloned.1.call-done.w = bf16[2048,4224]{1,0:T(8,128)(2,1)} async-done(((bf16[64,4224]{1,0:T(8,128)(2,1)}), bf16[2048,4224]{1,0:T(8,128)(2,1)}) %all-gather.2.cloned.1.call-update) | async-done | bytes 17301520 | tf_op jit(solution)/shard_map/all_gather | solution.py:243
  131.8 13.7 %ffn_first.1 = (bf16[512,1408]{1,0:T(8,128)(2,1)}, bf16[512,512]{1,0:T(8,128)(2,1)}) custom-call(bf16[512,2048]{1,0:T(8,128)(2,1)} %bitcast.46, bf16[2048,4224]{1,0:T(8,128)(2,1)} %all-gather.2.cloned.1.call-done.w), custom_call_target="tpu_custom_call" | custom-call | flops 6643777536 | bytes 15728640 | tf_op jit(solution)/shard_map/ffn_first/pallas_call | solution.py:79
  145.5 3.9 %all-to-all-start.2 = ((bf16[4,128,512]{2,1,0:T(8,128)(2,1)}), bf16[4,128,512]{2,1,0:T(8,128)(2,1)S(1)}, u32[]{:S(2)}, u32[]{:S(2)}) async-start(bf16[4,128,512]{2,1,0:T(8,128)(2,1)} %bitcast.49), calls=%async_computation.2 | async-start | bytes 1048576 | tf_op jit(solution)/shard_map/all_to_all | solution.py:178
  149.5 4.6 %ffn_next.3 = bf16[512,512]{1,0:T(8,128)(2,1)} custom-call(bf16[512,1408]{1,0:T(8,128)(2,1)} %get-tuple-element.12.hidden, bf16[2048,4224]{1,0:T(8,128)(2,1)} %all-gather.2.cloned.1.call-done.w), custom_call_target="tpu_custom_call" | custom-call | flops 738197504 | bytes 2883584 | tf_op jit(solution)/shard_map/ffn_next/pallas_call | solution.py:111
  154.0 4.5 %all-to-all-done.2.refs_1_ = bf16[4,128,512]{2,1,0:T(8,128)(2,1)S(1)} async-done(((bf16[4,128,512]{2,1,0:T(8,128)(2,1)}), bf16[4,128,512]{2,1,0:T(8,128)(2,1)S(1)}, u32[]{:S(2)}, u32[]{:S(2)}) %all-to-all-start.2) | async-done | bytes 524320 | tf_op jit(solution)/shard_map/all_to_all | solution.py:178
  158.5 3.6 %all-to-all-start.3 = ((bf16[4,128,512]{2,1,0:T(8,128)(2,1)}), bf16[4,128,512]{2,1,0:T(8,128)(2,1)S(1)}, u32[]{:S(2)}, u32[]{:S(2)}) async-start(bf16[4,128,512]{2,1,0:T(8,128)(2,1)} %bitcast.44), calls=%async_computation.3 | async-start | bytes 1048576 | tf_op jit(solution)/shard_map/all_to_all | solution.py:178
  162.0 4.5 %ffn_next.4 = bf16[512,512]{1,0:T(8,128)(2,1)} custom-call(bf16[512,1408]{1,0:T(8,128)(2,1)} %get-tuple-element.12.hidden, bf16[2048,4224]{1,0:T(8,128)(2,1)} %all-gather.2.cloned.1.call-done.w), custom_call_target="tpu_custom_call" | custom-call | flops 738197504 | bytes 2883584 | tf_op jit(solution)/shard_map/ffn_next/pallas_call | solution.py:111
  166.6 3.2 %all-to-all-done.3.refs_2_ = bf16[4,128,512]{2,1,0:T(8,128)(2,1)S(1)} async-done(((bf16[4,128,512]{2,1,0:T(8,128)(2,1)}), bf16[4,128,512]{2,1,0:T(8,128)(2,1)S(1)}, u32[]{:S(2)}, u32[]{:S(2)}) %all-to-all-start.3) | async-done | bytes 524320 | tf_op jit(solution)/shard_map/all_to_all | solution.py:178
  169.8 4.2 %all-to-all-start.4 = ((bf16[4,128,512]{2,1,0:T(8,128)(2,1)}), bf16[4,128,512]{2,1,0:T(8,128)(2,1)}, u32[]{:S(2)}, u32[]{:S(2)}) async-start(bf16[4,128,512]{2,1,0:T(8,128)(2,1)} %bitcast.43), calls=%async_computation.4 | async-start | bytes 1048576 | tf_op jit(solution)/shard_map/all_to_all | solution.py:178
  174.1 4.5 %ffn_next.5 = bf16[512,512]{1,0:T(8,128)(2,1)} custom-call(bf16[512,1408]{1,0:T(8,128)(2,1)} %get-tuple-element.12.hidden, bf16[2048,4224]{1,0:T(8,128)(2,1)} %all-gather.2.cloned.1.call-done.w), custom_call_target="tpu_custom_call" | custom-call | flops 738197504 | bytes 2883584 | tf_op jit(solution)/shard_map/ffn_next/pallas_call | solution.py:111
  178.6 0.0 copy-done.1
  178.6 2.4 %all-to-all-done.4.refs_3_ = bf16[4,128,512]{2,1,0:T(8,128)(2,1)} async-done(((bf16[4,128,512]{2,1,0:T(8,128)(2,1)}), bf16[4,128,512]{2,1,0:T(8,128)(2,1)}, u32[]{:S(2)}, u32[]{:S(2)}) %all-to-all-start.4) | async-done | bytes 524320 | tf_op jit(solution)/shard_map/all_to_all | solution.py:178
  181.0 11.2 %all_to_all.31.refs_4_ = bf16[4,128,512]{2,1,0:T(8,128)(2,1)} all-to-all(bf16[4,128,512]{2,1,0:T(8,128)(2,1)} %bitcast.45), channel_id=1, replica_groups=mesh['grp'=2,'sp'=32,'tp'=4] {'tp'}, dimensions={0} | all-to-all | bytes 1048576 | tf_op jit(solution)/shard_map/all_to_all | solution.py:178
  192.2 0.0 copy-done.2
  192.2 2.9 %finish.1 = bf16[128,2048]{1,0:T(8,128)(2,1)} custom-call(bf16[128,2048]{1,0:T(8,128)(2,1)} %get-tuple-element.9.refs_0_, bf16[4,128,512]{2,1,0:T(8,128)(2,1)} %copy-done.1, bf16[4,128,512]{2,1,0:T(8,128)(2,1)} %copy-done.2, bf16[4,128,512]{2,1,0:T(8,128)(2,1)} %all-to-all-done.4.refs_3_, bf16[4,128,512]{2,1,0:T(8,128)(2,1)} %all_to_all.31.refs_4_), custom_call_target="tpu_custom_call" | custom-call | tf_op jit(solution)/shard_map/finish/pallas_call | solution.py:140
  (13 shorter events, 0.1 us)
Async XLA Ops:
  6.5 40.2 %copy-start = (bf16[512,2048]{1,0:T(8,128)(2,1)S(1)}, bf16[512,2048]{1,0:T(8,128)(2,1)}, u32[]{:S(2)}) copy-start(bf16[512,2048]{1,0:T(8,128)(2,1)} %param.17) | copy-start | bytes 6291460
  6.6 33.8 %copy-start.4 = (f32[8]{0:T(128)S(1)}, f32[8]{0:T(128)}, u32[]{:S(2)}) copy-start(f32[8]{0:T(128)} %param.16) | copy-start | bytes 100
  6.6 125.2 %all-gather.2.cloned.1.call-start = ((), (), s32[]{:S(2)}) async-start(), calls=%async_computation.6 | async-start | bytes 17842176 | tf_op jit(solution)/shard_map/all_gather | solution.py:243
  11.3 25.7 %collective-permute-start.1 = (bf16[144,128]{0,1:T(8,128)(2,1)S(1)}, bf16[144,128]{0,1:T(8,128)(2,1)S(1)}, u32[]{:S(2)}, u32[]{:S(2)}) collective-permute-start(bf16[144,128]{0,1:T(8,128)(2,1)S(1)} %pad_maximum_fusion.2), channel_id=1, source_target_pairs={{4,0},{8,4},{12,8},{16,12},{20,16},{24,20},{28,24},{32,28},{36,32}... | collective-permute-start | bytes 110600 | tf_op jit(solution)/shard_map/ppermute | solution.py:198
  33.7 3.3 %collective-permute-start = (bf16[144,128]{0,1:T(8,128)(2,1)S(1)}, bf16[144,128]{0,1:T(8,128)(2,1)S(1)}, u32[]{:S(2)}, u32[]{:S(2)}) collective-permute-start(bf16[144,128]{0,1:T(8,128)(2,1)S(1)} %pad_maximum_fusion.1), channel_id=1, source_target_pairs={{0,4},{4,8},{8,12},{12,16},{16,20},{20,24},{24,28},{28,32},{32,36}... | collective-permute-start | bytes 110600 | tf_op jit(solution)/shard_map/ppermute | solution.py:197
  43.1 10.8 %copy-start.3 = (bf16[2048]{0:T(1024)(128)(2,1)S(1)}, bf16[2048]{0:T(1024)(128)(2,1)}, u32[]{:S(2)}) copy-start(bf16[2048]{0:T(1024)(128)(2,1)} %param.18) | copy-start | bytes 12292
  49.3 30.5 %all-to-all-start = ((bf16[4,128,2048]{2,1,0:T(8,128)(2,1)}), bf16[4,128,2048]{2,1,0:T(8,128)(2,1)}, u32[]{:S(2)}, u32[]{:S(2)}) async-start(bf16[4,128,2048]{2,1,0:T(8,128)(2,1)} %bitcast.47), calls=%async_computation | async-start | bytes 4194304 | tf_op jit(solution)/shard_map/all_to_all | solution.py:178
  145.5 13.0 %all-to-all-start.2 = ((bf16[4,128,512]{2,1,0:T(8,128)(2,1)}), bf16[4,128,512]{2,1,0:T(8,128)(2,1)S(1)}, u32[]{:S(2)}, u32[]{:S(2)}) async-start(bf16[4,128,512]{2,1,0:T(8,128)(2,1)} %bitcast.49), calls=%async_computation.2 | async-start | bytes 1048576 | tf_op jit(solution)/shard_map/all_to_all | solution.py:178
  158.5 20.1 %copy-start.1 = (bf16[4,128,512]{2,1,0:T(8,128)(2,1)}, bf16[4,128,512]{2,1,0:T(8,128)(2,1)S(1)}, u32[]{:S(2)}) copy-start(bf16[4,128,512]{2,1,0:T(8,128)(2,1)S(1)} %all-to-all-done.2.refs_1_) | copy-start | bytes 1572868
  158.5 11.3 %all-to-all-start.3 = ((bf16[4,128,512]{2,1,0:T(8,128)(2,1)}), bf16[4,128,512]{2,1,0:T(8,128)(2,1)S(1)}, u32[]{:S(2)}, u32[]{:S(2)}) async-start(bf16[4,128,512]{2,1,0:T(8,128)(2,1)} %bitcast.44), calls=%async_computation.3 | async-start | bytes 1048576 | tf_op jit(solution)/shard_map/all_to_all | solution.py:178
  169.8 22.3 %copy-start.2 = (bf16[4,128,512]{2,1,0:T(8,128)(2,1)}, bf16[4,128,512]{2,1,0:T(8,128)(2,1)S(1)}, u32[]{:S(2)}) copy-start(bf16[4,128,512]{2,1,0:T(8,128)(2,1)S(1)} %all-to-all-done.3.refs_2_) | copy-start | bytes 1572868
  169.8 11.2 %all-to-all-start.4 = ((bf16[4,128,512]{2,1,0:T(8,128)(2,1)}), bf16[4,128,512]{2,1,0:T(8,128)(2,1)}, u32[]{:S(2)}, u32[]{:S(2)}) async-start(bf16[4,128,512]{2,1,0:T(8,128)(2,1)} %bitcast.43), calls=%async_computation.4 | async-start | bytes 1048576 | tf_op jit(solution)/shard_map/all_to_all | solution.py:178
Sparse Core Ops, SparseCore 0:
  9.2 122.5 all-gather.1

commit v2 on v1

--- a/solution.py
+++ b/solution.py
@@ -10,11 +10,14 @@
 HD = 64
 WINDOW = 128
 LANES = 128
+WIDE = 1536
+TALL = 256
 
 epsilon = 1e-06
 masked = -1e30
 
 VMEM = pl.BlockSpec(memory_space=pltpu.VMEM)
+SMEM = pl.BlockSpec(memory_space=pltpu.SMEM)
 HBM = pl.BlockSpec(memory_space=pl.ANY)
 LIMIT = pltpu.CompilerParams(vmem_limit_bytes=56 * 1024 * 1024)
 
@@ -23,103 +26,142 @@
     return shard.reshape(length, shard.shape[0] // length, *shard.shape[1:])
 
 
-def pack_body(gate, up, down, out):
-    ff = gate.shape[1]
-    for i in range(ff // LANES):
+def pack_body(gate, up, out):
+    for i in range(gate.shape[1] // LANES):
         at = slice(i * LANES, (i + 1) * LANES)
         out[:, 2 * i * LANES : (2 * i + 1) * LANES] = gate[:, at]
         out[:, (2 * i + 1) * LANES : (2 * i + 2) * LANES] = up[:, at]
-    out[:, 2 * ff :] = down[...]
-
-
-def pack(gate, up, down):
+
+
+def pack(gate, up):
     rows, ff = gate.shape
     return pl.pallas_call(
         pack_body,
-        out_shape=jax.ShapeDtypeStruct((rows, 3 * ff), gate.dtype),
-        in_specs=[VMEM] * 3,
+        out_shape=jax.ShapeDtypeStruct((rows, 2 * ff), gate.dtype),
+        in_specs=[VMEM] * 2,
         out_specs=VMEM,
         name="pack",
-    )(gate, up, down)
-
-
-def down_part(hidden, weight):
-    return lax.dot_general(
-        hidden, weight, (((1,), (1,)), ((), ())), preferred_element_type=jnp.float32
-    ).astype(jnp.bfloat16)
-
-
-def first_body(width, x, w, hidden, part, wide, narrow, sems, sem):
-    ff = hidden.shape[1]
-    steps = [(a, min(a + 512, 2 * ff)) for a in range(0, 2 * ff, 512)]
-    copies = [
-        pltpu.make_async_copy(w.at[:, a:b], wide.at[:, a:b], sems.at[k])
+    )(gate, up)
+
+
+def pair_body(side, own, other, out):
+    out[side[0]] = own[...]
+    out[1 - side[0]] = other[...]
+
+
+def pair(side, own, other):
+    return pl.pallas_call(
+        pair_body,
+        out_shape=jax.ShapeDtypeStruct((2, *own.shape), own.dtype),
+        in_specs=[SMEM, VMEM, VMEM],
+        out_specs=VMEM,
+        name="pair",
+    )(side, own, other)
+
+
+def ring_of_pairs(shard):
+    size = lax.axis_size("sp")
+    pairs = size // 2
+    side = lax.axis_index("sp") % 2
+    around = [(i, (i + (2 if i % 2 == 0 else -2)) % size) for i in range(size)]
+    swap = [(i, i ^ 1) for i in range(size)]
+    block = pair(side.reshape(1), shard, lax.ppermute(shard, "sp", swap))
+    kept, swapped = [block], []
+    for step in range(1, pairs // 2 + 1):
+        if 2 * step == pairs:
+            block = lax.dynamic_index_in_dim(block, side, 0, keepdims=False)
+        block = lax.ppermute(block, "sp", around)
+        kept.append(block)
+        swapped.append(lax.ppermute(block, "sp", swap))
+    return kept, swapped
+
+
+def ffn_body(n_kept, n_swapped, place, rows, w, *refs):
+    blocks = refs[: n_kept + n_swapped]
+    out, x, wide, narrow, hidden, xsem, wsems, dsems = refs[n_kept + n_swapped :]
+    d, two_ff = wide.shape
+    ff = two_ff // 2
+    tokens = x.shape[0]
+    pairs = d // narrow.shape[1] // 2
+    here, side = place[0], place[1]
+    way = 1 - 2 * side
+    copies = []
+    for k, block in enumerate(blocks):
+        step = k if k < n_kept else k - n_kept + 1
+        sign = -way if k < n_kept else way
+        at = lax.rem(here + sign * step + pairs, pairs)
+        if len(block.shape) == 3:
+            target = narrow.at[pl.ds(2 * at, 2)]
+        else:
+            target = narrow.at[2 * at + (side if k < n_kept else 1 - side)]
+        copies.append(pltpu.make_async_copy(block, target, dsems.at[k]))
+    steps = [(a, min(a + WIDE, two_ff)) for a in range(0, two_ff, WIDE)]
+    loads = [
+        pltpu.make_async_copy(w.at[:, a:b], wide.at[:, a:b], wsems.at[k])
         for k, (a, b) in enumerate(steps)
     ]
-    last = pltpu.make_async_copy(w.at[0:width, 2 * ff :], narrow, sem)
+    load_x = pltpu.make_async_copy(rows, x, xsem)
+    load_x.start()
+    for c in loads + copies:
+        c.start()
+    load_x.wait()
+    for c, (a, b) in zip(loads, steps):
+        c.wait()
+
+        @pl.loop(0, tokens // TALL)
+        def _(m, a=a, b=b):
+            here = pl.ds(m * TALL, TALL)
+            both = jnp.dot(x[here], wide[:, a:b], preferred_element_type=jnp.float32)
+            for k in range((b - a) // (2 * LANES)):
+                gate = both[:, 2 * k * LANES : (2 * k + 1) * LANES]
+                up = both[:, (2 * k + 1) * LANES : (2 * k + 2) * LANES]
+                at = a // 2 + k * LANES
+                hidden[here, at : at + LANES] = (gate / (1.0 + jnp.exp(-gate)) * up).astype(
+                    hidden.dtype
+                )
+
     for c in copies:
-        c.start()
-    last.start()
-    for c, (a, b) in zip(copies, steps):
         c.wait()
-        both = jnp.dot(x[...], wide[:, a:b], preferred_element_type=jnp.float32)
-        for k in range((b - a) // (2 * LANES)):
-            gate = both[:, 2 * k * LANES : (2 * k + 1) * LANES]
-            up = both[:, (2 * k + 1) * LANES : (2 * k + 2) * LANES]
-            at = a // 2 + k * LANES
-            hidden[:, at : at + LANES] = (gate / (1.0 + jnp.exp(-gate)) * up).astype(hidden.dtype)
-    last.wait()
-    part[...] = down_part(hidden[...], narrow[...])
-
-
-def ffn_first(x, w, width):
-    rows, d = x.shape
-    ff = w.shape[1] // 3
-    n = -(-2 * ff // 512)
-    return pl.pallas_call(
-        functools.partial(first_body, width),
-        out_shape=(
-            jax.ShapeDtypeStruct((rows, ff), x.dtype),
-            jax.ShapeDtypeStruct((rows, width), x.dtype),
-        ),
-        in_specs=[VMEM, HBM],
-        out_specs=(VMEM, VMEM),
+    half = narrow.shape[0] // 2
+    for n in range(2):
+
+        @pl.loop(0, tokens // TALL)
+        def _(m, n=n):
+            here = pl.ds(m * TALL, TALL)
+            weight = narrow[n * half : (n + 1) * half].reshape(d // 2, ff)
+            out[here, n * d // 2 : (n + 1) * d // 2] = lax.dot_general(
+                hidden[here], weight, (((1,), (1,)), ((), ())), preferred_element_type=jnp.float32
+            ).astype(out.dtype)
+
+
+def ffn(rows, w, kept, swapped):
+    tokens, d = rows.shape
+    ff = w.shape[1] // 2
+    shard = kept[0].shape[1]
+    blocks = [*kept, *swapped]
+    index = lax.axis_index("sp")
+    place = jnp.stack([index // 2, index % 2]).astype(jnp.int32)
+    n = -(-2 * ff // WIDE)
+    return pl.pallas_call(
+        functools.partial(ffn_body, len(kept), len(swapped)),
+        out_shape=jax.ShapeDtypeStruct((tokens, d), rows.dtype),
+        in_specs=[SMEM] + [HBM] * (2 + len(blocks)),
+        out_specs=VMEM,
         scratch_shapes=[
-            pltpu.VMEM((d, 2 * ff), x.dtype),
-            pltpu.VMEM((width, ff), x.dtype),
+            pltpu.VMEM((tokens, d), rows.dtype),
+            pltpu.VMEM((d, 2 * ff), rows.dtype),
+            pltpu.VMEM((d // shard, shard, ff), rows.dtype),
+            pltpu.VMEM((tokens, ff), rows.dtype),
+            pltpu.SemaphoreType.DMA,
             pltpu.SemaphoreType.DMA((n,)),
-            pltpu.SemaphoreType.DMA,
+            pltpu.SemaphoreType.DMA((len(blocks),)),
         ],
         compiler_params=LIMIT,
         cost_estimate=pl.CostEstimate(
-            flops=2 * rows * ff * (2 * d + width), bytes_accessed=4 * d * ff + 4 * rows * d, transcendentals=rows * ff
+            flops=6 * tokens * ff * d, bytes_accessed=6 * d * ff + 4 * tokens * d, transcendentals=tokens * ff
         ),
-        name="ffn_first",
-    )(x, w)
-
-
-def next_body(start, width, hidden, w, part, narrow, sem):
-    ff = hidden.shape[1]
-    copy = pltpu.make_async_copy(w.at[start : start + width, 2 * ff :], narrow, sem)
-    copy.start()
-    copy.wait()
-    part[...] = down_part(hidden[...], narrow[...])
-
-
-def ffn_next(hidden, w, start, width):
-    rows, ff = hidden.shape
-    return pl.pallas_call(
-        functools.partial(next_body, start, width),
-        out_shape=jax.ShapeDtypeStruct((rows, width), hidden.dtype),
-        in_specs=[VMEM, HBM],
-        out_specs=VMEM,
-        scratch_shapes=[pltpu.VMEM((width, ff), hidden.dtype), pltpu.SemaphoreType.DMA],
-        compiler_params=LIMIT,
-        cost_estimate=pl.CostEstimate(
-            flops=2 * rows * ff * width, bytes_accessed=2 * (rows + width) * ff, transcendentals=0
-        ),
-        name="ffn_next",
-    )(hidden, w)
+        name="ffn",
+    )(place, rows, w, *blocks)
 
 
 def finish_body(*refs):
@@ -240,19 +282,15 @@
 ):
     n_tp = lax.axis_size("tp")
     d = residual.shape[1]
-    whole = lax.all_gather(pack(gate_weight, up_weight, down_weight), "sp", axis=0, tiled=True)
+    whole = lax.all_gather(pack(gate_weight, up_weight), "sp", axis=0, tiled=True)
+    kept, swapped = ring_of_pairs(down_weight)
     attended = attention(queries, key_heads, value_heads, documents, sink_logits)
     partial = jnp.dot(attended, out_weight, preferred_element_type=jnp.float32)
     parts = exchanged(split_up(partial.astype(jnp.bfloat16), n_tp))
     middle, copies = middle_and_normed(residual, parts, norm_gain)
     rows = exchanged(copies).reshape(-1, d)
-    width = d // 4
-    hidden, part = ffn_first(rows, whole, width)
-    mixes = [exchanged(split_up(part, n_tp))]
-    for k in range(1, 4):
-        part = ffn_next(hidden, whole, k * width, width)
-        mixes.append(exchanged(split_up(part, n_tp)))
-    return finish(middle, mixes)
+    mixed = exchanged(split_up(ffn(rows, whole, kept, swapped), n_tp))
+    return finish(middle, [mixed])
 
 
 def solution(mesh):

time: 206 us -> 213 us (1.034); the launches traced: 202 us -> 213 us
  starting transfers between devices: 40.6 us -> 60.4 us
  blocking collectives: 40.4 us -> 30.7 us
  Pallas kernels: 35.9 us -> 28.2 us
  waiting for transfers between devices: 54.6 us -> 61.9 us
    ppermute x0 -> x17, waiting for transfers between devices: none -> 61.8 us  [the longest x8 61 us: ring_of_pairs(): block = lax.ppermute(block, 'sp', around)]
    all_to_all x4 -> x2, waiting for transfers between devices: 35.4 us -> 0.01 us  [exchanged(): return lax.all_to_all(blocks, 'tp', 0, 0, tiled=True)]
    ppermute x0 -> x17, starting transfers between devices: none -> 27 us  [the longest x8 17.9 us: ring_of_pairs(): block = lax.ppermute(block, 'sp', around)]
    all_gather x1, waiting for transfers between devices: 19.2 us -> 0.01 us  [on_device(): lax.all_gather(pack(gate_weight, up_weight), 'sp', axis=0, tiled=True)]
    all_to_all x2 -> x1, blocking collectives: 40.4 us -> 30.7 us  [exchanged(): return lax.all_to_all(blocks, 'tp', 0, 0, tiled=True)]
    pallas_call x5 -> x3, Pallas kernels: 29.5 us -> 21.6 us  [the longest x1 17.9 us: ffn(): pl.pallas_call(functools.partial(ffn_body, len(kept), len(swapped)), out_...]
    all_to_all x4 -> x2, starting transfers between devices: 16.3 us -> 9.1 us  [exchanged(): return lax.all_to_all(blocks, 'tp', 0, 0, tiled=True)]
  transfers between devices with their start and end apart: 7 -> 22, of which waited for: 5 -> 8; matrix products, arithmetic and copies ran while one was open for 8% -> 8% of each run, Pallas kernels for 9% -> 3%
where the time goes in v2:
time: 213 us
  waiting for transfers between devices  61.9 us (29%)
  starting transfers between devices  60.4 us (28%)
  blocking collectives  30.7 us (14%)
  Pallas kernels  28.2 us (13%)
  between operations  13.7 us (6%)
  matrix products  8.27 us (4%)
  other arithmetic  5.04 us (2%)
  local copies, waits for them, and re-layouts  4.66 us (2%)
    ppermute x8, waiting for transfers between devices, ring_of_pairs(): block = lax.ppermute(block, 'sp', around)  61 us
    all_to_all x1, blocking collectives, exchanged(): return lax.all_to_all(blocks, 'tp', 0, 0, tiled=True)  30.7 us
    ppermute x1, starting transfers between devices, attention(): after = lax.ppermute(edge(0), 'sp', down)  22.4 us
    pallas_call x1, Pallas kernels, ffn(): pl.pallas_call(functools.partial(ffn_body, len(kept), len(swapped)), out_...  17.9 us
    ppermute x8, starting transfers between devices, ring_of_pairs(): block = lax.ppermute(block, 'sp', around)  17.9 us
    all_to_all x2, starting transfers between devices, exchanged(): return lax.all_to_all(blocks, 'tp', 0, 0, tiled=True)  9.1 us
    ppermute x8, starting transfers between devices, ring_of_pairs(): swapped.append(lax.ppermute(block, 'sp', swap))  8.53 us
  transfers between devices with their start and end apart: 22, of which 8 were waited for; matrix products, arithmetic and copies ran while one was open for 8% of the time, Pallas kernels for 3%

profile of v2, /device:TPU:33, one launch (start us, length us, event | category | flops | bytes accessed | tf_op | source)
XLA Modules:
  0.0 212.9 jit_solution(14973450581648431341)
XLA Ops:
  6.6 2.0 pack.1
  8.6 0.7 convert_element_type.21
  9.3 0.8 constant_dynamic-update-slice_fusion.1
  10.1 0.8 constant_dynamic-update-slice_fusion
  11.0 0.1 broadcast_in_dim.13
  11.1 22.4 %collective-permute-start.1 = (bf16[144,128]{0,1:T(8,128)(2,1)S(1)}, bf16[144,128]{0,1:T(8,128)(2,1)S(1)}, u32[]{:S(2)}, u32[]{:S(2)}) collective-permute-start(bf16[144,128]{0,1:T(8,128)(2,1)S(1)} %pad_maximum_fusion.2), channel_id=1, source_target_pairs={{4,0},{8,4},{12,8},{16,12},{20,16},{24,20},{28,24},{32,28},{36,32}... | collective-permute-start | bytes 110600 | tf_op jit(solution)/shard_map/ppermute | solution.py:240
  33.6 2.0 collective-permute-start
  35.5 0.6 collective-permute-start.2
  36.1 1.3 copy.14
  37.5 0.1 slice_reduce_fusion
  37.6 0.1 slice_reduce_fusion.1
  37.7 1.0 fusion.6
  38.7 2.0 fusion.1
  40.9 2.6 %fusion = f32[8,512]{1,0:T(8,128)S(1)} fusion(f32[768,512,8]{1,0,2:T(8,128)S(1)} %get-tuple-element.14, f32[8,512]{1,0:T(8,128)S(1)} %broadcast_maximum_fusion, pred[512,768]{0,1:T(8,128)(4,1)S(1)} %fusion.6), kind=kLoop, calls=%fused_computation.3 | loop fusion | flops 12578816 | bytes 13008896 | tf_op jit(solution)/shard_map/reduce_sum | solution.py:264
  43.5 3.6 %fusion.7 = bf16[64,8,512]{2,0,1:T(8,128)(2,1)S(1)} fusion(f32[8,512]{1,0:T(8,128)S(1)} %exponential_add_fusion, f32[8,512]{1,0:T(8,128)S(1)} %broadcast_maximum_fusion, f32[768,512,8]{1,0,2:T(8,128)S(1)} %get-tuple-element.14, pred[512,768]{0,1:T(8,128)(4,1)S(1)} %fusion.6, bf16[768,128]{0,1:T(8,128)(2,1)S(1)} %pad_maximum_fusion), kind=kOutput, calls=%fused_computation.12 | convolution fusion | flops 418643968 | bytes 13631488 | tf_op jit(solution)/shard_map/kgqj,jkd->qkgd/dot_general | solution.py:266
  47.1 2.6 %convolution_convert_fusion = bf16[512,2048]{1,0:T(8,128)(2,1)} fusion(bf16[512,512]{0,1:T(8,128)(2,1)S(1)} %bitcast.47, bf16[512,2048]{1,0:T(8,128)(2,1)S(1)} %copy-done), kind=kOutput, calls=%fused_computation.7 | convolution fusion | flops 1074790400 | bytes 4718592 | tf_op jit(solution)/shard_map/dot_general | solution.py:288
  49.8 4.6 %all-to-all-start = ((bf16[4,128,2048]{2,1,0:T(8,128)(2,1)}), bf16[4,128,2048]{2,1,0:T(8,128)(2,1)}, u32[]{:S(2)}, u32[]{:S(2)}) async-start(bf16[4,128,2048]{2,1,0:T(8,128)(2,1)} %bitcast.44), calls=%async_computation | async-start | bytes 4194304 | tf_op jit(solution)/shard_map/all_to_all | solution.py:220
  54.4 0.7 copy-done.1
  55.0 1.8 pair.1.refs_0_
  56.8 3.1 %collective-permute-start.3 = (bf16[2,64,1408]{2,1,0:T(8,128)(2,1)}, bf16[2,64,1408]{2,1,0:T(8,128)(2,1)S(1)}, u32[]{:S(2)}, u32[]{:S(2)}) collective-permute-start(bf16[2,64,1408]{2,1,0:T(8,128)(2,1)} %pair.1.refs_0_), channel_id=1, source_target_pairs={{0,8},{4,124},{8,16},{12,4},{16,24},{20,12},{24,32},{28,20},{32,40... | collective-permute-start | bytes 1081352 | tf_op jit(solution)/shard_map/ppermute | solution.py:73
  59.9 11.3 %collective-permute-done.3.refs_1_ = bf16[2,64,1408]{2,1,0:T(8,128)(2,1)S(1)} collective-permute-done((bf16[2,64,1408]{2,1,0:T(8,128)(2,1)}, bf16[2,64,1408]{2,1,0:T(8,128)(2,1)S(1)}, u32[]{:S(2)}, u32[]{:S(2)}) %collective-permute-start.3) | collective-permute-done | bytes 360480 | tf_op jit(solution)/shard_map/ppermute | solution.py:73
  71.3 3.5 %collective-permute-start.4 = (bf16[2,64,1408]{2,1,0:T(8,128)(2,1)S(1)}, bf16[2,64,1408]{2,1,0:T(8,128)(2,1)S(1)}, u32[]{:S(2)}, u32[]{:S(2)}) collective-permute-start(bf16[2,64,1408]{2,1,0:T(8,128)(2,1)S(1)} %collective-permute-done.3.refs_1_), channel_id=1, source_target_pairs={{0,8},{4,124},{8,16},{12,4},{16,24},{20,12},{24,32},{28,20},{32,40... | collective-permute-start | bytes 1081352 | tf_op jit(solution)/shard_map/ppermute | solution.py:73
  74.7 11.7 %collective-permute-done.4.refs_2_ = bf16[2,64,1408]{2,1,0:T(8,128)(2,1)S(1)} collective-permute-done((bf16[2,64,1408]{2,1,0:T(8,128)(2,1)S(1)}, bf16[2,64,1408]{2,1,0:T(8,128)(2,1)S(1)}, u32[]{:S(2)}, u32[]{:S(2)}) %collective-permute-start.4) | collective-permute-done | bytes 360480 | tf_op jit(solution)/shard_map/ppermute | solution.py:73
  86.4 3.5 %collective-permute-start.5 = (bf16[2,64,1408]{2,1,0:T(8,128)(2,1)S(1)}, bf16[2,64,1408]{2,1,0:T(8,128)(2,1)S(1)}, u32[]{:S(2)}, u32[]{:S(2)}) collective-permute-start(bf16[2,64,1408]{2,1,0:T(8,128)(2,1)S(1)} %collective-permute-done.4.refs_2_), channel_id=1, source_target_pairs={{0,8},{4,124},{8,16},{12,4},{16,24},{20,12},{24,32},{28,20},{32,40... | collective-permute-start | bytes 1081352 | tf_op jit(solution)/shard_map/ppermute | solution.py:73
  89.9 11.6 %collective-permute-done.5.refs_3_ = bf16[2,64,1408]{2,1,0:T(8,128)(2,1)S(1)} collective-permute-done((bf16[2,64,1408]{2,1,0:T(8,128)(2,1)S(1)}, bf16[2,64,1408]{2,1,0:T(8,128)(2,1)S(1)}, u32[]{:S(2)}, u32[]{:S(2)}) %collective-permute-start.5) | collective-permute-done | bytes 360480 | tf_op jit(solution)/shard_map/ppermute | solution.py:73
  101.5 3.5 %collective-permute-start.6 = (bf16[2,64,1408]{2,1,0:T(8,128)(2,1)S(1)}, bf16[2,64,1408]{2,1,0:T(8,128)(2,1)}, u32[]{:S(2)}, u32[]{:S(2)}) collective-permute-start(bf16[2,64,1408]{2,1,0:T(8,128)(2,1)S(1)} %collective-permute-done.5.refs_3_), channel_id=1, source_target_pairs={{0,8},{4,124},{8,16},{12,4},{16,24},{20,12},{24,32},{28,20},{32,40... | collective-permute-start | bytes 1081352 | tf_op jit(solution)/shard_map/ppermute | solution.py:73
  105.0 11.0 %collective-permute-done.6.refs_4_ = bf16[2,64,1408]{2,1,0:T(8,128)(2,1)} collective-permute-done((bf16[2,64,1408]{2,1,0:T(8,128)(2,1)S(1)}, bf16[2,64,1408]{2,1,0:T(8,128)(2,1)}, u32[]{:S(2)}, u32[]{:S(2)}) %collective-permute-start.6) | collective-permute-done | bytes 360480 | tf_op jit(solution)/shard_map/ppermute | solution.py:73
  116.0 2.8 %collective-permute-start.7 = (bf16[2,64,1408]{2,1,0:T(8,128)(2,1)}, bf16[2,64,1408]{2,1,0:T(8,128)(2,1)}, u32[]{:S(2)}, u32[]{:S(2)}) collective-permute-start(bf16[2,64,1408]{2,1,0:T(8,128)(2,1)} %collective-permute-done.6.refs_4_), channel_id=1, source_target_pairs={{0,8},{4,124},{8,16},{12,4},{16,24},{20,12},{24,32},{28,20},{32,40... | collective-permute-start | bytes 1081352 | tf_op jit(solution)/shard_map/ppermute | solution.py:73
  118.8 0.6 reshape.209.gain
  119.4 3.6 %middle.1 = (bf16[128,2048]{1,0:T(8,128)(2,1)}, bf16[4,128,2048]{2,1,0:T(8,128)(2,1)}) custom-call(bf16[128,2048]{1,0:T(8,128)(2,1)} %residual.1, bf16[4,128,2048]{2,1,0:T(8,128)(2,1)} %all-to-all-done.parts, bf16[1,2048]{1,0:T(2,128)(2,1)} %reshape.209.gain), custom_call_target="tpu_custom_call" | custom-call | tf_op jit(solution)/shard_map/middle/pallas_call | solution.py:207
  123.0 4.5 %all-to-all-start.1 = ((bf16[4,128,2048]{2,1,0:T(8,128)(2,1)}), bf16[4,128,2048]{2,1,0:T(8,128)(2,1)}, u32[]{:S(2)}, u32[]{:S(2)}) async-start(bf16[4,128,2048]{2,1,0:T(8,128)(2,1)} %get-tuple-element.8), calls=%async_computation.1 | async-start | bytes 4194304 | tf_op jit(solution)/shard_map/all_to_all | solution.py:220
  127.6 0.1 collective-permute-start.8
  127.7 6.9 %collective-permute-done.8.refs_6_ = bf16[2,64,1408]{2,1,0:T(8,128)(2,1)} collective-permute-done((bf16[2,64,1408]{2,1,0:T(8,128)(2,1)}, bf16[2,64,1408]{2,1,0:T(8,128)(2,1)}, u32[]{:S(2)}, u32[]{:S(2)}) %collective-permute-start.8) | collective-permute-done | bytes 360480 | tf_op jit(solution)/shard_map/ppermute | solution.py:73
  134.6 1.2 collective-permute-start.9
  135.8 0.9 collective-permute-start.11
  136.7 0.5 collective-permute-start.13
  137.2 4.2 %collective-permute-done.9.refs_7_ = bf16[2,64,1408]{2,1,0:T(8,128)(2,1)S(1)} collective-permute-done((bf16[2,64,1408]{2,1,0:T(8,128)(2,1)}, bf16[2,64,1408]{2,1,0:T(8,128)(2,1)S(1)}, u32[]{:S(2)}, u32[]{:S(2)}) %collective-permute-start.9) | collective-permute-done | bytes 360480 | tf_op jit(solution)/shard_map/ppermute | solution.py:73
  141.5 4.1 %collective-permute-start.15 = (bf16[2,64,1408]{2,1,0:T(8,128)(2,1)}, bf16[2,64,1408]{2,1,0:T(8,128)(2,1)}, u32[]{:S(2)}, u32[]{:S(2)}) collective-permute-start(bf16[2,64,1408]{2,1,0:T(8,128)(2,1)} %collective-permute-done.7.refs_5_), channel_id=1, source_target_pairs={{0,4},{4,0},{8,12},{12,8},{16,20},{20,16},{24,28},{28,24},{32,36},... | collective-permute-start | bytes 1081352 | tf_op jit(solution)/shard_map/ppermute | solution.py:75
  145.6 0.1 collective-permute-start.16
  145.7 0.1 collective-permute-start.10
  145.9 0.5 collective-permute-start.17
  146.3 4.3 %collective-permute-done.10.refs_8_ = bf16[64,1408]{1,0:T(8,128)(2,1)} collective-permute-done((bf16[64,1408]{1,0:T(8,128)(2,1)S(1)}, bf16[64,1408]{1,0:T(8,128)(2,1)}, u32[]{:S(2)}, u32[]{:S(2)}) %collective-permute-start.10) | collective-permute-done | bytes 180256 | tf_op jit(solution)/shard_map/ppermute | solution.py:73
  150.6 2.4 %collective-permute-start.18 = (bf16[64,1408]{1,0:T(8,128)(2,1)}, bf16[64,1408]{1,0:T(8,128)(2,1)}, u32[]{:S(2)}, u32[]{:S(2)}) collective-permute-start(bf16[64,1408]{1,0:T(8,128)(2,1)} %collective-permute-done.10.refs_8_), channel_id=1, source_target_pairs={{0,4},{4,0},{8,12},{12,8},{16,20},{20,16},{24,28},{28,24},{32,36},... | collective-permute-start | bytes 540680 | tf_op jit(solution)/shard_map/ppermute | solution.py:75
  153.0 0.6 pad_add_fusion.place
  153.6 0.8 collective-permute-done.18.refs_16_
  154.4 17.9 %ffn.1 = bf16[512,2048]{1,0:T(8,128)(2,1)} custom-call(s32[2]{0:T(128)} %pad_add_fusion.place, bf16[512,2048]{1,0:T(8,128)(2,1)} %bitcast.12.rows, bf16[2048,2816]{1,0:T(8,128)(2,1)} %all-gather.2.cloned.1.call-done.w, bf16[2,64,1408]{2,1,0:T(8,128)(2,1)} %pair.1.refs_0_, bf16[2,64,1408]{2,1,0:T(8,128)(2,1)} %copy-done.5, bf16[2,64,1408]{2,1,0:T(8,128)(2,1)} %copy-done.6, ...), custom_call_target="tpu_custom_call" | custom-call | flops 8858370048 | bytes 21495808 | tf_op jit(solution)/shard_map/ffn/pallas_call | solution.py:145
  172.3 30.7 %all_to_all.15.refs_1_ = bf16[4,128,2048]{2,1,0:T(8,128)(2,1)} all-to-all(bf16[4,128,2048]{2,1,0:T(8,128)(2,1)} %bitcast.45), channel_id=1, replica_groups=mesh['grp'=2,'sp'=32,'tp'=4] {'tp'}, dimensions={0} | all-to-all | bytes 4194304 | tf_op jit(solution)/shard_map/all_to_all | solution.py:220
  203.0 3.0 %finish.1 = bf16[128,2048]{1,0:T(8,128)(2,1)} custom-call(bf16[128,2048]{1,0:T(8,128)(2,1)} %get-tuple-element.7.refs_0_, bf16[4,128,2048]{2,1,0:T(8,128)(2,1)} %all_to_all.15.refs_1_), custom_call_target="tpu_custom_call" | custom-call | tf_op jit(solution)/shard_map/finish/pallas_call | solution.py:182
  (48 shorter events, 0.5 us)
Async XLA Ops:
  6.5 40.6 %copy-start = (bf16[512,2048]{1,0:T(8,128)(2,1)S(1)}, bf16[512,2048]{1,0:T(8,128)(2,1)}, u32[]{:S(2)}) copy-start(bf16[512,2048]{1,0:T(8,128)(2,1)} %param.17) | copy-start | bytes 6291460
  6.6 34.2 %copy-start.4 = (f32[8]{0:T(128)S(1)}, f32[8]{0:T(128)}, u32[]{:S(2)}) copy-start(f32[8]{0:T(128)} %param.16) | copy-start | bytes 100
  6.6 147.9 %all-gather.2.cloned.1.call-start = ((), (), s32[]{:S(2)}) async-start(), calls=%async_computation.3 | async-start | bytes 11894784 | tf_op jit(solution)/shard_map/all_gather | solution.py:285
  11.1 26.3 %collective-permute-start.1 = (bf16[144,128]{0,1:T(8,128)(2,1)S(1)}, bf16[144,128]{0,1:T(8,128)(2,1)S(1)}, u32[]{:S(2)}, u32[]{:S(2)}) collective-permute-start(bf16[144,128]{0,1:T(8,128)(2,1)S(1)} %pad_maximum_fusion.2), channel_id=1, source_target_pairs={{4,0},{8,4},{12,8},{16,12},{20,16},{24,20},{28,24},{32,28},{36,32}... | collective-permute-start | bytes 110600 | tf_op jit(solution)/shard_map/ppermute | solution.py:240
  33.6 3.9 %collective-permute-start = (bf16[144,128]{0,1:T(8,128)(2,1)S(1)}, bf16[144,128]{0,1:T(8,128)(2,1)S(1)}, u32[]{:S(2)}, u32[]{:S(2)}) collective-permute-start(bf16[144,128]{0,1:T(8,128)(2,1)S(1)} %pad_maximum_fusion.1), channel_id=1, source_target_pairs={{0,4},{4,8},{8,12},{12,16},{16,20},{20,24},{24,28},{28,32},{32,36}... | collective-permute-start | bytes 110600 | tf_op jit(solution)/shard_map/ppermute | solution.py:239
  35.5 18.8 %collective-permute-start.2 = (bf16[64,1408]{1,0:T(8,128)(2,1)}, bf16[64,1408]{1,0:T(8,128)(2,1)S(1)}, u32[]{:S(2)}, u32[]{:S(2)}) collective-permute-start(bf16[64,1408]{1,0:T(8,128)(2,1)} %own.1), channel_id=1, source_target_pairs={{0,4},{4,0},{8,12},{12,8},{16,20},{20,16},{24,28},{28,24},{32,36},... | collective-permute-start | bytes 540680 | tf_op jit(solution)/shard_map/ppermute | solution.py:68
  43.5 75.3 %copy-start.3 = (bf16[2048]{0:T(1024)(128)(2,1)S(1)}, bf16[2048]{0:T(1024)(128)(2,1)}, u32[]{:S(2)}) copy-start(bf16[2048]{0:T(1024)(128)(2,1)} %param.18) | copy-start | bytes 12292
  49.8 69.7 %all-to-all-start = ((bf16[4,128,2048]{2,1,0:T(8,128)(2,1)}), bf16[4,128,2048]{2,1,0:T(8,128)(2,1)}, u32[]{:S(2)}, u32[]{:S(2)}) async-start(bf16[4,128,2048]{2,1,0:T(8,128)(2,1)} %bitcast.44), calls=%async_computation | async-start | bytes 4194304 | tf_op jit(solution)/shard_map/all_to_all | solution.py:220
  54.3 0.7 copy-start.1
  56.8 14.5 %collective-permute-start.3 = (bf16[2,64,1408]{2,1,0:T(8,128)(2,1)}, bf16[2,64,1408]{2,1,0:T(8,128)(2,1)S(1)}, u32[]{:S(2)}, u32[]{:S(2)}) collective-permute-start(bf16[2,64,1408]{2,1,0:T(8,128)(2,1)} %pair.1.refs_0_), channel_id=1, source_target_pairs={{0,8},{4,124},{8,16},{12,4},{16,24},{20,12},{24,32},{28,20},{32,40... | collective-permute-start | bytes 1081352 | tf_op jit(solution)/shard_map/ppermute | solution.py:73
  71.3 83.1 %copy-start.5 = (bf16[2,64,1408]{2,1,0:T(8,128)(2,1)}, bf16[2,64,1408]{2,1,0:T(8,128)(2,1)S(1)}, u32[]{:S(2)}) copy-start(bf16[2,64,1408]{2,1,0:T(8,128)(2,1)S(1)} %collective-permute-done.3.refs_1_) | copy-start | bytes 1081348
  71.3 15.1 %collective-permute-start.4 = (bf16[2,64,1408]{2,1,0:T(8,128)(2,1)S(1)}, bf16[2,64,1408]{2,1,0:T(8,128)(2,1)S(1)}, u32[]{:S(2)}, u32[]{:S(2)}) collective-permute-start(bf16[2,64,1408]{2,1,0:T(8,128)(2,1)S(1)} %collective-permute-done.3.refs_1_), channel_id=1, source_target_pairs={{0,8},{4,124},{8,16},{12,4},{16,24},{20,12},{24,32},{28,20},{32,40... | collective-permute-start | bytes 1081352 | tf_op jit(solution)/shard_map/ppermute | solution.py:73
  86.4 68.0 %copy-start.6 = (bf16[2,64,1408]{2,1,0:T(8,128)(2,1)}, bf16[2,64,1408]{2,1,0:T(8,128)(2,1)S(1)}, u32[]{:S(2)}) copy-start(bf16[2,64,1408]{2,1,0:T(8,128)(2,1)S(1)} %collective-permute-done.4.refs_2_) | copy-start | bytes 1081348
  86.4 15.1 %collective-permute-start.5 = (bf16[2,64,1408]{2,1,0:T(8,128)(2,1)S(1)}, bf16[2,64,1408]{2,1,0:T(8,128)(2,1)S(1)}, u32[]{:S(2)}, u32[]{:S(2)}) collective-permute-start(bf16[2,64,1408]{2,1,0:T(8,128)(2,1)S(1)} %collective-permute-done.4.refs_2_), channel_id=1, source_target_pairs={{0,8},{4,124},{8,16},{12,4},{16,24},{20,12},{24,32},{28,20},{32,40... | collective-permute-start | bytes 1081352 | tf_op jit(solution)/shard_map/ppermute | solution.py:73
  101.5 52.9 %copy-start.7 = (bf16[2,64,1408]{2,1,0:T(8,128)(2,1)}, bf16[2,64,1408]{2,1,0:T(8,128)(2,1)S(1)}, u32[]{:S(2)}) copy-start(bf16[2,64,1408]{2,1,0:T(8,128)(2,1)S(1)} %collective-permute-done.5.refs_3_) | copy-start | bytes 1081348
  101.5 14.5 %collective-permute-start.6 = (bf16[2,64,1408]{2,1,0:T(8,128)(2,1)S(1)}, bf16[2,64,1408]{2,1,0:T(8,128)(2,1)}, u32[]{:S(2)}, u32[]{:S(2)}) collective-permute-start(bf16[2,64,1408]{2,1,0:T(8,128)(2,1)S(1)} %collective-permute-done.5.refs_3_), channel_id=1, source_target_pairs={{0,8},{4,124},{8,16},{12,4},{16,24},{20,12},{24,32},{28,20},{32,40... | collective-permute-start | bytes 1081352 | tf_op jit(solution)/shard_map/ppermute | solution.py:73
  116.0 11.5 %collective-permute-start.7 = (bf16[2,64,1408]{2,1,0:T(8,128)(2,1)}, bf16[2,64,1408]{2,1,0:T(8,128)(2,1)}, u32[]{:S(2)}, u32[]{:S(2)}) collective-permute-start(bf16[2,64,1408]{2,1,0:T(8,128)(2,1)} %collective-permute-done.6.refs_4_), channel_id=1, source_target_pairs={{0,8},{4,124},{8,16},{12,4},{16,24},{20,12},{24,32},{28,20},{32,40... | collective-permute-start | bytes 1081352 | tf_op jit(solution)/shard_map/ppermute | solution.py:73
  123.0 31.4 %all-to-all-start.1 = ((bf16[4,128,2048]{2,1,0:T(8,128)(2,1)}), bf16[4,128,2048]{2,1,0:T(8,128)(2,1)}, u32[]{:S(2)}, u32[]{:S(2)}) async-start(bf16[4,128,2048]{2,1,0:T(8,128)(2,1)} %get-tuple-element.8), calls=%async_computation.1 | async-start | bytes 4194304 | tf_op jit(solution)/shard_map/all_to_all | solution.py:220
  127.6 7.0 %collective-permute-start.8 = (bf16[2,64,1408]{2,1,0:T(8,128)(2,1)}, bf16[2,64,1408]{2,1,0:T(8,128)(2,1)}, u32[]{:S(2)}, u32[]{:S(2)}) collective-permute-start(bf16[2,64,1408]{2,1,0:T(8,128)(2,1)} %collective-permute-done.7.refs_5_), channel_id=1, source_target_pairs={{0,8},{4,124},{8,16},{12,4},{16,24},{20,12},{24,32},{28,20},{32,40... | collective-permute-start | bytes 1081352 | tf_op jit(solution)/shard_map/ppermute | solution.py:73
  134.6 6.9 %collective-permute-start.9 = (bf16[2,64,1408]{2,1,0:T(8,128)(2,1)}, bf16[2,64,1408]{2,1,0:T(8,128)(2,1)S(1)}, u32[]{:S(2)}, u32[]{:S(2)}) collective-permute-start(bf16[2,64,1408]{2,1,0:T(8,128)(2,1)} %collective-permute-done.8.refs_6_), channel_id=1, source_target_pairs={{0,8},{4,124},{8,16},{12,4},{16,24},{20,12},{24,32},{28,20},{32,40... | collective-permute-start | bytes 1081352 | tf_op jit(solution)/shard_map/ppermute | solution.py:73
  135.8 9.8 %collective-permute-start.11 = (bf16[2,64,1408]{2,1,0:T(8,128)(2,1)S(1)}, bf16[2,64,1408]{2,1,0:T(8,128)(2,1)}, u32[]{:S(2)}, u32[]{:S(2)}) collective-permute-start(bf16[2,64,1408]{2,1,0:T(8,128)(2,1)S(1)} %collective-permute-done.3.refs_1_), channel_id=1, source_target_pairs={{0,4},{4,0},{8,12},{12,8},{16,20},{20,16},{24,28},{28,24},{32,36},... | collective-permute-start | bytes 1081352 | tf_op jit(solution)/shard_map/ppermute | solution.py:75
  136.7 9.0 %collective-permute-start.12 = (bf16[2,64,1408]{2,1,0:T(8,128)(2,1)S(1)}, bf16[2,64,1408]{2,1,0:T(8,128)(2,1)}, u32[]{:S(2)}, u32[]{:S(2)}) collective-permute-start(bf16[2,64,1408]{2,1,0:T(8,128)(2,1)S(1)} %collective-permute-done.4.refs_2_), channel_id=1, source_target_pairs={{0,4},{4,0},{8,12},{12,8},{16,20},{20,16},{24,28},{28,24},{32,36},... | collective-permute-start | bytes 1081352 | tf_op jit(solution)/shard_map/ppermute | solution.py:75
  136.7 9.2 %collective-permute-start.13 = (bf16[2,64,1408]{2,1,0:T(8,128)(2,1)S(1)}, bf16[2,64,1408]{2,1,0:T(8,128)(2,1)}, u32[]{:S(2)}, u32[]{:S(2)}) collective-permute-start(bf16[2,64,1408]{2,1,0:T(8,128)(2,1)S(1)} %collective-permute-done.5.refs_3_), channel_id=1, source_target_pairs={{0,4},{4,0},{8,12},{12,8},{16,20},{20,16},{24,28},{28,24},{32,36},... | collective-permute-start | bytes 1081352 | tf_op jit(solution)/shard_map/ppermute | solution.py:75
  137.2 16.4 %collective-permute-start.14 = (bf16[2,64,1408]{2,1,0:T(8,128)(2,1)}, bf16[2,64,1408]{2,1,0:T(8,128)(2,1)}, u32[]{:S(2)}, u32[]{:S(2)}) collective-permute-start(bf16[2,64,1408]{2,1,0:T(8,128)(2,1)} %collective-permute-done.6.refs_4_), channel_id=1, source_target_pairs={{0,4},{4,0},{8,12},{12,8},{16,20},{20,16},{24,28},{28,24},{32,36},... | collective-permute-start | bytes 1081352 | tf_op jit(solution)/shard_map/ppermute | solution.py:75
  141.4 13.0 %copy-start.2 = (bf16[2,64,1408]{2,1,0:T(8,128)(2,1)}, bf16[2,64,1408]{2,1,0:T(8,128)(2,1)S(1)}, u32[]{:S(2)}) copy-start(bf16[2,64,1408]{2,1,0:T(8,128)(2,1)S(1)} %collective-permute-done.9.refs_7_) | copy-start | bytes 1081348
  141.5 12.1 %collective-permute-start.15 = (bf16[2,64,1408]{2,1,0:T(8,128)(2,1)}, bf16[2,64,1408]{2,1,0:T(8,128)(2,1)}, u32[]{:S(2)}, u32[]{:S(2)}) collective-permute-start(bf16[2,64,1408]{2,1,0:T(8,128)(2,1)} %collective-permute-done.7.refs_5_), channel_id=1, source_target_pairs={{0,4},{4,0},{8,12},{12,8},{16,20},{20,16},{24,28},{28,24},{32,36},... | collective-permute-start | bytes 1081352 | tf_op jit(solution)/shard_map/ppermute | solution.py:75
  145.6 8.0 %collective-permute-start.16 = (bf16[2,64,1408]{2,1,0:T(8,128)(2,1)}, bf16[2,64,1408]{2,1,0:T(8,128)(2,1)}, u32[]{:S(2)}, u32[]{:S(2)}) collective-permute-start(bf16[2,64,1408]{2,1,0:T(8,128)(2,1)} %collective-permute-done.8.refs_6_), channel_id=1, source_target_pairs={{0,4},{4,0},{8,12},{12,8},{16,20},{20,16},{24,28},{28,24},{32,36},... | collective-permute-start | bytes 1081352 | tf_op jit(solution)/shard_map/ppermute | solution.py:75
  145.7 4.9 %collective-permute-start.10 = (bf16[64,1408]{1,0:T(8,128)(2,1)S(1)}, bf16[64,1408]{1,0:T(8,128)(2,1)}, u32[]{:S(2)}, u32[]{:S(2)}) collective-permute-start(bf16[64,1408]{1,0:T(8,128)(2,1)S(1)} %dynamic-slice_bitcast_fusion), channel_id=1, source_target_pairs={{0,8},{4,124},{8,16},{12,4},{16,24},{20,12},{24,32},{28,20},{32,40... | collective-permute-start | bytes 540680 | tf_op jit(solution)/shard_map/ppermute | solution.py:73
  145.9 7.7 %collective-permute-start.17 = (bf16[2,64,1408]{2,1,0:T(8,128)(2,1)S(1)}, bf16[2,64,1408]{2,1,0:T(8,128)(2,1)}, u32[]{:S(2)}, u32[]{:S(2)}) collective-permute-start(bf16[2,64,1408]{2,1,0:T(8,128)(2,1)S(1)} %collective-permute-done.9.refs_7_), channel_id=1, source_target_pairs={{0,4},{4,0},{8,12},{12,8},{16,20},{20,16},{24,28},{28,24},{32,36},... | collective-permute-start | bytes 1081352 | tf_op jit(solution)/shard_map/ppermute | solution.py:75
  150.6 3.8 %collective-permute-start.18 = (bf16[64,1408]{1,0:T(8,128)(2,1)}, bf16[64,1408]{1,0:T(8,128)(2,1)}, u32[]{:S(2)}, u32[]{:S(2)}) collective-permute-start(bf16[64,1408]{1,0:T(8,128)(2,1)} %collective-permute-done.10.refs_8_), channel_id=1, source_target_pairs={{0,4},{4,0},{8,12},{12,8},{16,20},{20,16},{24,28},{28,24},{32,36},... | collective-permute-start | bytes 540680 | tf_op jit(solution)/shard_map/ppermute | solution.py:75
Sparse Core Ops, SparseCore 0:
  9.2 110.7 all-gather.1

commit v3 on v2

--- a/solution.py
+++ b/solution.py
@@ -7,12 +7,14 @@
 from jax.experimental.pallas import tpu as pltpu
 from jax.sharding import PartitionSpec as P
 
+
 HD = 64
 WINDOW = 128
 LANES = 128
 WIDE = 1536
 TALL = 256
 
+
 epsilon = 1e-06
 masked = -1e30
 
@@ -26,22 +28,24 @@
     return shard.reshape(length, shard.shape[0] // length, *shard.shape[1:])
 
 
-def pack_body(gate, up, out):
-    for i in range(gate.shape[1] // LANES):
+def pack_body(gate, up, down, out):
+    ff = gate.shape[1]
+    for i in range(ff // LANES):
         at = slice(i * LANES, (i + 1) * LANES)
         out[:, 2 * i * LANES : (2 * i + 1) * LANES] = gate[:, at]
         out[:, (2 * i + 1) * LANES : (2 * i + 2) * LANES] = up[:, at]
-
-
-def pack(gate, up):
+    out[:, 2 * ff :] = down[...]
+
+
+def pack(gate, up, down):
     rows, ff = gate.shape
     return pl.pallas_call(
         pack_body,
-        out_shape=jax.ShapeDtypeStruct((rows, 2 * ff), gate.dtype),
-        in_specs=[VMEM] * 2,
+        out_shape=jax.ShapeDtypeStruct((rows, 3 * ff), gate.dtype),
+        in_specs=[VMEM] * 3,
         out_specs=VMEM,
         name="pack",
-    )(gate, up)
+    )(gate, up, down)
 
 
 def pair_body(side, own, other, out):
@@ -59,101 +63,95 @@
     )(side, own, other)
 
 
-def ring_of_pairs(shard):
-    size = lax.axis_size("sp")
-    pairs = size // 2
-    side = lax.axis_index("sp") % 2
-    around = [(i, (i + (2 if i % 2 == 0 else -2)) % size) for i in range(size)]
-    swap = [(i, i ^ 1) for i in range(size)]
-    block = pair(side.reshape(1), shard, lax.ppermute(shard, "sp", swap))
-    kept, swapped = [block], []
-    for step in range(1, pairs // 2 + 1):
-        if 2 * step == pairs:
-            block = lax.dynamic_index_in_dim(block, side, 0, keepdims=False)
-        block = lax.ppermute(block, "sp", around)
-        kept.append(block)
-        swapped.append(lax.ppermute(block, "sp", swap))
-    return kept, swapped
-
-
-def ffn_body(n_kept, n_swapped, place, rows, w, *refs):
+class Ring:
+    def __init__(self, shard):
+        size = lax.axis_size("sp")
+        self.pairs = size // 2
+        self.side = lax.axis_index("sp") % 2
+        self.around = [(i, (i + (2 if i % 2 == 0 else -2)) % size) for i in range(size)]
+        self.swap = [(i, i ^ 1) for i in range(size)]
+        other = lax.ppermute(shard, "sp", self.swap)
+        self.block = pair(self.side.reshape(1), shard, other)
+        self.kept, self.swapped = [self.block], []
+
+    def run(self):
+        block = self.block
+        for step in range(1, self.pairs // 2 + 1):
+            if 2 * step == self.pairs:
+                block = lax.dynamic_index_in_dim(block, self.side, 0, keepdims=False)
+            block = lax.ppermute(block, "sp", self.around)
+            self.kept.append(block)
+            self.swapped.append(lax.ppermute(block, "sp", self.swap))
+
+
+def ffn_body(n_kept, n_swapped, place, rows, *refs):
     blocks = refs[: n_kept + n_swapped]
-    out, x, wide, narrow, hidden, xsem, wsems, dsems = refs[n_kept + n_swapped :]
-    d, two_ff = wide.shape
-    ff = two_ff // 2
+    out, x, whole, hidden, xsem, sems = refs[n_kept + n_swapped :]
+    d = x.shape[1]
+    ff = hidden.shape[1]
     tokens = x.shape[0]
-    pairs = d // narrow.shape[1] // 2
+    pairs = whole.shape[0] // 2
     here, side = place[0], place[1]
     way = 1 - 2 * side
-    copies = []
+    copies = [pltpu.make_async_copy(rows, x, xsem)]
     for k, block in enumerate(blocks):
         step = k if k < n_kept else k - n_kept + 1
         sign = -way if k < n_kept else way
         at = lax.rem(here + sign * step + pairs, pairs)
         if len(block.shape) == 3:
-            target = narrow.at[pl.ds(2 * at, 2)]
+            target = whole.at[pl.ds(2 * at, 2)]
         else:
-            target = narrow.at[2 * at + (side if k < n_kept else 1 - side)]
-        copies.append(pltpu.make_async_copy(block, target, dsems.at[k]))
-    steps = [(a, min(a + WIDE, two_ff)) for a in range(0, two_ff, WIDE)]
-    loads = [
-        pltpu.make_async_copy(w.at[:, a:b], wide.at[:, a:b], wsems.at[k])
-        for k, (a, b) in enumerate(steps)
-    ]
-    load_x = pltpu.make_async_copy(rows, x, xsem)
-    load_x.start()
-    for c in loads + copies:
+            target = whole.at[2 * at + (side if k < n_kept else 1 - side)]
+        copies.append(pltpu.make_async_copy(block, target, sems.at[k]))
+    for c in copies:
         c.start()
-    load_x.wait()
-    for c, (a, b) in zip(loads, steps):
+    for c in copies:
         c.wait()
+    for a in range(0, 2 * ff, WIDE):
+        b = min(a + WIDE, 2 * ff)
 
         @pl.loop(0, tokens // TALL)
         def _(m, a=a, b=b):
-            here = pl.ds(m * TALL, TALL)
-            both = jnp.dot(x[here], wide[:, a:b], preferred_element_type=jnp.float32)
+            at = pl.ds(m * TALL, TALL)
+            weight = whole[:, :, a:b].reshape(d, b - a)
+            both = jnp.dot(x[at], weight, preferred_element_type=jnp.float32)
             for k in range((b - a) // (2 * LANES)):
                 gate = both[:, 2 * k * LANES : (2 * k + 1) * LANES]
                 up = both[:, (2 * k + 1) * LANES : (2 * k + 2) * LANES]
-                at = a // 2 + k * LANES
-                hidden[here, at : at + LANES] = (gate / (1.0 + jnp.exp(-gate)) * up).astype(
+                lane = a // 2 + k * LANES
+                hidden[at, lane : lane + LANES] = (gate / (1.0 + jnp.exp(-gate)) * up).astype(
                     hidden.dtype
                 )
 
-    for c in copies:
-        c.wait()
-    half = narrow.shape[0] // 2
+    half = whole.shape[0] // 2
     for n in range(2):
 
         @pl.loop(0, tokens // TALL)
         def _(m, n=n):
-            here = pl.ds(m * TALL, TALL)
-            weight = narrow[n * half : (n + 1) * half].reshape(d // 2, ff)
-            out[here, n * d // 2 : (n + 1) * d // 2] = lax.dot_general(
-                hidden[here], weight, (((1,), (1,)), ((), ())), preferred_element_type=jnp.float32
+            at = pl.ds(m * TALL, TALL)
+            weight = whole[n * half : (n + 1) * half, :, 2 * ff :].reshape(d // 2, ff)
+            out[at, n * d // 2 : (n + 1) * d // 2] = lax.dot_general(
+                hidden[at], weight, (((1,), (1,)), ((), ())), preferred_element_type=jnp.float32
             ).astype(out.dtype)
 
 
-def ffn(rows, w, kept, swapped):
+def ffn(rows, kept, swapped):
     tokens, d = rows.shape
-    ff = w.shape[1] // 2
-    shard = kept[0].shape[1]
+    _, shard, three_ff = kept[0].shape
+    ff = three_ff // 3
     blocks = [*kept, *swapped]
     index = lax.axis_index("sp")
     place = jnp.stack([index // 2, index % 2]).astype(jnp.int32)
-    n = -(-2 * ff // WIDE)
     return pl.pallas_call(
         functools.partial(ffn_body, len(kept), len(swapped)),
         out_shape=jax.ShapeDtypeStruct((tokens, d), rows.dtype),
-        in_specs=[SMEM] + [HBM] * (2 + len(blocks)),
+        in_specs=[SMEM] + [HBM] * (1 + len(blocks)),
         out_specs=VMEM,
         scratch_shapes=[
             pltpu.VMEM((tokens, d), rows.dtype),
-            pltpu.VMEM((d, 2 * ff), rows.dtype),
-            pltpu.VMEM((d // shard, shard, ff), rows.dtype),
+            pltpu.VMEM((d // shard, shard, 3 * ff), rows.dtype),
             pltpu.VMEM((tokens, ff), rows.dtype),
             pltpu.SemaphoreType.DMA,
-            pltpu.SemaphoreType.DMA((n,)),
             pltpu.SemaphoreType.DMA((len(blocks),)),
         ],
         compiler_params=LIMIT,
@@ -161,7 +159,7 @@
             flops=6 * tokens * ff * d, bytes_accessed=6 * d * ff + 4 * tokens * d, transcendentals=tokens * ff
         ),
         name="ffn",
-    )(place, rows, w, *blocks)
+    )(place, rows, *blocks)
 
 
 def finish_body(*refs):
@@ -282,14 +280,15 @@
 ):
     n_tp = lax.axis_size("tp")
     d = residual.shape[1]
-    whole = lax.all_gather(pack(gate_weight, up_weight), "sp", axis=0, tiled=True)
-    kept, swapped = ring_of_pairs(down_weight)
+    ring = Ring(pack(gate_weight, up_weight, down_weight))
+    queries, ring.block = lax.optimization_barrier((queries, ring.block))
+    ring.run()
     attended = attention(queries, key_heads, value_heads, documents, sink_logits)
     partial = jnp.dot(attended, out_weight, preferred_element_type=jnp.float32)
     parts = exchanged(split_up(partial.astype(jnp.bfloat16), n_tp))
     middle, copies = middle_and_normed(residual, parts, norm_gain)
     rows = exchanged(copies).reshape(-1, d)
-    mixed = exchanged(split_up(ffn(rows, whole, kept, swapped), n_tp))
+    mixed = exchanged(split_up(ffn(rows, ring.kept, ring.swapped), n_tp))
     return finish(middle, [mixed])
 
 

time: 213 us -> 226 us (1.061)
  the two profiles are of different devices: /device:TPU:33 before, /device:TPU:40 now
where the time goes in v3:
time: 226 us; the launch traced here: 225 us
  waiting for transfers between devices  133 us (59%)
  Pallas kernels  30.4 us (13%)
  blocking collectives  26.8 us (12%)
  starting transfers between devices  18.6 us (8%)
  matrix products  9.09 us (4%)
  other arithmetic  5.05 us (2%)
    ppermute x8, waiting for transfers between devices, run(): block = lax.ppermute(block, 'sp', self.around)  102 us
    all_to_all x2, waiting for transfers between devices, exchanged(): return lax.all_to_all(blocks, 'tp', 0, 0, tiled=True)  28.2 us
    all_to_all x1, blocking collectives, exchanged(): return lax.all_to_all(blocks, 'tp', 0, 0, tiled=True)  26.8 us
    pallas_call x1, Pallas kernels, ffn(): pl.pallas_call(functools.partial(ffn_body, len(kept), len(swapped)), out_...  19.4 us
    all_to_all x2, starting transfers between devices, exchanged(): return lax.all_to_all(blocks, 'tp', 0, 0, tiled=True)  9.26 us
  transfers between devices with their start and end apart: 21, of which 11 were waited for; matrix products, arithmetic and copies ran while one was open for 7% of the time, Pallas kernels for 2%

profile of v3, /device:TPU:40, one launch (start us, length us, event | category | flops | bytes accessed | tf_op | source)
XLA Modules:
  0.0 225.2 jit_solution(155044463448901453)
XLA Ops:
  0.0 2.1 pack.1.own
  2.2 2.1 collective-permute-done.2.other
  4.3 0.8 copy-done.1
  5.1 2.3 %pair.1.refs_0_ = bf16[2,64,4224]{2,1,0:T(8,128)(2,1)} custom-call(s32[1]{0:T(128)} %bitcast.2.side, bf16[64,4224]{1,0:T(8,128)(2,1)} %pack.1.own, bf16[64,4224]{1,0:T(8,128)(2,1)} %copy-done.1), custom_call_target="tpu_custom_call" | custom-call | tf_op jit(solution)/shard_map/pair/pallas_call | solution.py:57
  7.4 2.8 %collective-permute-start.3 = (bf16[2,64,4224]{2,1,0:T(8,128)(2,1)}, bf16[2,64,4224]{2,1,0:T(8,128)(2,1)S(1)}, u32[]{:S(2)}, u32[]{:S(2)}) collective-permute-start(bf16[2,64,4224]{2,1,0:T(8,128)(2,1)} %pair.1.refs_0_), channel_id=1, source_target_pairs={{0,8},{4,124},{8,16},{12,4},{16,24},{20,12},{24,32},{28,20},{32,40... | collective-permute-start | bytes 3244040 | tf_op jit(solution)/shard_map/ppermute | solution.py:82
  10.2 32.9 %collective-permute-done.3.refs_1_ = bf16[2,64,4224]{2,1,0:T(8,128)(2,1)S(1)} collective-permute-done((bf16[2,64,4224]{2,1,0:T(8,128)(2,1)}, bf16[2,64,4224]{2,1,0:T(8,128)(2,1)S(1)}, u32[]{:S(2)}, u32[]{:S(2)}) %collective-permute-start.3) | collective-permute-done | bytes 1081376 | tf_op jit(solution)/shard_map/ppermute | solution.py:82
  43.2 16.4 %collective-permute-done.4.refs_2_ = bf16[2,64,4224]{2,1,0:T(8,128)(2,1)} collective-permute-done((bf16[2,64,4224]{2,1,0:T(8,128)(2,1)S(1)}, bf16[2,64,4224]{2,1,0:T(8,128)(2,1)}, u32[]{:S(2)}, u32[]{:S(2)}) %collective-permute-start.4) | collective-permute-done | bytes 1081376 | tf_op jit(solution)/shard_map/ppermute | solution.py:82
  59.6 0.1 broadcast_in_dim.13
  59.7 1.3 collective-permute-start.1
  61.0 0.1 broadcast_in_dim.12
  61.2 3.4 %collective-permute-start = (bf16[144,128]{0,1:T(8,128)(2,1)S(1)}, bf16[144,128]{0,1:T(8,128)(2,1)S(1)}, u32[]{:S(2)}, u32[]{:S(2)}) collective-permute-start(bf16[144,128]{0,1:T(8,128)(2,1)S(1)} %pad_maximum_fusion.1), channel_id=1, source_target_pairs={{0,4},{4,8},{8,12},{12,16},{16,20},{20,24},{24,28},{28,32},{32,36}... | collective-permute-start | bytes 110600 | tf_op jit(solution)/shard_map/ppermute | solution.py:237
  64.6 0.8 collective-permute-done
  65.4 0.1 slice_reduce_fusion
  65.5 0.1 slice_reduce_fusion.1
  65.7 0.7 pad_maximum_fusion
  66.4 9.9 %collective-permute-done.5.refs_3_ = bf16[2,64,4224]{2,1,0:T(8,128)(2,1)} collective-permute-done((bf16[2,64,4224]{2,1,0:T(8,128)(2,1)}, bf16[2,64,4224]{2,1,0:T(8,128)(2,1)}, u32[]{:S(2)}, u32[]{:S(2)}) %collective-permute-start.5) | collective-permute-done | bytes 1081376 | tf_op jit(solution)/shard_map/ppermute | solution.py:82
  76.3 1.0 fusion.6
  77.3 0.2 copy.14
  77.5 0.0 copy-start.8
  77.5 2.9 %fusion.1 = (f32[8,512]{1,0:T(8,128)S(1)}, f32[768,512,8]{1,0,2:T(8,128)S(1)}) fusion(pred[512,768]{0,1:T(8,128)(4,1)S(1)} %fusion.6, bf16[512,8,64]{0,2,1:T(8,128)(2,1)S(1)} %bitcast.46, bf16[768,128]{0,1:T(8,128)(2,1)} %pad_maximum_fusion), kind=kOutput, calls=%fused_computation.4 | convolution fusion | flops 412086272 | bytes 13615104 | tf_op jit(solution)/shard_map/qkgd,jkd->kgqj/dot_general | solution.py:255
  80.5 0.1 broadcast_maximum_fusion
  80.5 12.4 %collective-permute-done.6.refs_4_ = bf16[2,64,4224]{2,1,0:T(8,128)(2,1)} collective-permute-done((bf16[2,64,4224]{2,1,0:T(8,128)(2,1)}, bf16[2,64,4224]{2,1,0:T(8,128)(2,1)}, u32[]{:S(2)}, u32[]{:S(2)}) %collective-permute-start.6) | collective-permute-done | bytes 1081376 | tf_op jit(solution)/shard_map/ppermute | solution.py:82
  93.0 2.6 %fusion = f32[8,512]{1,0:T(8,128)S(1)} fusion(f32[768,512,8]{1,0,2:T(8,128)S(1)} %get-tuple-element.18, f32[8,512]{1,0:T(8,128)S(1)} %broadcast_maximum_fusion, pred[512,768]{0,1:T(8,128)(4,1)S(1)} %fusion.6), kind=kLoop, calls=%fused_computation.3 | loop fusion | flops 12578816 | bytes 13008896 | tf_op jit(solution)/shard_map/reduce_sum | solution.py:262
  95.5 0.1 exponential_add_fusion
  95.6 14.0 %collective-permute-done.7.refs_5_ = bf16[2,64,4224]{2,1,0:T(8,128)(2,1)} collective-permute-done((bf16[2,64,4224]{2,1,0:T(8,128)(2,1)}, bf16[2,64,4224]{2,1,0:T(8,128)(2,1)}, u32[]{:S(2)}, u32[]{:S(2)}) %collective-permute-start.7) | collective-permute-done | bytes 1081376 | tf_op jit(solution)/shard_map/ppermute | solution.py:82
  109.6 0.0 collective-permute-start.8
  109.6 3.6 %fusion.7 = bf16[64,8,512]{2,0,1:T(8,128)(2,1)S(1)} fusion(f32[8,512]{1,0:T(8,128)S(1)} %exponential_add_fusion, f32[8,512]{1,0:T(8,128)S(1)} %broadcast_maximum_fusion, f32[768,512,8]{1,0,2:T(8,128)S(1)} %get-tuple-element.18, pred[512,768]{0,1:T(8,128)(4,1)S(1)} %fusion.6, bf16[768,128]{0,1:T(8,128)(2,1)S(1)} %copy-done.3), kind=kOutput, calls=%fused_computation.12 | convolution fusion | flops 418643968 | bytes 13631488 | tf_op jit(solution)/shard_map/kgqj,jkd->qkgd/dot_general | solution.py:264
  113.3 2.6 %convolution_convert_fusion = bf16[512,2048]{1,0:T(8,128)(2,1)} fusion(bf16[512,512]{0,1:T(8,128)(2,1)S(1)} %bitcast.47, bf16[512,2048]{1,0:T(8,128)(2,1)S(1)} %copy-done), kind=kOutput, calls=%fused_computation.7 | convolution fusion | flops 1074790400 | bytes 4718592 | tf_op jit(solution)/shard_map/dot_general | solution.py:287
  115.8 4.7 %all-to-all-start = ((bf16[4,128,2048]{2,1,0:T(8,128)(2,1)}), bf16[4,128,2048]{2,1,0:T(8,128)(2,1)}, u32[]{:S(2)}, u32[]{:S(2)}) async-start(bf16[4,128,2048]{2,1,0:T(8,128)(2,1)} %bitcast.44), calls=%async_computation | async-start | bytes 4194304 | tf_op jit(solution)/shard_map/all_to_all | solution.py:218
  120.5 5.8 %collective-permute-done.8.refs_6_ = bf16[2,64,4224]{2,1,0:T(8,128)(2,1)} collective-permute-done((bf16[2,64,4224]{2,1,0:T(8,128)(2,1)}, bf16[2,64,4224]{2,1,0:T(8,128)(2,1)}, u32[]{:S(2)}, u32[]{:S(2)}) %collective-permute-start.8) | collective-permute-done | bytes 1081376 | tf_op jit(solution)/shard_map/ppermute | solution.py:82
  126.3 0.5 collective-permute-start.12
  126.8 0.0 collective-permute-start.13
  126.8 0.6 reshape.212.gain
  127.4 17.2 %all-to-all-done.parts = bf16[4,128,2048]{2,1,0:T(8,128)(2,1)} async-done(((bf16[4,128,2048]{2,1,0:T(8,128)(2,1)}), bf16[4,128,2048]{2,1,0:T(8,128)(2,1)}, u32[]{:S(2)}, u32[]{:S(2)}) %all-to-all-start) | async-done | bytes 2097184 | tf_op jit(solution)/shard_map/all_to_all | solution.py:218
  144.7 3.6 %middle.1 = (bf16[128,2048]{1,0:T(8,128)(2,1)}, bf16[4,128,2048]{2,1,0:T(8,128)(2,1)}) custom-call(bf16[128,2048]{1,0:T(8,128)(2,1)} %residual.1, bf16[4,128,2048]{2,1,0:T(8,128)(2,1)} %all-to-all-done.parts, bf16[1,2048]{1,0:T(2,128)(2,1)} %reshape.212.gain), custom_call_target="tpu_custom_call" | custom-call | tf_op jit(solution)/shard_map/middle/pallas_call | solution.py:205
  148.2 4.5 %all-to-all-start.1 = ((bf16[4,128,2048]{2,1,0:T(8,128)(2,1)}), bf16[4,128,2048]{2,1,0:T(8,128)(2,1)}, u32[]{:S(2)}, u32[]{:S(2)}) async-start(bf16[4,128,2048]{2,1,0:T(8,128)(2,1)} %get-tuple-element.11), calls=%async_computation.1 | async-start | bytes 4194304 | tf_op jit(solution)/shard_map/all_to_all | solution.py:218
  152.8 0.1 collective-permute-start.14
  152.9 0.5 collective-permute-start.15
  153.5 0.3 collective-permute-start.16
  153.8 0.0 collective-permute-start.10
  153.8 0.5 collective-permute-start.17
  154.2 10.2 %collective-permute-done.10.refs_8_ = bf16[64,4224]{1,0:T(8,128)(2,1)} collective-permute-done((bf16[64,4224]{1,0:T(8,128)(2,1)S(1)}, bf16[64,4224]{1,0:T(8,128)(2,1)}, u32[]{:S(2)}, u32[]{:S(2)}) %collective-permute-start.10) | collective-permute-done | bytes 540704 | tf_op jit(solution)/shard_map/ppermute | solution.py:82
  164.4 0.0 collective-permute-start.18
  164.4 0.6 pad_add_fusion.place
  165.0 10.9 %all-to-all-done.1 = bf16[4,128,2048]{2,1,0:T(8,128)(2,1)} async-done(((bf16[4,128,2048]{2,1,0:T(8,128)(2,1)}), bf16[4,128,2048]{2,1,0:T(8,128)(2,1)}, u32[]{:S(2)}, u32[]{:S(2)}) %all-to-all-start.1) | async-done | bytes 2097184 | tf_op jit(solution)/shard_map/all_to_all | solution.py:218
  176.0 19.4 %ffn.1 = bf16[512,2048]{1,0:T(8,128)(2,1)} custom-call(s32[2]{0:T(128)} %pad_add_fusion.place, bf16[512,2048]{1,0:T(8,128)(2,1)} %bitcast.12.rows, bf16[2,64,4224]{2,1,0:T(8,128)(2,1)} %pair.1.refs_0_, bf16[2,64,4224]{2,1,0:T(8,128)(2,1)} %copy-done.10, bf16[2,64,4224]{2,1,0:T(8,128)(2,1)} %collective-permute-done.4.refs_2_, ...), custom_call_target="tpu_custom_call" | custom-call | flops 8858370048 | bytes 21495808 | tf_op jit(solution)/shard_map/ffn/pallas_call | solution.py:145
  195.4 26.8 %all_to_all.15.refs_1_ = bf16[4,128,2048]{2,1,0:T(8,128)(2,1)} all-to-all(bf16[4,128,2048]{2,1,0:T(8,128)(2,1)} %bitcast.45), channel_id=1, replica_groups=mesh['grp'=2,'sp'=32,'tp'=4] {'tp'}, dimensions={0} | all-to-all | bytes 4194304 | tf_op jit(solution)/shard_map/all_to_all | solution.py:218
  222.2 3.0 %finish.1 = bf16[128,2048]{1,0:T(8,128)(2,1)} custom-call(bf16[128,2048]{1,0:T(8,128)(2,1)} %get-tuple-element.10.refs_0_, bf16[4,128,2048]{2,1,0:T(8,128)(2,1)} %all_to_all.15.refs_1_), custom_call_target="tpu_custom_call" | custom-call | tf_op jit(solution)/shard_map/finish/pallas_call | solution.py:180
  (51 shorter events, 0.2 us)
Async XLA Ops:
  0.0 113.2 %copy-start = (bf16[512,2048]{1,0:T(8,128)(2,1)S(1)}, bf16[512,2048]{1,0:T(8,128)(2,1)}, u32[]{:S(2)}) copy-start(bf16[512,2048]{1,0:T(8,128)(2,1)} %param.17) | copy-start | bytes 6291460
  0.0 43.1 %copy-start.9 = (s32[512]{0:T(512)S(1)}, s32[512]{0:T(512)}, u32[]{:S(2)}) copy-start(s32[512]{0:T(512)} %param.15) | copy-start | bytes 6148
  0.0 43.2 %copy-start.5 = (bf16[512,64]{0,1:T(8,128)(2,1)S(1)}, bf16[512,64]{0,1:T(8,128)(2,1)}, u32[]{:S(2)}) copy-start(bf16[512,64]{0,1:T(8,128)(2,1)} %param.13) | copy-start | bytes 196612
  0.0 43.2 %copy-start.6 = (bf16[512,64]{0,1:T(8,128)(2,1)S(1)}, bf16[512,64]{0,1:T(8,128)(2,1)}, u32[]{:S(2)}) copy-start(bf16[512,64]{0,1:T(8,128)(2,1)} %param.14) | copy-start | bytes 196612
  2.2 75.1 %copy-start.2 = (bf16[512,512]{1,0:T(8,128)(2,1)S(1)}, bf16[512,512]{1,0:T(8,128)(2,1)}, u32[]{:S(2)}) copy-start(bf16[512,512]{1,0:T(8,128)(2,1)} %param.12) | copy-start | bytes 1572868
  2.2 2.1 collective-permute-start.2
  4.3 0.8 copy-start.1
  7.4 35.7 %collective-permute-start.3 = (bf16[2,64,4224]{2,1,0:T(8,128)(2,1)}, bf16[2,64,4224]{2,1,0:T(8,128)(2,1)S(1)}, u32[]{:S(2)}, u32[]{:S(2)}) collective-permute-start(bf16[2,64,4224]{2,1,0:T(8,128)(2,1)} %pair.1.refs_0_), channel_id=1, source_target_pairs={{0,8},{4,124},{8,16},{12,4},{16,24},{20,12},{24,32},{28,20},{32,40... | collective-permute-start | bytes 3244040 | tf_op jit(solution)/shard_map/ppermute | solution.py:82
  43.1 18.0 %copy-start.10 = (bf16[2,64,4224]{2,1,0:T(8,128)(2,1)}, bf16[2,64,4224]{2,1,0:T(8,128)(2,1)S(1)}, u32[]{:S(2)}) copy-start(bf16[2,64,4224]{2,1,0:T(8,128)(2,1)S(1)} %collective-permute-done.3.refs_1_) | copy-start | bytes 3244036
  43.1 16.5 %collective-permute-start.4 = (bf16[2,64,4224]{2,1,0:T(8,128)(2,1)S(1)}, bf16[2,64,4224]{2,1,0:T(8,128)(2,1)}, u32[]{:S(2)}, u32[]{:S(2)}) collective-permute-start(bf16[2,64,4224]{2,1,0:T(8,128)(2,1)S(1)} %collective-permute-done.3.refs_1_), channel_id=1, source_target_pairs={{0,8},{4,124},{8,16},{12,4},{16,24},{20,12},{24,32},{28,20},{32,40... | collective-permute-start | bytes 3244040 | tf_op jit(solution)/shard_map/ppermute | solution.py:82
  59.6 16.7 %collective-permute-start.5 = (bf16[2,64,4224]{2,1,0:T(8,128)(2,1)}, bf16[2,64,4224]{2,1,0:T(8,128)(2,1)}, u32[]{:S(2)}, u32[]{:S(2)}) collective-permute-start(bf16[2,64,4224]{2,1,0:T(8,128)(2,1)} %collective-permute-done.4.refs_2_), channel_id=1, source_target_pairs={{0,8},{4,124},{8,16},{12,4},{16,24},{20,12},{24,32},{28,20},{32,40... | collective-permute-start | bytes 3244040 | tf_op jit(solution)/shard_map/ppermute | solution.py:82
  59.7 4.9 %collective-permute-start.1 = (bf16[144,128]{0,1:T(8,128)(2,1)S(1)}, bf16[144,128]{0,1:T(8,128)(2,1)S(1)}, u32[]{:S(2)}, u32[]{:S(2)}) collective-permute-start(bf16[144,128]{0,1:T(8,128)(2,1)S(1)} %pad_maximum_fusion.2), channel_id=1, source_target_pairs={{4,0},{8,4},{12,8},{16,12},{20,16},{24,20},{28,24},{32,28},{36,32}... | collective-permute-start | bytes 110600 | tf_op jit(solution)/shard_map/ppermute | solution.py:238
  61.2 4.3 %collective-permute-start = (bf16[144,128]{0,1:T(8,128)(2,1)S(1)}, bf16[144,128]{0,1:T(8,128)(2,1)S(1)}, u32[]{:S(2)}, u32[]{:S(2)}) collective-permute-start(bf16[144,128]{0,1:T(8,128)(2,1)S(1)} %pad_maximum_fusion.1), channel_id=1, source_target_pairs={{0,4},{4,8},{8,12},{12,16},{16,20},{20,24},{24,28},{28,32},{32,36}... | collective-permute-start | bytes 110600 | tf_op jit(solution)/shard_map/ppermute | solution.py:237
  76.3 16.7 %collective-permute-start.6 = (bf16[2,64,4224]{2,1,0:T(8,128)(2,1)}, bf16[2,64,4224]{2,1,0:T(8,128)(2,1)}, u32[]{:S(2)}, u32[]{:S(2)}) collective-permute-start(bf16[2,64,4224]{2,1,0:T(8,128)(2,1)} %collective-permute-done.5.refs_3_), channel_id=1, source_target_pairs={{0,8},{4,124},{8,16},{12,4},{16,24},{20,12},{24,32},{28,20},{32,40... | collective-permute-start | bytes 3244040 | tf_op jit(solution)/shard_map/ppermute | solution.py:82
  77.5 2.9 %copy-start.8 = (f32[8]{0:T(128)S(1)}, f32[8]{0:T(128)}, u32[]{:S(2)}) copy-start(f32[8]{0:T(128)} %param.16) | copy-start | bytes 100
  93.0 16.7 %collective-permute-start.7 = (bf16[2,64,4224]{2,1,0:T(8,128)(2,1)}, bf16[2,64,4224]{2,1,0:T(8,128)(2,1)}, u32[]{:S(2)}, u32[]{:S(2)}) collective-permute-start(bf16[2,64,4224]{2,1,0:T(8,128)(2,1)} %collective-permute-done.6.refs_4_), channel_id=1, source_target_pairs={{0,8},{4,124},{8,16},{12,4},{16,24},{20,12},{24,32},{28,20},{32,40... | collective-permute-start | bytes 3244040 | tf_op jit(solution)/shard_map/ppermute | solution.py:82
  93.0 16.7 %copy-start.3 = (bf16[768,128]{0,1:T(8,128)(2,1)S(1)}, bf16[768,128]{0,1:T(8,128)(2,1)}, u32[]{:S(2)}) copy-start(bf16[768,128]{0,1:T(8,128)(2,1)} %pad_maximum_fusion) | copy-start | bytes 589828
  109.6 16.7 %collective-permute-start.8 = (bf16[2,64,4224]{2,1,0:T(8,128)(2,1)}, bf16[2,64,4224]{2,1,0:T(8,128)(2,1)}, u32[]{:S(2)}, u32[]{:S(2)}) collective-permute-start(bf16[2,64,4224]{2,1,0:T(8,128)(2,1)} %collective-permute-done.7.refs_5_), channel_id=1, source_target_pairs={{0,8},{4,124},{8,16},{12,4},{16,24},{20,12},{24,32},{28,20},{32,40... | collective-permute-start | bytes 3244040 | tf_op jit(solution)/shard_map/ppermute | solution.py:82
  115.8 11.0 %copy-start.7 = (bf16[2048]{0:T(1024)(128)(2,1)S(1)}, bf16[2048]{0:T(1024)(128)(2,1)}, u32[]{:S(2)}) copy-start(bf16[2048]{0:T(1024)(128)(2,1)} %param.18) | copy-start | bytes 12292
  115.8 28.8 %all-to-all-start = ((bf16[4,128,2048]{2,1,0:T(8,128)(2,1)}), bf16[4,128,2048]{2,1,0:T(8,128)(2,1)}, u32[]{:S(2)}, u32[]{:S(2)}) async-start(bf16[4,128,2048]{2,1,0:T(8,128)(2,1)} %bitcast.44), calls=%async_computation | async-start | bytes 4194304 | tf_op jit(solution)/shard_map/all_to_all | solution.py:218
  126.3 26.6 %collective-permute-start.9 = (bf16[2,64,4224]{2,1,0:T(8,128)(2,1)}, bf16[2,64,4224]{2,1,0:T(8,128)(2,1)S(1)}, u32[]{:S(2)}, u32[]{:S(2)}) collective-permute-start(bf16[2,64,4224]{2,1,0:T(8,128)(2,1)} %collective-permute-done.8.refs_6_), channel_id=1, source_target_pairs={{0,8},{4,124},{8,16},{12,4},{16,24},{20,12},{24,32},{28,20},{32,40... | collective-permute-start | bytes 3244040 | tf_op jit(solution)/shard_map/ppermute | solution.py:82
  126.3 27.1 %collective-permute-start.11 = (bf16[2,64,4224]{2,1,0:T(8,128)(2,1)}, bf16[2,64,4224]{2,1,0:T(8,128)(2,1)}, u32[]{:S(2)}, u32[]{:S(2)}) collective-permute-start(bf16[2,64,4224]{2,1,0:T(8,128)(2,1)} %copy-done.10), channel_id=1, source_target_pairs={{0,4},{4,0},{8,12},{12,8},{16,20},{20,16},{24,28},{28,24},{32,36},... | collective-permute-start | bytes 3244040 | tf_op jit(solution)/shard_map/ppermute | solution.py:84
  126.3 27.4 %collective-permute-start.12 = (bf16[2,64,4224]{2,1,0:T(8,128)(2,1)}, bf16[2,64,4224]{2,1,0:T(8,128)(2,1)}, u32[]{:S(2)}, u32[]{:S(2)}) collective-permute-start(bf16[2,64,4224]{2,1,0:T(8,128)(2,1)} %collective-permute-done.4.refs_2_), channel_id=1, source_target_pairs={{0,4},{4,0},{8,12},{12,8},{16,20},{20,16},{24,28},{28,24},{32,36},... | collective-permute-start | bytes 3244040 | tf_op jit(solution)/shard_map/ppermute | solution.py:84
  126.8 26.9 %collective-permute-start.13 = (bf16[2,64,4224]{2,1,0:T(8,128)(2,1)}, bf16[2,64,4224]{2,1,0:T(8,128)(2,1)}, u32[]{:S(2)}, u32[]{:S(2)}) collective-permute-start(bf16[2,64,4224]{2,1,0:T(8,128)(2,1)} %collective-permute-done.5.refs_3_), channel_id=1, source_target_pairs={{0,4},{4,0},{8,12},{12,8},{16,20},{20,16},{24,28},{28,24},{32,36},... | collective-permute-start | bytes 3244040 | tf_op jit(solution)/shard_map/ppermute | solution.py:84
  148.2 27.7 %all-to-all-start.1 = ((bf16[4,128,2048]{2,1,0:T(8,128)(2,1)}), bf16[4,128,2048]{2,1,0:T(8,128)(2,1)}, u32[]{:S(2)}, u32[]{:S(2)}) async-start(bf16[4,128,2048]{2,1,0:T(8,128)(2,1)} %get-tuple-element.11), calls=%async_computation.1 | async-start | bytes 4194304 | tf_op jit(solution)/shard_map/all_to_all | solution.py:218
  152.8 23.2 %collective-permute-start.14 = (bf16[2,64,4224]{2,1,0:T(8,128)(2,1)}, bf16[2,64,4224]{2,1,0:T(8,128)(2,1)}, u32[]{:S(2)}, u32[]{:S(2)}) collective-permute-start(bf16[2,64,4224]{2,1,0:T(8,128)(2,1)} %collective-permute-done.6.refs_4_), channel_id=1, source_target_pairs={{0,4},{4,0},{8,12},{12,8},{16,20},{20,16},{24,28},{28,24},{32,36},... | collective-permute-start | bytes 3244040 | tf_op jit(solution)/shard_map/ppermute | solution.py:84
  152.9 23.0 %copy-start.4 = (bf16[2,64,4224]{2,1,0:T(8,128)(2,1)}, bf16[2,64,4224]{2,1,0:T(8,128)(2,1)S(1)}, u32[]{:S(2)}) copy-start(bf16[2,64,4224]{2,1,0:T(8,128)(2,1)S(1)} %collective-permute-done.9.refs_7_) | copy-start | bytes 3244036
  152.9 23.0 %collective-permute-start.15 = (bf16[2,64,4224]{2,1,0:T(8,128)(2,1)}, bf16[2,64,4224]{2,1,0:T(8,128)(2,1)}, u32[]{:S(2)}, u32[]{:S(2)}) collective-permute-start(bf16[2,64,4224]{2,1,0:T(8,128)(2,1)} %collective-permute-done.7.refs_5_), channel_id=1, source_target_pairs={{0,4},{4,0},{8,12},{12,8},{16,20},{20,16},{24,28},{28,24},{32,36},... | collective-permute-start | bytes 3244040 | tf_op jit(solution)/shard_map/ppermute | solution.py:84
  153.5 22.5 %collective-permute-start.16 = (bf16[2,64,4224]{2,1,0:T(8,128)(2,1)}, bf16[2,64,4224]{2,1,0:T(8,128)(2,1)}, u32[]{:S(2)}, u32[]{:S(2)}) collective-permute-start(bf16[2,64,4224]{2,1,0:T(8,128)(2,1)} %collective-permute-done.8.refs_6_), channel_id=1, source_target_pairs={{0,4},{4,0},{8,12},{12,8},{16,20},{20,16},{24,28},{28,24},{32,36},... | collective-permute-start | bytes 3244040 | tf_op jit(solution)/shard_map/ppermute | solution.py:84
  153.8 10.7 %collective-permute-start.10 = (bf16[64,4224]{1,0:T(8,128)(2,1)S(1)}, bf16[64,4224]{1,0:T(8,128)(2,1)}, u32[]{:S(2)}, u32[]{:S(2)}) collective-permute-start(bf16[64,4224]{1,0:T(8,128)(2,1)S(1)} %dynamic-slice_bitcast_fusion), channel_id=1, source_target_pairs={{0,8},{4,124},{8,16},{12,4},{16,24},{20,12},{24,32},{28,20},{32,40... | collective-permute-start | bytes 1622024 | tf_op jit(solution)/shard_map/ppermute | solution.py:82
  153.8 22.2 %collective-permute-start.17 = (bf16[2,64,4224]{2,1,0:T(8,128)(2,1)S(1)}, bf16[2,64,4224]{2,1,0:T(8,128)(2,1)}, u32[]{:S(2)}, u32[]{:S(2)}) collective-permute-start(bf16[2,64,4224]{2,1,0:T(8,128)(2,1)S(1)} %collective-permute-done.9.refs_7_), channel_id=1, source_target_pairs={{0,4},{4,0},{8,12},{12,8},{16,20},{20,16},{24,28},{28,24},{32,36},... | collective-permute-start | bytes 3244040 | tf_op jit(solution)/shard_map/ppermute | solution.py:84
  164.4 11.5 %collective-permute-start.18 = (bf16[64,4224]{1,0:T(8,128)(2,1)}, bf16[64,4224]{1,0:T(8,128)(2,1)}, u32[]{:S(2)}, u32[]{:S(2)}) collective-permute-start(bf16[64,4224]{1,0:T(8,128)(2,1)} %collective-permute-done.10.refs_8_), channel_id=1, source_target_pairs={{0,4},{4,0},{8,12},{12,8},{16,20},{20,16},{24,28},{28,24},{32,36},... | collective-permute-start | bytes 1622024 | tf_op jit(solution)/shard_map/ppermute | solution.py:84

commit v4 on v3

--- a/solution.py
+++ b/solution.py
@@ -7,19 +7,17 @@
 from jax.experimental.pallas import tpu as pltpu
 from jax.sharding import PartitionSpec as P
 
-
 HD = 64
 WINDOW = 128
 LANES = 128
-WIDE = 1536
 TALL = 256
-
+ROW_STEPS = 4
+TILES = ((0, 512), (512, 1536), (1536, 2816))
 
 epsilon = 1e-06
 masked = -1e30
 
 VMEM = pl.BlockSpec(memory_space=pltpu.VMEM)
-SMEM = pl.BlockSpec(memory_space=pltpu.SMEM)
 HBM = pl.BlockSpec(memory_space=pl.ANY)
 LIMIT = pltpu.CompilerParams(vmem_limit_bytes=56 * 1024 * 1024)
 
@@ -48,73 +46,34 @@
     )(gate, up, down)
 
 
-def pair_body(side, own, other, out):
-    out[side[0]] = own[...]
-    out[1 - side[0]] = other[...]
-
-
-def pair(side, own, other):
-    return pl.pallas_call(
-        pair_body,
-        out_shape=jax.ShapeDtypeStruct((2, *own.shape), own.dtype),
-        in_specs=[SMEM, VMEM, VMEM],
-        out_specs=VMEM,
-        name="pair",
-    )(side, own, other)
-
-
-class Ring:
-    def __init__(self, shard):
-        size = lax.axis_size("sp")
-        self.pairs = size // 2
-        self.side = lax.axis_index("sp") % 2
-        self.around = [(i, (i + (2 if i % 2 == 0 else -2)) % size) for i in range(size)]
-        self.swap = [(i, i ^ 1) for i in range(size)]
-        other = lax.ppermute(shard, "sp", self.swap)
-        self.block = pair(self.side.reshape(1), shard, other)
-        self.kept, self.swapped = [self.block], []
-
-    def run(self):
-        block = self.block
-        for step in range(1, self.pairs // 2 + 1):
-            if 2 * step == self.pairs:
-                block = lax.dynamic_index_in_dim(block, self.side, 0, keepdims=False)
-            block = lax.ppermute(block, "sp", self.around)
-            self.kept.append(block)
-            self.swapped.append(lax.ppermute(block, "sp", self.swap))
-
-
-def ffn_body(n_kept, n_swapped, place, rows, *refs):
-    blocks = refs[: n_kept + n_swapped]
-    out, x, whole, hidden, xsem, sems = refs[n_kept + n_swapped :]
-    d = x.shape[1]
+def ffn_body(rows, w, out, x, wide, narrow, hidden, xsem, sems, dsems):
+    tokens, d = x.shape
     ff = hidden.shape[1]
-    tokens = x.shape[0]
-    pairs = whole.shape[0] // 2
-    here, side = place[0], place[1]
-    way = 1 - 2 * side
-    copies = [pltpu.make_async_copy(rows, x, xsem)]
-    for k, block in enumerate(blocks):
-        step = k if k < n_kept else k - n_kept + 1
-        sign = -way if k < n_kept else way
-        at = lax.rem(here + sign * step + pairs, pairs)
-        if len(block.shape) == 3:
-            target = whole.at[pl.ds(2 * at, 2)]
-        else:
-            target = whole.at[2 * at + (side if k < n_kept else 1 - side)]
-        copies.append(pltpu.make_async_copy(block, target, sems.at[k]))
-    for c in copies:
+    loads = [
+        pltpu.make_async_copy(w.at[:, a:b], wide.at[:, a:b], sems.at[k])
+        for k, (a, b) in enumerate(TILES)
+    ]
+    half = d // 2
+    later = [
+        pltpu.make_async_copy(
+            w.at[n * half : (n + 1) * half, 2 * ff :],
+            narrow.at[n * half : (n + 1) * half],
+            dsems.at[n],
+        )
+        for n in range(2)
+    ]
+    load_x = pltpu.make_async_copy(rows, x, xsem)
+    load_x.start()
+    for c in loads + later:
         c.start()
-    for c in copies:
+    load_x.wait()
+    for c, (a, b) in zip(loads, TILES):
         c.wait()
-    for a in range(0, 2 * ff, WIDE):
-        b = min(a + WIDE, 2 * ff)
 
         @pl.loop(0, tokens // TALL)
         def _(m, a=a, b=b):
             at = pl.ds(m * TALL, TALL)
-            weight = whole[:, :, a:b].reshape(d, b - a)
-            both = jnp.dot(x[at], weight, preferred_element_type=jnp.float32)
+            both = jnp.dot(x[at], wide[:, a:b], preferred_element_type=jnp.float32)
             for k in range((b - a) // (2 * LANES)):
                 gate = both[:, 2 * k * LANES : (2 * k + 1) * LANES]
                 up = both[:, (2 * k + 1) * LANES : (2 * k + 2) * LANES]
@@ -123,67 +82,67 @@
                     hidden.dtype
                 )
 
-    half = whole.shape[0] // 2
-    for n in range(2):
+    for n, c in enumerate(later):
+        c.wait()
 
         @pl.loop(0, tokens // TALL)
         def _(m, n=n):
             at = pl.ds(m * TALL, TALL)
-            weight = whole[n * half : (n + 1) * half, :, 2 * ff :].reshape(d // 2, ff)
-            out[at, n * d // 2 : (n + 1) * d // 2] = lax.dot_general(
-                hidden[at], weight, (((1,), (1,)), ((), ())), preferred_element_type=jnp.float32
+            out[at, n * half : (n + 1) * half] = lax.dot_general(
+                hidden[at],
+                narrow[n * half : (n + 1) * half],
+                (((1,), (1,)), ((), ())),
+                preferred_element_type=jnp.float32,
             ).astype(out.dtype)
 
 
-def ffn(rows, kept, swapped):
+def ffn(rows, w):
     tokens, d = rows.shape
-    _, shard, three_ff = kept[0].shape
-    ff = three_ff // 3
-    blocks = [*kept, *swapped]
-    index = lax.axis_index("sp")
-    place = jnp.stack([index // 2, index % 2]).astype(jnp.int32)
-    return pl.pallas_call(
-        functools.partial(ffn_body, len(kept), len(swapped)),
+    ff = w.shape[1] // 3
+    assert TILES[-1][1] == 2 * ff
+    return pl.pallas_call(
+        ffn_body,
         out_shape=jax.ShapeDtypeStruct((tokens, d), rows.dtype),
-        in_specs=[SMEM] + [HBM] * (1 + len(blocks)),
+        in_specs=[HBM] * 2,
         out_specs=VMEM,
         scratch_shapes=[
             pltpu.VMEM((tokens, d), rows.dtype),
-            pltpu.VMEM((d // shard, shard, 3 * ff), rows.dtype),
+            pltpu.VMEM((d, 2 * ff), rows.dtype),
+            pltpu.VMEM((d, ff), rows.dtype),
             pltpu.VMEM((tokens, ff), rows.dtype),
             pltpu.SemaphoreType.DMA,
-            pltpu.SemaphoreType.DMA((len(blocks),)),
+            pltpu.SemaphoreType.DMA((len(TILES),)),
+            pltpu.SemaphoreType.DMA((2,)),
         ],
         compiler_params=LIMIT,
         cost_estimate=pl.CostEstimate(
             flops=6 * tokens * ff * d, bytes_accessed=6 * d * ff + 4 * tokens * d, transcendentals=tokens * ff
         ),
         name="ffn",
-    )(place, rows, *blocks)
-
-
-def finish_body(*refs):
-    middle, parts, out = refs[0], refs[1:-1], refs[-1]
-    at = 0
-    for part in parts:
-        width = part.shape[2]
-        total = part[0].astype(jnp.float32)
-        for k in range(1, part.shape[0]):
-            total = total + part[k].astype(jnp.float32)
-        mixed = total.astype(jnp.bfloat16).astype(jnp.float32)
-        here = slice(at, at + width)
-        out[:, here] = (middle[:, here].astype(jnp.float32) + 0.5 * mixed).astype(out.dtype)
-        at += width
+    )(rows, w)
+
+
+def finish_body(middle, parts, out):
+    total = parts[0].astype(jnp.float32)
+    for k in range(1, parts.shape[0]):
+        total = total + parts[k].astype(jnp.float32)
+    mixed = total.astype(jnp.bfloat16).astype(jnp.float32)
+    out[...] = (middle[...].astype(jnp.float32) + 0.5 * mixed).astype(out.dtype)
 
 
 def finish(middle, parts):
+    rows, d = middle.shape
+    tall = rows // ROW_STEPS
+    one = pl.BlockSpec((tall, d), lambda i: (i, 0))
+    all_parts = pl.BlockSpec((parts.shape[0], tall, d), lambda i: (0, i, 0))
     return pl.pallas_call(
         finish_body,
-        out_shape=jax.ShapeDtypeStruct(middle.shape, middle.dtype),
-        in_specs=[VMEM] * (1 + len(parts)),
-        out_specs=VMEM,
+        grid=(ROW_STEPS,),
+        out_shape=jax.ShapeDtypeStruct((rows, d), middle.dtype),
+        in_specs=[one, all_parts],
+        out_specs=one,
         name="finish",
-    )(middle, *parts)
+    )(middle, parts)
 
 
 def middle_body(residual, parts, gain, middle, normed):
@@ -202,14 +161,18 @@
 
 def middle_and_normed(residual, parts, gain):
     rows, d = residual.shape
+    tall = rows // ROW_STEPS
+    one = pl.BlockSpec((tall, d), lambda i: (i, 0))
+    all_parts = pl.BlockSpec((parts.shape[0], tall, d), lambda i: (0, i, 0))
     return pl.pallas_call(
         middle_body,
+        grid=(ROW_STEPS,),
         out_shape=(
             jax.ShapeDtypeStruct((rows, d), residual.dtype),
             jax.ShapeDtypeStruct((parts.shape[0], rows, d), residual.dtype),
         ),
-        in_specs=[VMEM] * 3,
-        out_specs=(VMEM, VMEM),
+        in_specs=[one, all_parts, pl.BlockSpec((1, d), lambda i: (0, 0))],
+        out_specs=(one, all_parts),
         name="middle",
     )(residual, parts, gain.reshape(1, d))
 
@@ -280,16 +243,14 @@
 ):
     n_tp = lax.axis_size("tp")
     d = residual.shape[1]
-    ring = Ring(pack(gate_weight, up_weight, down_weight))
-    queries, ring.block = lax.optimization_barrier((queries, ring.block))
-    ring.run()
+    whole = lax.all_gather(pack(gate_weight, up_weight, down_weight), "sp", axis=0, tiled=True)
     attended = attention(queries, key_heads, value_heads, documents, sink_logits)
     partial = jnp.dot(attended, out_weight, preferred_element_type=jnp.float32)
     parts = exchanged(split_up(partial.astype(jnp.bfloat16), n_tp))
     middle, copies = middle_and_normed(residual, parts, norm_gain)
     rows = exchanged(copies).reshape(-1, d)
-    mixed = exchanged(split_up(ffn(rows, ring.kept, ring.swapped), n_tp))
-    return finish(middle, [mixed])
+    mixed = exchanged(split_up(ffn(rows, whole), n_tp))
+    return finish(middle, mixed)
 
 
 def solution(mesh):

time: 226 us -> 190 us (0.84)
  the two profiles are of different devices: /device:TPU:40 before, /device:TPU:33 now
where the time goes in v4:
time: 190 us
  blocking collectives  59.9 us (32%)
  waiting for transfers between devices  43.6 us (23%)
  starting transfers between devices  28.8 us (15%)
  Pallas kernels  27.2 us (14%)
  between operations  13.6 us (7%)
  matrix products  8.25 us (4%)
  other arithmetic  4.47 us (2%)
  local copies, waits for them, and re-layouts  3.96 us (2%)
    all_to_all x2, blocking collectives, exchanged(): return lax.all_to_all(blocks, 'tp', 0, 0, tiled=True)  59.9 us
    all_to_all x1, waiting for transfers between devices, exchanged(): return lax.all_to_all(blocks, 'tp', 0, 0, tiled=True)  25.3 us
    ppermute x1, starting transfers between devices, attention(): after = lax.ppermute(edge(0), 'sp', down)  22.4 us
    all_gather x1, waiting for transfers between devices, on_device(): lax.all_gather(pack(gate_weight, up_weight, down_weight), 'sp', axis=0, t...  18.3 us
    pallas_call x1, Pallas kernels, ffn(): pl.pallas_call(ffn_body, out_shape=jax.ShapeDtypeStruct((tokens, d), rows...  16.8 us
    all_to_all x1, starting transfers between devices, exchanged(): return lax.all_to_all(blocks, 'tp', 0, 0, tiled=True)  4.52 us
    pallas_call x1, Pallas kernels, middle_and_normed(): pl.pallas_call(middle_body, grid=(ROW_STEPS,), out_shape=(jax.ShapeDtypeS...  4.41 us
  transfers between devices with their start and end apart: 4, of which 2 were waited for; matrix products, arithmetic and copies ran while one was open for 9% of the time, Pallas kernels for 2%

profile of v4, /device:TPU:33, one launch (start us, length us, event | category | flops | bytes accessed | tf_op | source)
XLA Modules:
  0.0 189.8 jit_solution(12103885527988952833)
XLA Ops:
  6.5 0.0 copy-start
  6.6 0.0 copy-start.2
  6.6 0.0 all-gather.2.cloned.1.call-start
  6.6 2.1 %pack.1 = bf16[64,4224]{1,0:T(8,128)(2,1)} custom-call(bf16[64,1408]{1,0:T(8,128)(2,1)} %gate.1, bf16[64,1408]{1,0:T(8,128)(2,1)} %up.1, bf16[64,1408]{1,0:T(8,128)(2,1)} %down.1), custom_call_target="tpu_custom_call" | custom-call | tf_op jit(solution)/shard_map/pack/pallas_call | solution.py:40
  8.7 0.1 all-gather.2.cloned.1.call-update
  8.8 0.7 convert_element_type.21
  9.5 0.8 constant_dynamic-update-slice_fusion.1
  10.3 0.8 constant_dynamic-update-slice_fusion
  11.2 0.1 broadcast_in_dim.13
  11.3 22.4 %collective-permute-start.1 = (bf16[144,128]{0,1:T(8,128)(2,1)S(1)}, bf16[144,128]{0,1:T(8,128)(2,1)S(1)}, u32[]{:S(2)}, u32[]{:S(2)}) collective-permute-start(bf16[144,128]{0,1:T(8,128)(2,1)S(1)} %pad_maximum_fusion.2), channel_id=1, source_target_pairs={{4,0},{8,4},{12,8},{16,12},{20,16},{24,20},{28,24},{32,28},{36,32}... | collective-permute-start | bytes 110600 | tf_op jit(solution)/shard_map/ppermute | solution.py:201
  33.6 0.1 broadcast_in_dim.12
  33.7 2.0 %collective-permute-start = (bf16[144,128]{0,1:T(8,128)(2,1)S(1)}, bf16[144,128]{0,1:T(8,128)(2,1)S(1)}, u32[]{:S(2)}, u32[]{:S(2)}) collective-permute-start(bf16[144,128]{0,1:T(8,128)(2,1)S(1)} %pad_maximum_fusion.1), channel_id=1, source_target_pairs={{0,4},{4,8},{8,12},{12,16},{16,20},{20,24},{24,28},{28,32},{32,36}... | collective-permute-start | bytes 110600 | tf_op jit(solution)/shard_map/ppermute | solution.py:200
  35.7 1.3 copy.14
  37.0 0.0 collective-permute-done.1
  37.0 0.0 collective-permute-done
  37.0 0.1 slice_reduce_fusion
  37.2 0.1 slice_reduce_fusion.1
  37.3 1.0 fusion.6
  38.3 2.0 %fusion.1 = (f32[8,512]{1,0:T(8,128)S(1)}, f32[768,512,8]{1,0,2:T(8,128)S(1)}) fusion(pred[512,768]{0,1:T(8,128)(4,1)S(1)} %fusion.6, bf16[512,8,64]{0,2,1:T(8,128)(2,1)S(1)} %bitcast.43, bf16[768,128]{0,1:T(8,128)(2,1)S(1)} %pad_maximum_fusion), kind=kOutput, calls=%fused_computation.4 | convolution fusion | flops 412086272 | bytes 13615104 | tf_op jit(solution)/shard_map/qkgd,jkd->kgqj/dot_general | solution.py:218
  40.4 0.0 copy-done.2
  40.4 0.1 broadcast_maximum_fusion
  40.5 2.6 %fusion = f32[8,512]{1,0:T(8,128)S(1)} fusion(f32[768,512,8]{1,0,2:T(8,128)S(1)} %get-tuple-element.14, f32[8,512]{1,0:T(8,128)S(1)} %broadcast_maximum_fusion, pred[512,768]{0,1:T(8,128)(4,1)S(1)} %fusion.6), kind=kLoop, calls=%fused_computation.3 | loop fusion | flops 12578816 | bytes 13008896 | tf_op jit(solution)/shard_map/reduce_sum | solution.py:225
  43.0 0.1 exponential_add_fusion
  43.1 0.0 copy-start.1
  43.1 3.6 %fusion.7 = bf16[64,8,512]{2,0,1:T(8,128)(2,1)S(1)} fusion(f32[8,512]{1,0:T(8,128)S(1)} %exponential_add_fusion, f32[8,512]{1,0:T(8,128)S(1)} %broadcast_maximum_fusion, f32[768,512,8]{1,0,2:T(8,128)S(1)} %get-tuple-element.14, pred[512,768]{0,1:T(8,128)(4,1)S(1)} %fusion.6, bf16[768,128]{0,1:T(8,128)(2,1)S(1)} %pad_maximum_fusion), kind=kOutput, calls=%fused_computation.12 | convolution fusion | flops 418643968 | bytes 13631488 | tf_op jit(solution)/shard_map/kgqj,jkd->qkgd/dot_general | solution.py:227
  46.7 0.0 copy-done
  46.7 2.6 %convolution_convert_fusion = bf16[512,2048]{1,0:T(8,128)(2,1)} fusion(bf16[512,512]{0,1:T(8,128)(2,1)S(1)} %bitcast.44, bf16[512,2048]{1,0:T(8,128)(2,1)S(1)} %copy-done), kind=kOutput, calls=%fused_computation.7 | convolution fusion | flops 1074790400 | bytes 4718592 | tf_op jit(solution)/shard_map/dot_general | solution.py:248
  49.3 4.5 %all-to-all-start = ((bf16[4,128,2048]{2,1,0:T(8,128)(2,1)}), bf16[4,128,2048]{2,1,0:T(8,128)(2,1)}, u32[]{:S(2)}, u32[]{:S(2)}) async-start(bf16[4,128,2048]{2,1,0:T(8,128)(2,1)} %bitcast.40), calls=%async_computation | async-start | bytes 4194304 | tf_op jit(solution)/shard_map/all_to_all | solution.py:181
  53.9 0.0 copy-done.1
  53.9 0.6 reshape.208.gain
  54.5 25.3 %all-to-all-done.parts = bf16[4,128,2048]{2,1,0:T(8,128)(2,1)} async-done(((bf16[4,128,2048]{2,1,0:T(8,128)(2,1)}), bf16[4,128,2048]{2,1,0:T(8,128)(2,1)}, u32[]{:S(2)}, u32[]{:S(2)}) %all-to-all-start) | async-done | bytes 2097184 | tf_op jit(solution)/shard_map/all_to_all | solution.py:181
  79.8 4.4 %middle.1 = (bf16[128,2048]{1,0:T(8,128)(2,1)}, bf16[4,128,2048]{2,1,0:T(8,128)(2,1)}) custom-call(bf16[128,2048]{1,0:T(8,128)(2,1)} %residual.1, bf16[4,128,2048]{2,1,0:T(8,128)(2,1)} %all-to-all-done.parts, bf16[1,2048]{1,0:T(2,128)(2,1)} %reshape.208.gain), custom_call_target="tpu_custom_call" | custom-call | tf_op jit(solution)/shard_map/middle/pallas_call | solution.py:167
  84.2 29.3 %all_to_all.15 = bf16[4,128,2048]{2,1,0:T(8,128)(2,1)} all-to-all(bf16[4,128,2048]{2,1,0:T(8,128)(2,1)} %get-tuple-element.8), channel_id=1, replica_groups=mesh['grp'=2,'sp'=32,'tp'=4] {'tp'}, dimensions={0} | all-to-all | bytes 4194304 | tf_op jit(solution)/shard_map/all_to_all | solution.py:181
  113.5 18.3 %all-gather.2.cloned.1.call-done.w = bf16[2048,4224]{1,0:T(8,128)(2,1)} async-done(((bf16[64,4224]{1,0:T(8,128)(2,1)}), bf16[2048,4224]{1,0:T(8,128)(2,1)}) %all-gather.2.cloned.1.call-update) | async-done | bytes 17301520 | tf_op jit(solution)/shard_map/all_gather | solution.py:246
  131.7 16.8 %ffn.1 = bf16[512,2048]{1,0:T(8,128)(2,1)} custom-call(bf16[512,2048]{1,0:T(8,128)(2,1)} %bitcast.41, bf16[2048,4224]{1,0:T(8,128)(2,1)} %all-gather.2.cloned.1.call-done.w), custom_call_target="tpu_custom_call" | custom-call | flops 8858370048 | bytes 21495808 | tf_op jit(solution)/shard_map/ffn/pallas_call | solution.py:103
  148.6 30.6 %all_to_all.16.parts = bf16[4,128,2048]{2,1,0:T(8,128)(2,1)} all-to-all(bf16[4,128,2048]{2,1,0:T(8,128)(2,1)} %bitcast.42), channel_id=1, replica_groups=mesh['grp'=2,'sp'=32,'tp'=4] {'tp'}, dimensions={0} | all-to-all | bytes 4194304 | tf_op jit(solution)/shard_map/all_to_all | solution.py:181
  179.2 3.8 %finish.1 = bf16[128,2048]{1,0:T(8,128)(2,1)} custom-call(bf16[128,2048]{1,0:T(8,128)(2,1)} %get-tuple-element.7.middle, bf16[4,128,2048]{2,1,0:T(8,128)(2,1)} %all_to_all.16.parts), custom_call_target="tpu_custom_call" | custom-call | tf_op jit(solution)/shard_map/finish/pallas_call | solution.py:138
  (11 shorter events, 0.1 us)
Async XLA Ops:
  6.5 40.2 %copy-start = (bf16[512,2048]{1,0:T(8,128)(2,1)S(1)}, bf16[512,2048]{1,0:T(8,128)(2,1)}, u32[]{:S(2)}) copy-start(bf16[512,2048]{1,0:T(8,128)(2,1)} %param.17) | copy-start | bytes 6291460
  6.6 33.8 %copy-start.2 = (f32[8]{0:T(128)S(1)}, f32[8]{0:T(128)}, u32[]{:S(2)}) copy-start(f32[8]{0:T(128)} %param.16) | copy-start | bytes 100
  6.6 125.2 %all-gather.2.cloned.1.call-start = ((), (), s32[]{:S(2)}) async-start(), calls=%async_computation.3 | async-start | bytes 17842176 | tf_op jit(solution)/shard_map/all_gather | solution.py:246
  11.3 25.7 %collective-permute-start.1 = (bf16[144,128]{0,1:T(8,128)(2,1)S(1)}, bf16[144,128]{0,1:T(8,128)(2,1)S(1)}, u32[]{:S(2)}, u32[]{:S(2)}) collective-permute-start(bf16[144,128]{0,1:T(8,128)(2,1)S(1)} %pad_maximum_fusion.2), channel_id=1, source_target_pairs={{4,0},{8,4},{12,8},{16,12},{20,16},{24,20},{28,24},{32,28},{36,32}... | collective-permute-start | bytes 110600 | tf_op jit(solution)/shard_map/ppermute | solution.py:201
  33.7 3.3 %collective-permute-start = (bf16[144,128]{0,1:T(8,128)(2,1)S(1)}, bf16[144,128]{0,1:T(8,128)(2,1)S(1)}, u32[]{:S(2)}, u32[]{:S(2)}) collective-permute-start(bf16[144,128]{0,1:T(8,128)(2,1)S(1)} %pad_maximum_fusion.1), channel_id=1, source_target_pairs={{0,4},{4,8},{8,12},{12,16},{16,20},{20,24},{24,28},{28,32},{32,36}... | collective-permute-start | bytes 110600 | tf_op jit(solution)/shard_map/ppermute | solution.py:200
  43.1 10.8 %copy-start.1 = (bf16[2048]{0:T(1024)(128)(2,1)S(1)}, bf16[2048]{0:T(1024)(128)(2,1)}, u32[]{:S(2)}) copy-start(bf16[2048]{0:T(1024)(128)(2,1)} %param.18) | copy-start | bytes 12292
  49.3 30.4 %all-to-all-start = ((bf16[4,128,2048]{2,1,0:T(8,128)(2,1)}), bf16[4,128,2048]{2,1,0:T(8,128)(2,1)}, u32[]{:S(2)}, u32[]{:S(2)}) async-start(bf16[4,128,2048]{2,1,0:T(8,128)(2,1)} %bitcast.40), calls=%async_computation | async-start | bytes 4194304 | tf_op jit(solution)/shard_map/all_to_all | solution.py:181
Sparse Core Ops, SparseCore 0:
  9.2 122.4 all-gather.1

commit v5 on v4

--- a/solution.py
+++ b/solution.py
@@ -11,13 +11,13 @@
 WINDOW = 128
 LANES = 128
 TALL = 256
-ROW_STEPS = 4
 TILES = ((0, 512), (512, 1536), (1536, 2816))
 
 epsilon = 1e-06
 masked = -1e30
 
 VMEM = pl.BlockSpec(memory_space=pltpu.VMEM)
+SMEM = pl.BlockSpec(memory_space=pltpu.SMEM)
 HBM = pl.BlockSpec(memory_space=pl.ANY)
 LIMIT = pltpu.CompilerParams(vmem_limit_bytes=56 * 1024 * 1024)
 
@@ -46,9 +46,10 @@
     )(gate, up, down)
 
 
-def ffn_body(rows, w, out, x, wide, narrow, hidden, xsem, sems, dsems):
+def ffn_body(places, rows, w, out, x, wide, narrow, hidden, xsem, sems, dsems):
     tokens, d = x.shape
     ff = hidden.shape[1]
+    tall = min(TALL, tokens)
     loads = [
         pltpu.make_async_copy(w.at[:, a:b], wide.at[:, a:b], sems.at[k])
         for k, (a, b) in enumerate(TILES)
@@ -62,17 +63,21 @@
         )
         for n in range(2)
     ]
-    load_x = pltpu.make_async_copy(rows, x, xsem)
-    load_x.start()
-    for c in loads + later:
+    each = rows.shape[1]
+    x_loads = [
+        pltpu.make_async_copy(rows.at[places[k]], x.at[k * each : (k + 1) * each], xsem.at[k])
+        for k in range(tokens // each)
+    ]
+    for c in x_loads + loads + later:
         c.start()
-    load_x.wait()
+    for c in x_loads:
+        c.wait()
     for c, (a, b) in zip(loads, TILES):
         c.wait()
 
-        @pl.loop(0, tokens // TALL)
+        @pl.loop(0, tokens // tall)
         def _(m, a=a, b=b):
-            at = pl.ds(m * TALL, TALL)
+            at = pl.ds(m * tall, tall)
             both = jnp.dot(x[at], wide[:, a:b], preferred_element_type=jnp.float32)
             for k in range((b - a) // (2 * LANES)):
                 gate = both[:, 2 * k * LANES : (2 * k + 1) * LANES]
@@ -85,9 +90,9 @@
     for n, c in enumerate(later):
         c.wait()
 
-        @pl.loop(0, tokens // TALL)
+        @pl.loop(0, tokens // tall)
         def _(m, n=n):
-            at = pl.ds(m * TALL, TALL)
+            at = pl.ds(m * tall, tall)
             out[at, n * half : (n + 1) * half] = lax.dot_general(
                 hidden[at],
                 narrow[n * half : (n + 1) * half],
@@ -96,21 +101,22 @@
             ).astype(out.dtype)
 
 
-def ffn(rows, w):
-    tokens, d = rows.shape
+def ffn(rows, w, blocks, name):
+    _, each, d = rows.shape
     ff = w.shape[1] // 3
+    tokens = each * len(blocks)
     assert TILES[-1][1] == 2 * ff
     return pl.pallas_call(
         ffn_body,
         out_shape=jax.ShapeDtypeStruct((tokens, d), rows.dtype),
-        in_specs=[HBM] * 2,
+        in_specs=[SMEM] + [HBM] * 2,
         out_specs=VMEM,
         scratch_shapes=[
             pltpu.VMEM((tokens, d), rows.dtype),
             pltpu.VMEM((d, 2 * ff), rows.dtype),
             pltpu.VMEM((d, ff), rows.dtype),
             pltpu.VMEM((tokens, ff), rows.dtype),
-            pltpu.SemaphoreType.DMA,
+            pltpu.SemaphoreType.DMA((len(blocks),)),
             pltpu.SemaphoreType.DMA((len(TILES),)),
             pltpu.SemaphoreType.DMA((2,)),
         ],
@@ -118,31 +124,69 @@
         cost_estimate=pl.CostEstimate(
             flops=6 * tokens * ff * d, bytes_accessed=6 * d * ff + 4 * tokens * d, transcendentals=tokens * ff
         ),
-        name="ffn",
-    )(rows, w)
-
-
-def finish_body(middle, parts, out):
-    total = parts[0].astype(jnp.float32)
-    for k in range(1, parts.shape[0]):
-        total = total + parts[k].astype(jnp.float32)
+        name=f"ffn_{name}",
+    )(jnp.stack(blocks).astype(jnp.int32), rows, w)
+
+
+def joined_body(near, half_up, half_down, up, down):
+    rows, half = up.shape[0], half_up.shape[0]
+    up[half:] = near[half:rows]
+    up[:half] = (near[:half].astype(jnp.float32) + half_up[...].astype(jnp.float32)).astype(up.dtype)
+    down[:half] = near[rows : rows + half]
+    down[half:] = (near[rows + half :].astype(jnp.float32) + half_down[...].astype(jnp.float32)).astype(
+        down.dtype
+    )
+
+
+def joined(near, half_up, half_down):
+    out = jax.ShapeDtypeStruct((near.shape[0] // 2, near.shape[1]), near.dtype)
+    return pl.pallas_call(
+        joined_body,
+        out_shape=(out, out),
+        in_specs=[VMEM] * 3,
+        out_specs=(VMEM, VMEM),
+        name="joined",
+    )(near, half_up, half_down)
+
+
+def finish_body(middle, own, from_down, from_up, out):
+    total = own[...].astype(jnp.float32) + from_down[...].astype(jnp.float32)
+    total = total + from_up[...].astype(jnp.float32)
     mixed = total.astype(jnp.bfloat16).astype(jnp.float32)
     out[...] = (middle[...].astype(jnp.float32) + 0.5 * mixed).astype(out.dtype)
 
 
-def finish(middle, parts):
-    rows, d = middle.shape
-    tall = rows // ROW_STEPS
-    one = pl.BlockSpec((tall, d), lambda i: (i, 0))
-    all_parts = pl.BlockSpec((parts.shape[0], tall, d), lambda i: (0, i, 0))
+def finish(*arrays):
     return pl.pallas_call(
         finish_body,
-        grid=(ROW_STEPS,),
-        out_shape=jax.ShapeDtypeStruct((rows, d), middle.dtype),
-        in_specs=[one, all_parts],
-        out_specs=one,
+        out_shape=jax.ShapeDtypeStruct(arrays[0].shape, arrays[0].dtype),
+        in_specs=[VMEM] * len(arrays),
+        out_specs=VMEM,
         name="finish",
-    )(middle, parts)
+    )(*arrays)
+
+
+def mixed_into(middle, rows, w):
+    size = lax.axis_size("tp")
+    assert size == 4
+    me = lax.axis_index("tp")
+    up = [(i, (i + 1) % size) for i in range(size)]
+    down = [(i, (i - 1) % size) for i in range(size)]
+    half = rows.shape[1] // 2
+    far = ffn(rows, w, [(me + 2) % size], "far")
+    half_up = moved(far[:half], up, "half_up")
+    half_down = moved(far[half:], down, "half_down")
+    near = ffn(rows, w, [(me + 1) % size, (me + 3) % size], "near")
+    to_up, to_down = joined(near, half_up, half_down)
+    from_down = moved(to_up, up, "whole_up")
+    from_up = moved(to_down, down, "whole_down")
+    own = ffn(rows, w, [me], "own")
+    return finish(middle, own, from_down, from_up)
+
+
+def moved(block, perm, name):
+    with jax.named_scope(name):
+        return lax.ppermute(block, "tp", perm)
 
 
 def middle_body(residual, parts, gain, middle, normed):
@@ -161,18 +205,14 @@
 
 def middle_and_normed(residual, parts, gain):
     rows, d = residual.shape
-    tall = rows // ROW_STEPS
-    one = pl.BlockSpec((tall, d), lambda i: (i, 0))
-    all_parts = pl.BlockSpec((parts.shape[0], tall, d), lambda i: (0, i, 0))
     return pl.pallas_call(
         middle_body,
-        grid=(ROW_STEPS,),
         out_shape=(
             jax.ShapeDtypeStruct((rows, d), residual.dtype),
             jax.ShapeDtypeStruct((parts.shape[0], rows, d), residual.dtype),
         ),
-        in_specs=[one, all_parts, pl.BlockSpec((1, d), lambda i: (0, 0))],
-        out_specs=(one, all_parts),
+        in_specs=[VMEM] * 3,
+        out_specs=(VMEM, VMEM),
         name="middle",
     )(residual, parts, gain.reshape(1, d))
 
@@ -242,15 +282,12 @@
     down_weight,
 ):
     n_tp = lax.axis_size("tp")
-    d = residual.shape[1]
     whole = lax.all_gather(pack(gate_weight, up_weight, down_weight), "sp", axis=0, tiled=True)
     attended = attention(queries, key_heads, value_heads, documents, sink_logits)
     partial = jnp.dot(attended, out_weight, preferred_element_type=jnp.float32)
     parts = exchanged(split_up(partial.astype(jnp.bfloat16), n_tp))
     middle, copies = middle_and_normed(residual, parts, norm_gain)
-    rows = exchanged(copies).reshape(-1, d)
-    mixed = exchanged(split_up(ffn(rows, whole), n_tp))
-    return finish(middle, mixed)
+    return mixed_into(middle, exchanged(copies), whole)
 
 
 def solution(mesh):

time: 190 us -> 186 us (0.979)
  blocking collectives: 59.9 us -> 0 us
  waiting for transfers between devices: 43.6 us -> 70.2 us
  Pallas kernels: 27.2 us -> 41.5 us
  starting transfers between devices: 28.8 us -> 39 us
  local copies, waits for them, and re-layouts: 3.96 us -> 7.42 us
    all_to_all x2 -> x0, blocking collectives: 59.9 us -> none  [exchanged(): return lax.all_to_all(blocks, 'tp', 0, 0, tiled=True)]
    all_to_all x1 -> x2, waiting for transfers between devices: 25.3 us -> 49.5 us  [exchanged(): return lax.all_to_all(blocks, 'tp', 0, 0, tiled=True)]
    pallas_call x1 -> x3, Pallas kernels: 16.8 us -> 30.7 us  [ffn(): pl.pallas_call(ffn_body, out_shape=jax.ShapeDtypeStruct((tokens, d), rows...]
    ppermute x0 -> x4, starting transfers between devices: none -> 5.47 us  [moved(): return lax.ppermute(block, 'tp', perm)]
    all_to_all x1 -> x2, starting transfers between devices: 4.52 us -> 9.26 us  [exchanged(): return lax.all_to_all(blocks, 'tp', 0, 0, tiled=True)]
    unnamed x8 -> x16, local copies, waits for them, and re-layouts: 2.11 us -> 4.5 us
    ppermute x0 -> x4, waiting for transfers between devices: none -> 2.02 us  [moved(): return lax.ppermute(block, 'tp', perm)]
    pallas_call x2 -> x3, Pallas kernels: 8.17 us -> 8.67 us  [the longest x1 3.63 us: middle_and_normed(): pl.pallas_call(middle_body, out_shape=(jax.ShapeDtypeStruct((rows, d), re...]
  transfers between devices with their start and end apart: 4 -> 9, of which waited for: 2 -> 4; matrix products, arithmetic and copies ran while one was open for 9% -> 9% of each run, Pallas kernels for 2% -> 13%
where the time goes in v5:
time: 186 us; the launch traced here: 185 us
  waiting for transfers between devices  70.2 us (38%)
  Pallas kernels  41.5 us (22%)
  starting transfers between devices  39 us (21%)
  between operations  13.7 us (7%)
  matrix products  8.27 us (4%)
  local copies, waits for them, and re-layouts  7.42 us (4%)
  other arithmetic  5.13 us (3%)
    all_to_all x2, waiting for transfers between devices, exchanged(): return lax.all_to_all(blocks, 'tp', 0, 0, tiled=True)  49.5 us
    pallas_call x3, Pallas kernels, ffn(): pl.pallas_call(ffn_body, out_shape=jax.ShapeDtypeStruct((tokens, d), rows...  30.7 us
    ppermute x1, starting transfers between devices, attention(): after = lax.ppermute(edge(0), 'sp', down)  22.4 us
    all_gather x1, waiting for transfers between devices, on_device(): lax.all_gather(pack(gate_weight, up_weight, down_weight), 'sp', axis=0, t...  18.7 us
    all_to_all x2, starting transfers between devices, exchanged(): return lax.all_to_all(blocks, 'tp', 0, 0, tiled=True)  9.26 us
    ppermute x4, starting transfers between devices, moved(): return lax.ppermute(block, 'tp', perm)  5.47 us
    unnamed x16, local copies, waits for them, and re-layouts  4.5 us
  transfers between devices with their start and end apart: 9, of which 4 were waited for; matrix products, arithmetic and copies ran while one was open for 9% of the time, Pallas kernels for 13%

profile of v5, /device:TPU:33, one launch (start us, length us, event | category | flops | bytes accessed | tf_op | source)
XLA Modules:
  0.0 185.3 jit_solution(3984386730085620723)
XLA Ops:
  6.6 2.1 %pack.1 = bf16[64,4224]{1,0:T(8,128)(2,1)} custom-call(bf16[64,1408]{1,0:T(8,128)(2,1)} %gate.1, bf16[64,1408]{1,0:T(8,128)(2,1)} %up.1, bf16[64,1408]{1,0:T(8,128)(2,1)} %down.1), custom_call_target="tpu_custom_call" | custom-call | tf_op jit(solution)/shard_map/pack/pallas_call | solution.py:40
  8.7 0.1 all-gather.2.cloned.1.call-update
  8.8 0.7 convert_element_type.21
  9.4 0.8 constant_dynamic-update-slice_fusion.1
  10.3 0.8 constant_dynamic-update-slice_fusion
  11.2 0.1 broadcast_in_dim.13
  11.3 22.4 %collective-permute-start.1 = (bf16[144,128]{0,1:T(8,128)(2,1)S(1)}, bf16[144,128]{0,1:T(8,128)(2,1)S(1)}, u32[]{:S(2)}, u32[]{:S(2)}) collective-permute-start(bf16[144,128]{0,1:T(8,128)(2,1)S(1)} %pad_maximum_fusion.2), channel_id=1, source_target_pairs={{4,0},{8,4},{12,8},{16,12},{20,16},{24,20},{28,24},{32,28},{36,32}... | collective-permute-start | bytes 110600 | tf_op jit(solution)/shard_map/ppermute | solution.py:241
  33.6 0.1 broadcast_in_dim.12
  33.7 2.0 %collective-permute-start = (bf16[144,128]{0,1:T(8,128)(2,1)S(1)}, bf16[144,128]{0,1:T(8,128)(2,1)S(1)}, u32[]{:S(2)}, u32[]{:S(2)}) collective-permute-start(bf16[144,128]{0,1:T(8,128)(2,1)S(1)} %pad_maximum_fusion.1), channel_id=1, source_target_pairs={{0,4},{4,8},{8,12},{12,16},{16,20},{20,24},{24,28},{28,32},{32,36}... | collective-permute-start | bytes 110600 | tf_op jit(solution)/shard_map/ppermute | solution.py:240
  35.7 1.3 copy.14
  37.0 0.0 collective-permute-done.1
  37.0 0.0 collective-permute-done
  37.0 0.1 slice_reduce_fusion
  37.1 0.1 slice_reduce_fusion.1
  37.3 1.0 fusion.6
  38.3 2.0 %fusion.1 = (f32[8,512]{1,0:T(8,128)S(1)}, f32[768,512,8]{1,0,2:T(8,128)S(1)}) fusion(pred[512,768]{0,1:T(8,128)(4,1)S(1)} %fusion.6, bf16[512,8,64]{0,2,1:T(8,128)(2,1)S(1)} %bitcast.43, bf16[768,128]{0,1:T(8,128)(2,1)S(1)} %pad_maximum_fusion), kind=kOutput, calls=%fused_computation.4 | convolution fusion | flops 412086272 | bytes 13615104 | tf_op jit(solution)/shard_map/qkgd,jkd->kgqj/dot_general | solution.py:258
  40.4 0.0 copy-done.6
  40.4 0.1 broadcast_maximum_fusion
  40.4 2.6 %fusion = f32[8,512]{1,0:T(8,128)S(1)} fusion(f32[768,512,8]{1,0,2:T(8,128)S(1)} %get-tuple-element.20, f32[8,512]{1,0:T(8,128)S(1)} %broadcast_maximum_fusion, pred[512,768]{0,1:T(8,128)(4,1)S(1)} %fusion.6), kind=kLoop, calls=%fused_computation.3 | loop fusion | flops 12578816 | bytes 13008896 | tf_op jit(solution)/shard_map/reduce_sum | solution.py:265
  43.0 0.1 exponential_add_fusion
  43.1 3.6 %fusion.7 = bf16[64,8,512]{2,0,1:T(8,128)(2,1)S(1)} fusion(f32[8,512]{1,0:T(8,128)S(1)} %exponential_add_fusion, f32[8,512]{1,0:T(8,128)S(1)} %broadcast_maximum_fusion, f32[768,512,8]{1,0,2:T(8,128)S(1)} %get-tuple-element.20, pred[512,768]{0,1:T(8,128)(4,1)S(1)} %fusion.6, bf16[768,128]{0,1:T(8,128)(2,1)S(1)} %pad_maximum_fusion), kind=kOutput, calls=%fused_computation.12 | convolution fusion | flops 418643968 | bytes 13631488 | tf_op jit(solution)/shard_map/kgqj,jkd->qkgd/dot_general | solution.py:267
  46.7 2.6 %convolution_convert_fusion = bf16[512,2048]{1,0:T(8,128)(2,1)} fusion(bf16[512,512]{0,1:T(8,128)(2,1)S(1)} %bitcast.44, bf16[512,2048]{1,0:T(8,128)(2,1)S(1)} %copy-done), kind=kOutput, calls=%fused_computation.7 | convolution fusion | flops 1074790400 | bytes 4718592 | tf_op jit(solution)/shard_map/dot_general | solution.py:287
  49.3 4.5 %all-to-all-start = ((bf16[4,128,2048]{2,1,0:T(8,128)(2,1)}), bf16[4,128,2048]{2,1,0:T(8,128)(2,1)}, u32[]{:S(2)}, u32[]{:S(2)}) async-start(bf16[4,128,2048]{2,1,0:T(8,128)(2,1)} %bitcast.42), calls=%async_computation | async-start | bytes 4194304 | tf_op jit(solution)/shard_map/all_to_all | solution.py:221
  53.9 0.6 reshape.202.gain
  54.5 25.3 %all-to-all-done.parts = bf16[4,128,2048]{2,1,0:T(8,128)(2,1)} async-done(((bf16[4,128,2048]{2,1,0:T(8,128)(2,1)}), bf16[4,128,2048]{2,1,0:T(8,128)(2,1)}, u32[]{:S(2)}, u32[]{:S(2)}) %all-to-all-start) | async-done | bytes 2097184 | tf_op jit(solution)/shard_map/all_to_all | solution.py:221
  79.8 3.6 %middle.1 = (bf16[128,2048]{1,0:T(8,128)(2,1)}, bf16[4,128,2048]{2,1,0:T(8,128)(2,1)}) custom-call(bf16[128,2048]{1,0:T(8,128)(2,1)} %residual.1, bf16[4,128,2048]{2,1,0:T(8,128)(2,1)} %all-to-all-done.parts, bf16[1,2048]{1,0:T(2,128)(2,1)} %reshape.202.gain), custom_call_target="tpu_custom_call" | custom-call | tf_op jit(solution)/shard_map/middle/pallas_call | solution.py:208
  83.4 4.7 %all-to-all-start.1 = ((bf16[4,128,2048]{2,1,0:T(8,128)(2,1)}), bf16[4,128,2048]{2,1,0:T(8,128)(2,1)}, u32[]{:S(2)}, u32[]{:S(2)}) async-start(bf16[4,128,2048]{2,1,0:T(8,128)(2,1)} %get-tuple-element.10), calls=%async_computation.1 | async-start | bytes 4194304 | tf_op jit(solution)/shard_map/all_to_all | solution.py:221
  88.2 0.7 pad_add_fusion.places
  88.9 24.2 %all-to-all-done.1.rows = bf16[4,128,2048]{2,1,0:T(8,128)(2,1)} async-done(((bf16[4,128,2048]{2,1,0:T(8,128)(2,1)}), bf16[4,128,2048]{2,1,0:T(8,128)(2,1)}, u32[]{:S(2)}, u32[]{:S(2)}) %all-to-all-start.1) | async-done | bytes 2097184 | tf_op jit(solution)/shard_map/all_to_all | solution.py:221
  113.0 18.7 %all-gather.2.cloned.1.call-done.w = bf16[2048,4224]{1,0:T(8,128)(2,1)} async-done(((bf16[64,4224]{1,0:T(8,128)(2,1)}), bf16[2048,4224]{1,0:T(8,128)(2,1)}) %all-gather.2.cloned.1.call-update) | async-done | bytes 17301520 | tf_op jit(solution)/shard_map/all_gather | solution.py:285
  131.7 9.4 %ffn_far.1 = bf16[128,2048]{1,0:T(8,128)(2,1)} custom-call(s32[1]{0:T(128)} %bitcast.13.places, bf16[4,128,2048]{2,1,0:T(8,128)(2,1)} %all-to-all-done.1.rows, bf16[2048,4224]{1,0:T(8,128)(2,1)} %all-gather.2.cloned.1.call-done.w), custom_call_target="tpu_custom_call" | custom-call | flops 2214592512 | bytes 18350080 | tf_op jit(solution)/shard_map/ffn_far/pallas_call | solution.py:109
  141.1 1.1 fusion.15
  142.2 1.3 collective-permute-start.2
  143.5 1.5 collective-permute-start.3
  145.0 11.9 %ffn_near.1.near = bf16[256,2048]{1,0:T(8,128)(2,1)} custom-call(s32[2]{0:T(128)} %pad_add_fusion.places, bf16[4,128,2048]{2,1,0:T(8,128)(2,1)} %all-to-all-done.1.rows, bf16[2048,4224]{1,0:T(8,128)(2,1)} %all-gather.2.cloned.1.call-done.w), custom_call_target="tpu_custom_call" | custom-call | flops 4429185024 | bytes 19398656 | tf_op jit(solution)/shard_map/ffn_near/pallas_call | solution.py:109
  156.9 0.0 collective-permute-done.2.half_up
  156.9 0.0 collective-permute-done.3.half_down
  156.9 0.7 copy-done.3
  157.6 0.7 copy-done.4
  158.3 2.4 %joined.1 = (bf16[128,2048]{1,0:T(8,128)(2,1)}, bf16[128,2048]{1,0:T(8,128)(2,1)}) custom-call(bf16[256,2048]{1,0:T(8,128)(2,1)} %ffn_near.1.near, bf16[64,2048]{1,0:T(8,128)(2,1)} %copy-done.3, bf16[64,2048]{1,0:T(8,128)(2,1)} %copy-done.4), custom_call_target="tpu_custom_call" | custom-call | tf_op jit(solution)/shard_map/joined/pallas_call | solution.py:143
  160.7 0.0 collective-permute-start.4
  160.7 2.7 %collective-permute-start.5 = (bf16[128,2048]{1,0:T(8,128)(2,1)}, bf16[128,2048]{1,0:T(8,128)(2,1)S(1)}, u32[]{:S(2)}, u32[]{:S(2)}) collective-permute-start(bf16[128,2048]{1,0:T(8,128)(2,1)} %get-tuple-element.12), channel_id=1, source_target_pairs={{0,3},{1,0},{2,1},{3,2},{4,7},{5,4},{6,5},{7,6},{8,11},{9,8},{10,9... | collective-permute-start | bytes 1572872 | tf_op jit(solution)/shard_map/whole_down/ppermute | solution.py:189
  163.4 9.4 %ffn_own.1.own = bf16[128,2048]{1,0:T(8,128)(2,1)} custom-call(s32[1]{0:T(128)} %bitcast.10.places, bf16[4,128,2048]{2,1,0:T(8,128)(2,1)} %all-to-all-done.1.rows, bf16[2048,4224]{1,0:T(8,128)(2,1)} %all-gather.2.cloned.1.call-done.w), custom_call_target="tpu_custom_call" | custom-call | flops 2214592512 | bytes 18350080 | tf_op jit(solution)/shard_map/ffn_own/pallas_call | solution.py:109
  172.8 2.0 %collective-permute-done.4.from_down = bf16[128,2048]{1,0:T(8,128)(2,1)S(1)} collective-permute-done((bf16[128,2048]{1,0:T(8,128)(2,1)}, bf16[128,2048]{1,0:T(8,128)(2,1)S(1)}, u32[]{:S(2)}, u32[]{:S(2)}) %collective-permute-start.4) | collective-permute-done | bytes 524320 | tf_op jit(solution)/shard_map/whole_up/ppermute | solution.py:189
  174.8 0.0 collective-permute-done.5.from_up
  174.8 0.8 copy-done.1
  175.6 0.2 copy-done.2
  175.8 2.6 %finish.1 = bf16[128,2048]{1,0:T(8,128)(2,1)} custom-call(bf16[128,2048]{1,0:T(8,128)(2,1)} %get-tuple-element.9.middle, bf16[128,2048]{1,0:T(8,128)(2,1)} %ffn_own.1.own, bf16[128,2048]{1,0:T(8,128)(2,1)} %copy-done.1, bf16[128,2048]{1,0:T(8,128)(2,1)} %copy-done.2), custom_call_target="tpu_custom_call" | custom-call | tf_op jit(solution)/shard_map/finish/pallas_call | solution.py:160
  (21 shorter events, 0.1 us)
Async XLA Ops:
  6.5 40.2 %copy-start = (bf16[512,2048]{1,0:T(8,128)(2,1)S(1)}, bf16[512,2048]{1,0:T(8,128)(2,1)}, u32[]{:S(2)}) copy-start(bf16[512,2048]{1,0:T(8,128)(2,1)} %param.17) | copy-start | bytes 6291460
  6.6 33.8 %copy-start.6 = (f32[8]{0:T(128)S(1)}, f32[8]{0:T(128)}, u32[]{:S(2)}) copy-start(f32[8]{0:T(128)} %param.16) | copy-start | bytes 100
  6.6 125.2 %all-gather.2.cloned.1.call-start = ((), (), s32[]{:S(2)}) async-start(), calls=%async_computation.2 | async-start | bytes 17842176 | tf_op jit(solution)/shard_map/all_gather | solution.py:285
  11.3 25.7 %collective-permute-start.1 = (bf16[144,128]{0,1:T(8,128)(2,1)S(1)}, bf16[144,128]{0,1:T(8,128)(2,1)S(1)}, u32[]{:S(2)}, u32[]{:S(2)}) collective-permute-start(bf16[144,128]{0,1:T(8,128)(2,1)S(1)} %pad_maximum_fusion.2), channel_id=1, source_target_pairs={{4,0},{8,4},{12,8},{16,12},{20,16},{24,20},{28,24},{32,28},{36,32}... | collective-permute-start | bytes 110600 | tf_op jit(solution)/shard_map/ppermute | solution.py:241
  33.7 3.3 %collective-permute-start = (bf16[144,128]{0,1:T(8,128)(2,1)S(1)}, bf16[144,128]{0,1:T(8,128)(2,1)S(1)}, u32[]{:S(2)}, u32[]{:S(2)}) collective-permute-start(bf16[144,128]{0,1:T(8,128)(2,1)S(1)} %pad_maximum_fusion.1), channel_id=1, source_target_pairs={{0,4},{4,8},{8,12},{12,16},{16,20},{20,24},{24,28},{28,32},{32,36}... | collective-permute-start | bytes 110600 | tf_op jit(solution)/shard_map/ppermute | solution.py:240
  43.1 10.8 %copy-start.5 = (bf16[2048]{0:T(1024)(128)(2,1)S(1)}, bf16[2048]{0:T(1024)(128)(2,1)}, u32[]{:S(2)}) copy-start(bf16[2048]{0:T(1024)(128)(2,1)} %param.18) | copy-start | bytes 12292
  49.3 30.5 %all-to-all-start = ((bf16[4,128,2048]{2,1,0:T(8,128)(2,1)}), bf16[4,128,2048]{2,1,0:T(8,128)(2,1)}, u32[]{:S(2)}, u32[]{:S(2)}) async-start(bf16[4,128,2048]{2,1,0:T(8,128)(2,1)} %bitcast.42), calls=%async_computation | async-start | bytes 4194304 | tf_op jit(solution)/shard_map/all_to_all | solution.py:221
  83.4 29.6 %all-to-all-start.1 = ((bf16[4,128,2048]{2,1,0:T(8,128)(2,1)}), bf16[4,128,2048]{2,1,0:T(8,128)(2,1)}, u32[]{:S(2)}, u32[]{:S(2)}) async-start(bf16[4,128,2048]{2,1,0:T(8,128)(2,1)} %get-tuple-element.10), calls=%async_computation.1 | async-start | bytes 4194304 | tf_op jit(solution)/shard_map/all_to_all | solution.py:221
  142.2 14.7 %collective-permute-start.2 = (bf16[64,2048]{1,0:T(8,128)(2,1)S(1)}, bf16[64,2048]{1,0:T(8,128)(2,1)S(1)}, u32[]{:S(2)}, u32[]{:S(2)}) collective-permute-start(bf16[64,2048]{1,0:T(8,128)(2,1)S(1)} %get-tuple-element.14), channel_id=1, source_target_pairs={{0,1},{1,2},{2,3},{3,0},{4,5},{5,6},{6,7},{7,4},{8,9},{9,10},{10,1... | collective-permute-start | bytes 786440 | tf_op jit(solution)/shard_map/half_up/ppermute | solution.py:189
  143.5 13.5 %collective-permute-start.3 = (bf16[64,2048]{1,0:T(8,128)(2,1)S(1)}, bf16[64,2048]{1,0:T(8,128)(2,1)S(1)}, u32[]{:S(2)}, u32[]{:S(2)}) collective-permute-start(bf16[64,2048]{1,0:T(8,128)(2,1)S(1)} %get-tuple-element.13), channel_id=1, source_target_pairs={{0,3},{1,0},{2,1},{3,2},{4,7},{5,4},{6,5},{7,6},{8,11},{9,8},{10,9... | collective-permute-start | bytes 786440 | tf_op jit(solution)/shard_map/half_down/ppermute | solution.py:189
  156.9 0.7 copy-start.3
  157.6 0.7 copy-start.4
  160.7 14.1 %collective-permute-start.4 = (bf16[128,2048]{1,0:T(8,128)(2,1)}, bf16[128,2048]{1,0:T(8,128)(2,1)S(1)}, u32[]{:S(2)}, u32[]{:S(2)}) collective-permute-start(bf16[128,2048]{1,0:T(8,128)(2,1)} %get-tuple-element.11), channel_id=1, source_target_pairs={{0,1},{1,2},{2,3},{3,0},{4,5},{5,6},{6,7},{7,4},{8,9},{9,10},{10,1... | collective-permute-start | bytes 1572872 | tf_op jit(solution)/shard_map/whole_up/ppermute | solution.py:189
  160.7 14.1 %collective-permute-start.5 = (bf16[128,2048]{1,0:T(8,128)(2,1)}, bf16[128,2048]{1,0:T(8,128)(2,1)S(1)}, u32[]{:S(2)}, u32[]{:S(2)}) collective-permute-start(bf16[128,2048]{1,0:T(8,128)(2,1)} %get-tuple-element.12), channel_id=1, source_target_pairs={{0,3},{1,0},{2,1},{3,2},{4,7},{5,4},{6,5},{7,6},{8,11},{9,8},{10,9... | collective-permute-start | bytes 1572872 | tf_op jit(solution)/shard_map/whole_down/ppermute | solution.py:189
  174.8 0.8 copy-start.1
  174.8 1.0 copy-start.2
Sparse Core Ops, SparseCore 0:
  9.2 122.4 all-gather.1
